TPU v7x, 128 devices: a whole 4x4x4 slice. The times are simulated.
128 devices in a mesh: fs: 16 (over z, x), tp: 8 (over y, core).
Axes of the slice: x: 4, y: 4, z: 4, core: 2. Of those that a mesh axis runs over, the one named last changes fastest.
Arguments:
- saved_input: bfloat16 [49152, 2048], P('fs'), may hold values from -6 to 6
- proj_cot: bfloat16 [3, 49152, 2048], P(None, 'fs', 'tp'), may hold values from -0.02734375 to 0.02734375
- log_cache: float32 [16, 49152], P(None, 'fs'), as said below
- cache_cot: float32 [16, 49152], P(None, 'fs'), may hold values from -0.02734375 to 0.02734375
- proj_master: float32 [3, 2048, 2048], P(None, 'fs', 'tp'), may hold values from -0.125 to 0.125
- factors: bfloat16 [3, 2048, 256], P(None, 'fs'), may hold values from -0.125 to 0.125
- first_moment: float32 [3, 256, 2048], P(None, None, 'tp'), may hold values from -6 to 6
- second_moment: float32 [3, 256, 2048], P(None, None, 'tp'), may hold values from 0.01 to 10
- gate_master: float32 [16, 2048], replicated, may hold values from -0.125 to 0.125
- gate_first: float32 [16, 2048], replicated, may hold values from -6 to 6
- gate_second: float32 [16, 2048], replicated, may hold values from 0.1 to 3
Outputs:
- proj_step: float32 [3, 2048, 2048], P(None, 'fs', 'tp')
- proj_new: float32 [3, 2048, 2048], P(None, 'fs', 'tp')
- proj_copy: bfloat16 [3, 2048, 2048], P(None, None, 'tp')
- first_new: float32 [3, 256, 2048], P(None, None, 'tp')
- second_new: float32 [3, 256, 2048], P(None, None, 'tp')
- gate_new: float32 [16, 2048], replicated
- gate_copy: bfloat16 [16, 2048], replicated
- gate_first_new: float32 [16, 2048], replicated
- gate_second_new: float32 [16, 2048], replicated
Inputs may be any that keep to these rules, and one draw needn't show every extreme that they name: `log_cache`: each head's values never rise along positions.
All inputs are finite; a program needn't handle non-finite values.
Results may differ from a plain program's by a relative error of at most 0.0004.
Values may be sent and summed in bfloat16 or wider, within the bound.
No kernel may reach another device: no remote copies, remote signals or barrier semaphores. Data moves between devices by JAX's collectives and lax.ppermute only.
A program may use at most 128 MiB of HBM per device.

v0:
```python
import jax
import jax.numpy as jnp
from jax import lax
from jax.sharding import PartitionSpec as P

BETA_ONE = 0.8
BETA_TWO = 0.9
LEARN = 0.001


def from_behind(x, axis, by):
    peers = lax.axis_size(axis)
    pairs = [(i, i + by) for i in range(peers) if 0 <= i + by < peers]
    return lax.ppermute(x, axis, pairs)


def from_everyone(x, axis):
    copies = jnp.broadcast_to(x, (lax.axis_size(axis), *x.shape))
    return lax.all_to_all(copies, axis, split_axis=0, concat_axis=0, tiled=True)


def folded_in_pairs(pieces, combine):
    while len(jax.tree.leaves(pieces)[0]) > 1:
        pieces = jax.vmap(combine)(*(pieces[side::2] for side in (0, 1)))
    return pieces[0]


def carried_in(x, axis, combine, identity):
    peers, place = (lax.axis_size(axis), lax.axis_index(axis))
    passed = jnp.arange(peers) > place

    def kept(part, zero, own):
        part = jnp.where(
            passed.reshape(-1, *(1 for _ in own.shape)), part, jnp.asarray(zero, own.dtype)
        )
        return part[::-1]

    pieces = from_everyone(x, axis)
    return folded_in_pairs(kept(pieces, identity, x), combine)


def rows_for(lines, peers):
    spare = -lines.shape[0] % peers
    if not spare:
        return lines
    return jnp.concatenate([lines, jnp.zeros((spare, *lines.shape[1:]), lines.dtype)])


def in_order(parts, dim):
    parts = jnp.moveaxis(parts, 0, dim)
    lengths = parts.shape
    return parts.reshape(*lengths[:dim], lengths[dim] * lengths[dim + 1], *lengths[dim + 2 :])


def collect(x, axis, dim):
    return in_order(from_everyone(x, axis), dim)


def cut_along(x, dim, peers):
    lengths = x.shape
    parts = x.reshape(*lengths[:dim], peers, lengths[dim] // peers, *lengths[dim + 1 :])
    return jnp.moveaxis(parts, dim, 0)


def summed_on_arrival(x, axis, dim):
    parts = cut_along(x, dim, lax.axis_size(axis))
    arrived = lax.all_to_all(parts, axis, split_axis=0, concat_axis=0, tiled=True)
    return arrived.sum(axis=0)


def total_of(x, axes):
    padded = rows_for(x, lax.axis_size(axes))
    whole = collect(summed_on_arrival(padded, axes, 0), axes, 0)
    return lax.slice_in_dim(whole, 0, len(x)).reshape(x.shape)


def in_one(arrays, axis):
    ravelled, at, finished = (jnp.concatenate([a.reshape(-1) for a in arrays]), 0, [])
    so_far = total_of(ravelled, axis)
    for a in arrays:
        finished.append(so_far[at : at + a.size].reshape(a.shape))
        at += a.size
    return tuple(finished)


def over_copies(x, axis):
    everything = from_everyone(x, axis)
    return jnp.sum(everything, axis=0)


def add_pair(earlier, later_part):
    return earlier + later_part


def local(
    saved_input,
    proj_cot,
    log_cache,
    cache_cot,
    proj_master,
    factors,
    first_moment,
    second_moment,
    gate_master,
    gate_first,
    gate_second,
):
    heads = log_cache.shape[0]
    edge = from_behind(log_cache[:, -1:], "fs", 1)
    previous = jnp.concatenate([edge, log_cache[:, :-1]], axis=1)
    gate_logarithm = log_cache - previous
    carried = carried_in(
        jnp.sum(cache_cot, axis=1), "fs", add_pair, jnp.zeros((heads,), jnp.float32)
    )
    later = jnp.flip(jnp.cumsum(jnp.flip(cache_cot, 1), axis=1), 1) + carried[:, None]
    gate_cot = (later * -jnp.expm1(gate_logarithm)).astype(jnp.bfloat16)
    gate_part = jnp.dot(gate_cot, saved_input, preferred_element_type=jnp.float32)
    all_factors = lax.all_gather(factors, "fs", axis=1, tiled=True)
    reduced = jnp.einsum(
        "td,rdk->rtk", saved_input, all_factors, preferred_element_type=jnp.float32
    )
    upper_half = lax.optimization_barrier(reduced.astype(jnp.bfloat16))
    lower_half = (reduced - upper_half.astype(jnp.float32)).astype(jnp.bfloat16)
    low_part = jnp.einsum("rtk,rtw->rkw", upper_half, proj_cot, preferred_element_type=jnp.float32)
    low_part = low_part + jnp.einsum(
        "rtk,rtw->rkw", lower_half, proj_cot, preferred_element_type=jnp.float32
    )
    low, gate_grad = in_one((low_part, gate_part), "fs")
    first_new = BETA_ONE * first_moment + (1.0 - BETA_ONE) * low
    second_new = BETA_TWO * second_moment + (1.0 - BETA_TWO) * low * low
    direction = first_new / jnp.sqrt(second_new)
    squares = over_copies(jnp.sum(direction * direction), "tp")
    entries = direction.shape[0] * direction.shape[1] * direction.shape[2] * lax.axis_size("tp")
    scale = lax.rsqrt(squares / entries + 1e-06)
    product = jnp.einsum(
        "rdk,rkw->rdw", factors.astype(jnp.float32), direction, precision=lax.Precision.HIGHEST
    )
    proj_step = scale * product
    proj_new = proj_master - LEARN * proj_step
    proj_copy = lax.all_gather(proj_new.astype(jnp.bfloat16), "fs", axis=1, tiled=True)
    gate_first_new = BETA_ONE * gate_first + (1.0 - BETA_ONE) * gate_grad
    gate_second_new = BETA_TWO * gate_second + (1.0 - BETA_TWO) * gate_grad * gate_grad
    gate_new = gate_master - LEARN * gate_first_new / jnp.sqrt(gate_second_new)
    gate_copy = gate_new.astype(jnp.bfloat16)
    return (
        proj_step,
        proj_new,
        proj_copy,
        first_new,
        second_new,
        gate_new,
        gate_copy,
        gate_first_new,
        gate_second_new,
    )


def solution(mesh):
    placed = (
        P("fs", None),
        P(None, "fs", "tp"),
        P(None, "fs"),
        P(None, "fs"),
        P(None, "fs", "tp"),
        P(None, "fs", None),
        P(None, None, "tp"),
        P(None, None, "tp"),
        P(),
        P(),
        P(),
    )
    return jax.shard_map(
        local,
        mesh=mesh,
        in_specs=placed,
        out_specs=(
            P(None, "fs", "tp"),
            P(None, "fs", "tp"),
            P(None, None, "tp"),
            P(None, None, "tp"),
            P(None, None, "tp"),
            P(),
            P(),
            P(),
            P(),
        ),
        check_vma=False,
    )
```

profile of v0, /device:TPU:0, one launch (start us, length us, event | category | flops | bytes accessed | tf_op | source)
XLA Modules:
  0.0 206.4 jit_solution(16304343146461172091)
XLA Ops:
  7.2 0.0 all-gather.3.cloned.1.call-start
  7.2 1.7 copy.44
  9.0 0.0 all-gather.3.cloned.1.call-update
  9.0 1.1 reduce_sum.36
  10.1 0.6 broadcast_in_dim.22
  10.7 8.0 %all-to-all-start = ((f32[16,1,16]{2,1,0:T(1,128)}), f32[16,1,16]{2,1,0:T(1,128)S(1)}, u32[]{:S(2)}, u32[]{:S(2)}) async-start(f32[16,1,16]{2,1,0:T(1,128)} %broadcast_in_dim.22), calls=%async_computation | async-start | bytes 16384 | tf_op jit(solution)/shard_map/all_to_all | solution.py:19
  18.7 0.8 slice.65
  19.4 3.8 %collective-permute-start = (f32[16,1]{1,0:T(8,128)S(1)}, f32[16,1]{1,0:T(8,128)S(1)}, u32[]{:S(2)}, u32[]{:S(2)}) collective-permute-start(f32[16,1]{1,0:T(8,128)S(1)} %slice.65), channel_id=1, source_target_pairs={{0,8},{8,16},{16,24},{24,32},{32,40},{40,48},{48,56},{56,64},{64,7... | collective-permute-start | bytes 200 | tf_op jit(solution)/shard_map/ppermute | solution.py:14
  23.3 9.3 %rev.8 = f32[16,3072]{1,0:T(8,128)S(1)} reverse(f32[16,3072]{1,0:T(8,128)} %param.14), dimensions={1} | reverse | bytes 393216 | tf_op jit(solution)/shard_map/jit(_flip)/rev | solution.py:115
  32.6 4.6 %reduce-window.6 = f32[16,24,128]{2,1,0:T(8,128)S(1)} reduce-window(f32[16,24,128]{2,1,0:T(8,128)S(1)} %bitcast.46, f32[]{:T(128)} %constant.11.clone.1), window={size=1x1x128 pad=0_0x0_0x127_0}, to_apply=%region_0.0 | reduce-window | flops 6242304 | bytes 393220 | tf_op jit(solution)/shard_map/reduce-window
  37.3 0.2 slice_reduce_fusion
  37.5 0.2 reduce-window.9
  37.7 0.1 broadcast_add_fusion
  37.8 1.8 rev.9
  39.6 0.0 all-to-all-done
  39.6 0.1 broadcast_select_fusion
  39.9 0.0 collective-permute-done
  39.9 6.6 %convolution_bitcast_fusion = f32[2,16,8,128]{3,2,1,0:T(8,128)S(1)} fusion(bf16[3072,2048]{1,0:T(8,128)(2,1)} %param.11, f32[16,3072]{1,0:T(8,128)} %param.13, f32[16,3071]{1,0:T(8,128)} %bitcast.43, f32[16,1]{1,0:T(8,128)S(1)} %collective-permute-done, f32[16,3072]{1,0:T(8,128)S(1)} %rev.9, f32[16]{0:T(128)S(1)} %add_bitcast_fusion), kind=kOutput, calls=%fused_computation.10 | convolution fusion | flops 201621504 | bytes 13303872 | tf_op jit(solution)/shard_map/dot_general | solution.py:117
  46.5 18.7 %all-gather.3.cloned.1.call-done = bf16[3,2048,256]{1,2,0:T(8,128)(2,1)} async-done(((bf16[3,128,256]{1,2,0:T(8,128)(2,1)}), bf16[3,2048,256]{1,2,0:T(8,128)(2,1)}) %all-gather.3.cloned.1.call-update) | async-done | bytes 3145744 | tf_op jit(solution)/shard_map/all_gather | solution.py:118
  65.3 16.1 %bitcast_convert_fusion = (bf16[3,3072,256]{1,2,0:T(8,128)(2,1)S(1)}, f32[3,256,3072]{2,1,0:T(8,128)}) fusion(bf16[3,2048,256]{1,2,0:T(8,128)(2,1)} %all-gather.3.cloned.1.call-done, bf16[3072,2048]{1,0:T(8,128)(2,1)} %param.11), kind=kOutput, calls=%fused_computation.3 | convolution fusion | flops 9666035712 | bytes 29884416 | tf_op jit(solution)/shard_map/td,rdk->rtk/dot_general | solution.py:119
  81.4 3.7 %fusion.22 = f32[3,256,256]{2,1,0:T(8,128)S(1)} fusion(bf16[3,3072,256]{1,2,0:T(8,128)(2,1)S(1)} %get-tuple-element.63, bf16[3,3072,256]{2,1,0:T(8,128)(2,1)} %param.12), kind=kOutput, calls=%fused_computation.36 | convolution fusion | flops 1207959552 | bytes 10223616 | tf_op jit(solution)/shard_map/rtk,rtw->rkw/dot_general | solution.py:124
  85.1 6.4 %fusion.5 = f32[3,256,256]{2,1,0:T(8,128)S(1)} fusion(f32[3,256,256]{2,1,0:T(8,128)S(1)} %fusion.22, bf16[3,3072,256]{2,1,0:T(8,128)(2,1)} %param.12, f32[3,256,3072]{2,1,0:T(8,128)} %get-tuple-element.64, bf16[3,3072,256]{1,2,0:T(8,128)(2,1)S(1)} %get-tuple-element.63), kind=kOutput, calls=%fused_computation.6 | convolution fusion | flops 1215234048 | bytes 20447232 | tf_op jit(solution)/shard_map/rtk,rtw->rkw/dot_general | solution.py:125
  91.5 0.0 copy-start.3
  91.5 0.4 copy.55
  91.9 0.1 pad_maximum_fusion
  92.0 19.2 %all_to_all.30 = f32[16,1,14336]{2,1,0:T(1,128)S(1)} all-to-all(f32[16,1,14336]{2,1,0:T(1,128)S(1)} %bitcast.40), channel_id=1, replica_groups=mesh['fs'=16,'tp'=8] {'fs'}, dimensions={0} | all-to-all | bytes 1835008 | tf_op jit(solution)/shard_map/all_to_all | solution.py:67
  111.2 0.6 reduce_sum.37
  111.8 1.4 broadcast_in_dim.24
  113.2 3.8 %all-to-all-start.2 = ((f32[16,1,14336]{2,1,0:T(1,128)}), f32[16,1,14336]{2,1,0:T(1,128)S(1)}, u32[]{:S(2)}, u32[]{:S(2)}) async-start(f32[16,1,14336]{2,1,0:T(1,128)} %broadcast_in_dim.24), calls=%async_computation.2 | async-start | bytes 1835008 | tf_op jit(solution)/shard_map/all_to_all | solution.py:19
  117.0 0.2 all-gather.5.cloned.1.call-start
  117.2 0.0 copy-done.3
  117.2 0.9 copy.48
  118.1 12.4 %all-to-all-done.2 = f32[16,1,14336]{2,1,0:T(1,128)S(1)} async-done(((f32[16,1,14336]{2,1,0:T(1,128)}), f32[16,1,14336]{2,1,0:T(1,128)S(1)}, u32[]{:S(2)}, u32[]{:S(2)}) %all-to-all-start.2) | async-done | bytes 917536 | tf_op jit(solution)/shard_map/all_to_all | solution.py:19
  130.5 0.1 slice.72
  130.6 0.2 reshape.69
  130.8 2.3 %multiply_reduce_fusion = (f32[]{:T(128)}, f32[3,256,256]{2,1,0:T(8,128)S(1)}, f32[3,256,256]{2,1,0:T(8,128)S(1)}) fusion(f32[3,256,256]{2,1,0:T(8,128)S(1)} %reshape.69, f32[3,256,256]{2,1,0:T(8,128)} %param.18, f32[3,256,256]{2,1,0:T(8,128)} %param.17), kind=kLoop, calls=%fused_computation.13 | loop fusion | flops 1966079 | bytes 3932164 | tf_op jit(solution)/shard_map/reduce_sum | solution.py:132
  133.1 0.7 broadcast_in_dim.25
  133.8 9.4 %all_to_all.31 = f32[8,1,1]{2,1,0:T(1,128)S(1)} all-to-all(f32[8,1,1]{2,1,0:T(1,128)S(1)} %broadcast_in_dim.25), channel_id=1, replica_groups=mesh['fs'=16,'tp'=8] {'tp'}, dimensions={0} | all-to-all | bytes 64 | tf_op jit(solution)/shard_map/all_to_all | solution.py:19
  143.2 0.6 reduce_sum.39
  144.5 2.7 %fusion.20 = (bf16[3,128,256]{1,2,0:T(8,128)(2,1)}, f32[3,128,256]{1,2,0:T(8,128)S(1)}, f32[3,128,256]{1,2,0:T(8,128)}) fusion(f32[3,128,256]{1,2,0:T(8,128)} %copy.48, bf16[3,128,256]{2,1,0:T(8,128)(2,1)S(1)} %copy-done.2, f32[3,256,256]{2,1,0:T(8,128)S(1)} %get-tuple-element.62, f32[3,256,256]{2,1,0:T(8,128)S(1)} %get-tuple-element.61, f32[]{:T(128)S(6)} %rsqrt.5), kind=kOutput, calls=%fused_computation.35 | convolution fusion | flops 302579712 | bytes 3145732 | tf_op jit(solution)/shard_map/rdk,rkw->rdw/dot_general | solution.py:135
  147.1 0.0 all-gather.5.cloned.1.call-update
  147.2 2.2 %reduce.3 = f32[16,14336]{1,0:T(8,128)S(1)} reduce(f32[16,1,14336]{2,1,0:T(1,128)S(1)} %all-to-all-done.2, f32[]{:T(128)} %constant.8), dimensions={1}, to_apply=%all_to_all.24.reduce_sub_computation | reduce | bytes 1835012 | tf_op jit(solution)/shard_map/all_to_all | solution.py:19
  149.4 0.1 slice.68
  149.5 1.7 fusion.18
  151.2 1.9 copy.49
  153.1 0.9 copy.50
  154.1 40.8 %all-gather.5.cloned.1.call-done = bf16[3,2048,256]{1,2,0:T(8,128)(2,1)} async-done(((bf16[3,128,256]{1,2,0:T(8,128)(2,1)}), bf16[3,2048,256]{1,2,0:T(8,128)(2,1)}) %all-gather.5.cloned.1.call-update) | async-done | bytes 3145744 | tf_op jit(solution)/shard_map/all_gather | solution.py:140
  194.9 4.6 %copy.51 = bf16[3,2048,256]{2,1,0:T(8,128)(2,1)} copy(bf16[3,2048,256]{1,2,0:T(8,128)(2,1)} %all-gather.5.cloned.1.call-done) | data formatting | bytes 6291456
  (26 shorter events, 0.3 us)
Async XLA Ops:
  7.2 58.1 %all-gather.3.cloned.1.call-start = ((), (), s32[]{:S(2)}) async-start(), calls=%async_computation.4 | async-start | bytes 3342336 | tf_op jit(solution)/shard_map/all_gather | solution.py:118
  10.7 28.9 %all-to-all-start = ((f32[16,1,16]{2,1,0:T(1,128)}), f32[16,1,16]{2,1,0:T(1,128)S(1)}, u32[]{:S(2)}, u32[]{:S(2)}) async-start(f32[16,1,16]{2,1,0:T(1,128)} %broadcast_in_dim.22), calls=%async_computation | async-start | bytes 16384 | tf_op jit(solution)/shard_map/all_to_all | solution.py:19
  19.4 20.4 %collective-permute-start = (f32[16,1]{1,0:T(8,128)S(1)}, f32[16,1]{1,0:T(8,128)S(1)}, u32[]{:S(2)}, u32[]{:S(2)}) collective-permute-start(f32[16,1]{1,0:T(8,128)S(1)} %slice.65), channel_id=1, source_target_pairs={{0,8},{8,16},{16,24},{24,32},{32,40},{40,48},{48,56},{56,64},{64,7... | collective-permute-start | bytes 200 | tf_op jit(solution)/shard_map/ppermute | solution.py:14
  91.5 25.7 %copy-start.3 = (f32[3,128,256]{2,1,0:T(8,128)S(1)}, f32[3,128,256]{2,1,0:T(8,128)}, u32[]{:S(2)}) copy-start(f32[3,128,256]{2,1,0:T(8,128)} %param.15) | copy-start | bytes 1179652
  113.2 31.3 %copy-start.2 = (bf16[3,128,256]{2,1,0:T(8,128)(2,1)S(1)}, bf16[3,128,256]{2,1,0:T(8,128)(2,1)}, u32[]{:S(2)}) copy-start(bf16[3,128,256]{2,1,0:T(8,128)(2,1)} %param.16) | copy-start | bytes 589828
  113.2 17.3 %all-to-all-start.2 = ((f32[16,1,14336]{2,1,0:T(1,128)}), f32[16,1,14336]{2,1,0:T(1,128)S(1)}, u32[]{:S(2)}, u32[]{:S(2)}) async-start(f32[16,1,14336]{2,1,0:T(1,128)} %broadcast_in_dim.24), calls=%async_computation.2 | async-start | bytes 1835008 | tf_op jit(solution)/shard_map/all_to_all | solution.py:19
  117.0 77.9 %all-gather.5.cloned.1.call-start = ((), (), s32[]{:S(2)}) async-start(), calls=%async_computation.5 | async-start | bytes 3342336 | tf_op jit(solution)/shard_map/all_gather | solution.py:140
  133.1 14.1 %copy-start.1 = (f32[3,256,256]{2,1,0:T(8,128)}, f32[3,256,256]{2,1,0:T(8,128)S(1)}, u32[]{:S(2)}) copy-start(f32[3,256,256]{2,1,0:T(8,128)S(1)} %get-tuple-element.62) | copy-start | bytes 2359300
  133.1 21.0 %copy-start = (f32[3,256,256]{2,1,0:T(8,128)}, f32[3,256,256]{2,1,0:T(8,128)S(1)}, u32[]{:S(2)}) copy-start(f32[3,256,256]{2,1,0:T(8,128)S(1)} %get-tuple-element.61) | copy-start | bytes 2359300
  133.1 16.5 %copy-start.4 = (f32[16,2048]{1,0:T(8,128)S(1)}, f32[16,2048]{1,0:T(8,128)}, u32[]{:S(2)}) copy-start(f32[16,2048]{1,0:T(8,128)} %param.19) | copy-start | bytes 393220
  133.1 16.5 %copy-start.5 = (f32[16,2048]{1,0:T(8,128)S(1)}, f32[16,2048]{1,0:T(8,128)}, u32[]{:S(2)}) copy-start(f32[16,2048]{1,0:T(8,128)} %param.20) | copy-start | bytes 393220
Sparse Core Ops, SparseCore 0:
  10.7 54.5 all-gather.2
  147.3 47.5 all-gather.4
where the time goes:
time: 208 us; the launch traced here: 206 us
  waiting for transfers between devices  72 us (35%)
  matrix products  35.5 us (17%)
  blocking collectives  28.6 us (14%)
  local copies, waits for them, and re-layouts  26.1 us (13%)
  starting transfers between devices  15.8 us (8%)
  between operations  14.9 us (7%)
  other arithmetic  13.5 us (6%)
    all_gather x1, waiting for transfers between devices, local(): lax.all_gather(proj_new.astype(jnp.bfloat16), 'fs', axis=1, tiled=True)  40.8 us
    all_to_all x1, blocking collectives, summed_on_arrival(): lax.all_to_all(parts, axis, split_axis=0, concat_axis=0, tiled=True)  19.2 us
    all_gather x1, waiting for transfers between devices, local(): all_factors = lax.all_gather(factors, 'fs', axis=1, tiled=True)  18.7 us
    dot_general x1, matrix products, local(): jnp.einsum('td,rdk->rtk', saved_input, all_factors, preferred_element_typ...  16.1 us
    all_to_all x2, waiting for transfers between devices, from_everyone(): return lax.all_to_all(copies, axis, split_axis=0, concat_axis=0, tiled=True)  12.4 us
    all_to_all x2, starting transfers between devices, from_everyone(): return lax.all_to_all(copies, axis, split_axis=0, concat_axis=0, tiled=True)  11.8 us
    unnamed x21, local copies, waits for them, and re-layouts  10.7 us
    all_to_all x1, blocking collectives, from_everyone(): return lax.all_to_all(copies, axis, split_axis=0, concat_axis=0, tiled=True)  9.37 us
  transfers between devices with their start and end apart: 5, of which 3 were waited for; matrix products, arithmetic and copies ran while one was open for 16% of the time, Pallas kernels for 0%

commit v1 on v0

v1 whole, which is shorter than its diff:
```python
import functools

import jax
import jax.numpy as jnp
from jax import lax
from jax.experimental import pallas as pl
from jax.experimental.pallas import tpu as pltpu
from jax.sharding import Mesh
from jax.sharding import PartitionSpec as P

BETA_ONE = 0.8
BETA_TWO = 0.9
LEARN = 0.001
FS = ("z", "x")
TP = ("y", "c")


def from_everyone(x, axis):
    copies = jnp.broadcast_to(x, (lax.axis_size(axis), *x.shape))
    return lax.all_to_all(copies, axis, split_axis=0, concat_axis=0, tiled=True)


def gate_kernel(me_ref, log_ref, cot_ref, ends_ref, out_ref):
    me = me_ref[0]
    heads, length = log_ref.shape
    ends = ends_ref[...]
    source = lax.broadcasted_iota(jnp.int32, ends.shape, 0)
    after = jnp.sum(jnp.where(source > me, ends, 0.0), axis=0, keepdims=True)
    before = jnp.sum(jnp.where(source == me - 1, ends, 0.0), axis=0, keepdims=True)
    lane = lax.broadcasted_iota(jnp.int32, (heads, ends.shape[1]), 1)
    row = lax.broadcasted_iota(jnp.int32, (heads, ends.shape[1]), 0)
    carried = jnp.sum(jnp.where(lane == row, after, 0.0), axis=1, keepdims=True)
    edge = jnp.sum(jnp.where(lane == row + heads, before, 0.0), axis=1, keepdims=True)
    place = lax.broadcasted_iota(jnp.int32, (heads, length), 1)
    total = cot_ref[...]
    step = 1
    while step < length:
        total = total + jnp.where(place < length - step, pltpu.roll(total, length - step, 1), 0.0)
        step *= 2
    log = log_ref[...]
    previous = jnp.where(place == 0, edge, pltpu.roll(log, 1, 1))
    delta = log - previous
    closed = -jnp.tanh(0.5 * delta) * (jnp.exp(delta) + 1.0)
    out_ref[...] = ((total + carried) * closed).astype(out_ref.dtype)


def gate_cotangent(log_cache, cache_cot, ends, me):
    heads, length = log_cache.shape
    vmem = pl.BlockSpec(memory_space=pltpu.VMEM)
    return pl.pallas_call(
        gate_kernel,
        out_shape=jax.ShapeDtypeStruct((heads, length), jnp.bfloat16),
        in_specs=[pl.BlockSpec(memory_space=pltpu.SMEM), vmem, vmem, vmem],
        out_specs=vmem,
        cost_estimate=pl.CostEstimate(
            flops=40 * heads * length, bytes_accessed=10 * heads * length, transcendentals=0
        ),
        name="gate_cotangent",
    )(me.reshape(1).astype(jnp.int32), log_cache, cache_cot, ends)


def local(
    saved_input,
    proj_cot,
    log_cache,
    cache_cot,
    proj_master,
    factors,
    first_moment,
    second_moment,
    gate_master,
    gate_first,
    gate_second,
):
    roles, rows, rank = factors.shape
    heads = log_cache.shape[0]
    width = proj_cot.shape[2]
    peers = lax.axis_size(FS)
    me = lax.axis_index(FS)
    core = lax.axis_index("c")
    cores = lax.axis_size("c")
    half = rank // cores

    ends = jnp.concatenate([jnp.sum(cache_cot, axis=1), log_cache[:, -1]])
    ends = from_everyone(ends.reshape(1, 1, -1), FS).reshape(peers, -1)
    ends = jnp.pad(ends, ((0, 0), (0, 128 - ends.shape[1])))
    own_factors = lax.dynamic_slice_in_dim(factors, core * half, half, axis=2)
    near = from_everyone(own_factors, FS)
    far = lax.ppermute(near, "c", [(0, 1), (1, 0)])

    grad = jnp.einsum("td,rtw->rdw", saved_input, proj_cot, preferred_element_type=jnp.float32)
    upper = lax.optimization_barrier(grad.astype(jnp.bfloat16))
    lower = (grad - upper.astype(jnp.float32)).astype(jnp.bfloat16)

    gate_cot = gate_cotangent(log_cache, cache_cot, ends, me)
    gate_part = jnp.dot(gate_cot, saved_input, preferred_element_type=jnp.float32)

    def projected(pieces):
        pieces = jnp.moveaxis(pieces, 0, 1).reshape(roles, peers * rows, half)
        return sum(
            jnp.einsum("rdk,rdw->rkw", pieces, side, preferred_element_type=jnp.float32)
            for side in (upper, lower)
        )

    parts = jnp.concatenate(
        [
            projected(near).reshape(-1, width),
            projected(far).reshape(-1, width),
            gate_part.reshape(-1, width),
        ]
    )
    lines = parts.shape[0]
    arrived = lax.all_to_all(
        parts.reshape(peers, lines // peers, width), FS, split_axis=0, concat_axis=0, tiled=True
    )
    sums = from_everyone(jnp.sum(arrived, axis=0)[None], FS).reshape(lines, width)
    pair = sums[: roles * rank].reshape(cores, roles, half, width)
    low = jnp.where(core == 0, pair, pair[::-1])
    low = jnp.moveaxis(low, 0, 1).reshape(roles, rank, width)
    gate_grad = sums[roles * rank :].reshape(heads, -1)

    first_new = BETA_ONE * first_moment + (1.0 - BETA_ONE) * low
    second_new = BETA_TWO * second_moment + (1.0 - BETA_TWO) * low * low
    direction = first_new / jnp.sqrt(second_new)
    squares = jnp.sum(from_everyone(jnp.sum(direction * direction).reshape(1, 1), TP))
    entries = direction.size * lax.axis_size(TP)
    scale = lax.rsqrt(squares / entries + 1e-06)
    product = jnp.einsum(
        "rdk,rkw->rdw", factors.astype(jnp.float32), direction, precision=lax.Precision.HIGHEST
    )
    proj_step = scale * product
    proj_new = proj_master - LEARN * proj_step
    proj_copy = from_everyone(proj_new.astype(jnp.bfloat16)[None], FS)
    proj_copy = proj_copy.reshape(peers, roles, rows, width)
    proj_copy = jnp.moveaxis(proj_copy, 0, 1).reshape(roles, peers * rows, width)
    gate_first_new = BETA_ONE * gate_first + (1.0 - BETA_ONE) * gate_grad
    gate_second_new = BETA_TWO * gate_second + (1.0 - BETA_TWO) * gate_grad * gate_grad
    gate_new = gate_master - LEARN * gate_first_new / jnp.sqrt(gate_second_new)
    return (
        proj_step,
        proj_new,
        proj_copy,
        first_new,
        second_new,
        gate_new,
        gate_new.astype(jnp.bfloat16),
        gate_first_new,
        gate_second_new,
    )


def solution(mesh):
    fine = Mesh(mesh.devices.reshape(4, 4, 4, 2), (*FS, *TP))
    placed = (
        P(FS, None),
        P(None, FS, TP),
        P(None, FS),
        P(None, FS),
        P(None, FS, TP),
        P(None, FS, None),
        P(None, None, TP),
        P(None, None, TP),
        P(),
        P(),
        P(),
    )
    return jax.shard_map(
        local,
        mesh=fine,
        in_specs=placed,
        out_specs=(
            P(None, FS, TP),
            P(None, FS, TP),
            P(None, None, TP),
            P(None, None, TP),
            P(None, None, TP),
            P(),
            P(),
            P(),
            P(),
        ),
        check_vma=False,
    )
```

time: 208 us -> 180 us (0.87)
  between operations: 14.9 us -> 1.57 us
  local copies, waits for them, and re-layouts: 26.1 us -> 16.8 us
  other arithmetic: 13.5 us -> 6.14 us
  waiting for transfers between devices: 72 us -> 65.9 us
  starting transfers between devices: 15.8 us -> 20 us
  Pallas kernels: 0 us -> 2.28 us
    all_gather x2 -> x0, waiting for transfers between devices: 59.6 us -> none  [the longest x1 40.8 us: local(): lax.all_gather(proj_new.astype(jnp.bfloat16), 'fs', axis=1, tiled=True)]
    all_to_all x2 -> x4, waiting for transfers between devices: 12.4 us -> 65.9 us  [from_everyone(): return lax.all_to_all(copies, axis, split_axis=0, concat_axis=0, tiled=True)]
    rev x2 -> x0, local copies, waits for them, and re-layouts: 11.1 us -> none  [the longest x1 9.34 us: local(): jnp.flip(cache_cot, 1)]
    all_to_all x2 -> x4, starting transfers between devices: 11.8 us -> 20 us  [from_everyone(): return lax.all_to_all(copies, axis, split_axis=0, concat_axis=0, tiled=True)]
    unnamed x21 -> x19, local copies, waits for them, and re-layouts: 10.7 us -> 4.01 us
    another operation x3 -> x0, other arithmetic: 4.9 us -> none
    ppermute x1, starting transfers between devices: 3.82 us -> 0.01 us  [local(): far = lax.ppermute(near, 'c', [(0, 1), (1, 0)])]
    broadcast_in_dim x3 -> x5, local copies, waits for them, and re-layouts: 2.74 us -> 5.79 us  [from_everyone(): copies = jnp.broadcast_to(x, (lax.axis_size(axis), *x.shape))]
  transfers between devices with their start and end apart: 5 -> 5, of which waited for: 3 -> 4; matrix products, arithmetic and copies ran while one was open for 16% -> 22% of each run, Pallas kernels for 0% -> 1%
where the time goes in v1:
time: 180 us; the launch traced here: 179 us
  waiting for transfers between devices  65.9 us (37%)
  matrix products  36.7 us (20%)
  blocking collectives  29.7 us (16%)
  starting transfers between devices  20 us (11%)
  local copies, waits for them, and re-layouts  16.8 us (9%)
  other arithmetic  6.14 us (3%)
  Pallas kernels  2.28 us (1%)
    all_to_all x4, waiting for transfers between devices, from_everyone(): return lax.all_to_all(copies, axis, split_axis=0, concat_axis=0, tiled=True)  65.9 us
    all_to_all x1, blocking collectives, local(): lax.all_to_all(parts.reshape(peers, lines // peers, width), FS, split_axi...  20.1 us
    all_to_all x4, starting transfers between devices, from_everyone(): return lax.all_to_all(copies, axis, split_axis=0, concat_axis=0, tiled=True)  20 us
    dot_general x1, matrix products, local(): jnp.einsum('td,rtw->rdw', saved_input, proj_cot, preferred_element_type=j...  16.2 us
    dot_general x4, matrix products, projected(): jnp.einsum('rdk,rdw->rkw', pieces, side, preferred_element_type=jnp.float32)  12.5 us
    all_to_all x1, blocking collectives, from_everyone(): return lax.all_to_all(copies, axis, split_axis=0, concat_axis=0, tiled=True)  9.56 us
    dot_general x1, matrix products, local(): jnp.dot(gate_cot, saved_input, preferred_element_type=jnp.float32)  6.37 us
    broadcast_in_dim x5, local copies, waits for them, and re-layouts, from_everyone(): copies = jnp.broadcast_to(x, (lax.axis_size(axis), *x.shape))  5.79 us
  transfers between devices with their start and end apart: 5, of which 4 were waited for; matrix products, arithmetic and copies ran while one was open for 22% of the time, Pallas kernels for 1%

profile of v1, /device:TPU:0, one launch (start us, length us, event | category | flops | bytes accessed | tf_op | source)
XLA Modules:
  0.0 179.0 jit_solution(17551765824104717049)
XLA Ops:
  0.6 0.0 copy-start
  0.7 0.9 slice_reduce_fusion
  1.6 1.1 reduce_sum.36
  2.6 0.1 pad_maximum_fusion.1
  2.7 0.6 broadcast_in_dim.18
  3.3 8.0 %all-to-all-start.1 = ((f32[16,1,1,32]{3,2,1,0:T(1,128)}), f32[16,1,1,32]{3,2,1,0:T(1,128)S(1)}, u32[]{:S(2)}, u32[]{:S(2)}) async-start(f32[16,1,1,32]{3,2,1,0:T(1,128)} %broadcast_in_dim.18), calls=%async_computation.1 | async-start | bytes 16384 | tf_op jit(solution)/shard_map/all_to_all | solution.py:20
  11.4 0.1 copy.93
  11.5 7.3 %all-to-all-done.1 = f32[16,1,1,32]{3,2,1,0:T(1,128)S(1)} async-done(((f32[16,1,1,32]{3,2,1,0:T(1,128)}), f32[16,1,1,32]{3,2,1,0:T(1,128)S(1)}, u32[]{:S(2)}, u32[]{:S(2)}) %all-to-all-start.1) | async-done | bytes 2080 | tf_op jit(solution)/shard_map/all_to_all | solution.py:20
  18.8 1.5 broadcast_in_dim.17
  20.4 4.4 %all-to-all-start = ((bf16[16,3,128,128]{2,3,1,0:T(8,128)(2,1)}), bf16[16,3,128,128]{2,3,1,0:T(8,128)(2,1)}, u32[]{:S(2)}, u32[]{:S(2)}) async-start(bf16[16,3,128,128]{2,3,1,0:T(8,128)(2,1)} %broadcast_in_dim.17), calls=%async_computation | async-start | bytes 3145728 | tf_op jit(solution)/shard_map/all_to_all | solution.py:20
  24.8 16.2 %bitcast_convert_fusion = (bf16[3,2048,256]{1,2,0:T(8,128)(2,1)S(1)}, f32[3,256,2048]{2,1,0:T(8,128)}) fusion(bf16[3,3072,256]{2,1,0:T(8,128)(2,1)} %param.12, bf16[3072,2048]{1,0:T(8,128)(2,1)} %param.11), kind=kOutput, calls=%fused_computation.3 | convolution fusion | flops 9665249280 | bytes 26738688 | tf_op jit(solution)/shard_map/td,rtw->rdw/dot_general | solution.py:91
  40.9 0.6 pad.4.ends_ref
  41.5 2.3 %gate_cotangent.1 = bf16[16,3072]{1,0:T(8,128)(2,1)} custom-call(s32[1]{0:T(128)} %bitcast.6.me_ref, f32[16,3072]{1,0:T(8,128)} %log_ref.1, f32[16,3072]{1,0:T(8,128)} %cot_ref.1, f32[16,128]{1,0:T(8,128)} %pad.4.ends_ref), custom_call_target="tpu_custom_call" | custom-call | flops 1966080 | bytes 491520 | tf_op jit(solution)/shard_map/gate_cotangent/pallas_call | solution.py:50
  43.8 3.4 %all-to-all-done = bf16[16,3,128,128]{2,3,1,0:T(8,128)(2,1)} async-done(((bf16[16,3,128,128]{2,3,1,0:T(8,128)(2,1)}), bf16[16,3,128,128]{2,3,1,0:T(8,128)(2,1)}, u32[]{:S(2)}, u32[]{:S(2)}) %all-to-all-start) | async-done | bytes 1572896 | tf_op jit(solution)/shard_map/all_to_all | solution.py:20
  47.2 0.0 collective-permute-start
  47.2 6.4 %fusion.32 = f32[16,2048]{1,0:T(8,128)S(1)} fusion(bf16[16,3072]{1,0:T(8,128)(2,1)} %gate_cotangent.1, bf16[3072,2048]{1,0:T(8,128)(2,1)} %param.11), kind=kOutput, calls=%fused_computation.39 | convolution fusion | flops 201326592 | bytes 12812288 | tf_op jit(solution)/shard_map/dot_general | solution.py:96
  53.5 0.7 reshape.68
  54.2 4.6 %fusion.7 = f32[3,128,256]{2,1,0:T(8,128)S(1)} fusion(f32[3,256,2048]{2,1,0:T(8,128)} %get-tuple-element.73, bf16[3,2048,256]{1,2,0:T(8,128)(2,1)S(1)} %get-tuple-element.72, bf16[16,3,128,128]{2,3,1,0:T(8,128)(2,1)} %all-to-all-done), kind=kOutput, calls=%fused_computation.9 | convolution fusion | flops 407371776 | bytes 11403264 | tf_op jit(solution)/shard_map/rdk,rdw->rkw/dot_general | solution.py:101
  58.8 2.6 %fusion.15 = f32[3,128,256]{2,1,0:T(8,128)S(1)} fusion(f32[3,128,256]{2,1,0:T(8,128)S(1)} %fusion.7, bf16[3,2048,256]{1,2,0:T(8,128)(2,1)S(1)} %get-tuple-element.72, bf16[16,3,128,128]{2,3,1,0:T(8,128)(2,1)} %all-to-all-done), kind=kOutput, calls=%fused_computation.17 | convolution fusion | flops 402751488 | bytes 5505024 | tf_op jit(solution)/shard_map/rdk,rdw->rkw/dot_general | solution.py:101
  61.5 2.7 %fusion.3 = f32[3,128,256]{2,1,0:T(8,128)S(1)} fusion(f32[3,256,2048]{2,1,0:T(8,128)S(1)} %bitcast.72, bf16[3,2048,256]{1,2,0:T(8,128)(2,1)S(1)} %get-tuple-element.72, bf16[16,3,128,128]{2,3,1,0:T(8,128)(2,1)} %collective-permute-done), kind=kOutput, calls=%fused_computation.5 | convolution fusion | flops 407371776 | bytes 11403264 | tf_op jit(solution)/shard_map/rdk,rdw->rkw/dot_general | solution.py:101
  64.2 0.0 copy-start.4
  64.2 2.6 %fusion.18 = f32[3,128,256]{2,1,0:T(8,128)S(1)} fusion(f32[3,128,256]{2,1,0:T(8,128)S(1)} %fusion.3, bf16[3,2048,256]{1,2,0:T(8,128)(2,1)S(1)} %get-tuple-element.72, bf16[16,3,128,128]{2,3,1,0:T(8,128)(2,1)} %collective-permute-done), kind=kOutput, calls=%fused_computation.18 | convolution fusion | flops 402751488 | bytes 5505024 | tf_op jit(solution)/shard_map/rdk,rdw->rkw/dot_general | solution.py:101
  66.8 0.1 pad_maximum_fusion
  66.9 0.0 copy-start.5
  66.9 20.1 %all_to_all.30 = f32[16,56,256]{2,1,0:T(8,128)S(1)} all-to-all(f32[16,56,256]{2,1,0:T(8,128)S(1)} %bitcast.75), channel_id=1, replica_groups=mesh['z'=4,'x'=4,'y'=4,'c'=2] {'z','x'}, dimensions={0} | all-to-all | bytes 1835008 | tf_op jit(solution)/shard_map/all_to_all | solution.py:113
  87.0 0.1 reduce_sum.37
  87.0 1.0 broadcast_in_dim.19
  88.0 3.8 %all-to-all-start.3 = ((f32[16,1,56,256]{3,2,1,0:T(8,128)}), f32[16,1,56,256]{3,2,1,0:T(8,128)S(1)}, u32[]{:S(2)}, u32[]{:S(2)}) async-start(f32[16,1,56,256]{3,2,1,0:T(8,128)} %broadcast_in_dim.19), calls=%async_computation.3 | async-start | bytes 1835008 | tf_op jit(solution)/shard_map/all_to_all | solution.py:20
  91.9 0.2 copy.105
  92.0 15.1 %all-to-all-done.3 = f32[16,1,56,256]{3,2,1,0:T(8,128)S(1)} async-done(((f32[16,1,56,256]{3,2,1,0:T(8,128)}), f32[16,1,56,256]{3,2,1,0:T(8,128)S(1)}, u32[]{:S(2)}, u32[]{:S(2)}) %all-to-all-start.3) | async-done | bytes 917536 | tf_op jit(solution)/shard_map/all_to_all | solution.py:20
  107.1 0.1 slice.12
  107.1 0.1 copy.102
  107.2 0.1 reverse_select_fusion
  107.3 2.4 %multiply_reduce_fusion = (f32[]{:T(128)}, f32[3,256,256]{2,1,0:T(8,128)S(1)}, f32[3,256,256]{2,1,0:T(8,128)S(1)}) fusion(f32[2,3,128,256]{3,2,0,1:T(8,128)S(1)} %reverse_select_fusion, f32[3,256,256]{2,1,0:T(8,128)} %param.18, f32[3,256,256]{2,1,0:T(8,128)} %param.17), kind=kLoop, calls=%fused_computation.27 | loop fusion | flops 1966079 | bytes 3932164 | tf_op jit(solution)/shard_map/reduce_sum | solution.py:125
  109.7 0.6 broadcast_in_dim.20
  110.3 9.6 %all_to_all.31 = f32[8,1,1]{2,1,0:T(1,128)S(1)} all-to-all(f32[8,1,1]{2,1,0:T(1,128)S(1)} %broadcast_in_dim.20), channel_id=1, replica_groups=mesh['z'=4,'x'=4,'y'=4,'c'=2] {'y','c'}, dimensions={0} | all-to-all | bytes 64 | tf_op jit(solution)/shard_map/all_to_all | solution.py:20
  119.9 0.6 reduce_sum.39
  121.2 1.7 fusion.29
  123.0 0.1 copy.106
  123.1 2.0 %broadcast_in_dim.21 = bf16[16,1,3,128,256]{4,3,2,1,0:T(8,128)(2,1)} broadcast(bf16[3,128,256]{2,1,0:T(8,128)(2,1)S(1)} %copy.106), dimensions={2,3,4} | broadcast | bytes 3342336 | tf_op jit(solution)/shard_map/broadcast_in_dim | solution.py:19
  125.1 3.7 %all-to-all-start.5 = ((bf16[16,1,3,128,256]{4,3,2,1,0:T(8,128)(2,1)}), bf16[16,1,3,128,256]{4,3,2,1,0:T(8,128)(2,1)S(1)}, u32[]{:S(2)}, u32[]{:S(2)}) async-start(bf16[16,1,3,128,256]{4,3,2,1,0:T(8,128)(2,1)} %broadcast_in_dim.21), calls=%async_computation.5 | async-start | bytes 6291456 | tf_op jit(solution)/shard_map/all_to_all | solution.py:20
  128.9 1.6 slice.13
  130.5 0.9 reshape.75
  131.4 1.8 %fusion.27 = (bf16[16,2048]{1,0:T(8,128)(2,1)}, f32[16,2048]{1,0:T(8,128)}, f32[16,2048]{1,0:T(8,128)}, f32[16,2048]{1,0:T(8,128)}) fusion(f32[16,2048]{1,0:T(8,128)} %param.19, f32[16,2048]{1,0:T(8,128)S(1)} %reshape.75, f32[16,2048]{1,0:T(8,128)} %param.20, f32[16,2048]{1,0:T(8,128)} %param.21), kind=kLoop, calls=%fused_computation.37 | loop fusion | flops 360448 | bytes 983040 | tf_op jit(solution)/shard_map/convert_element_type | solution.py:146
  133.2 1.9 %copy.108 = f32[3,128,256]{2,1,0:T(8,128)} copy(f32[3,128,256]{1,2,0:T(8,128)} %get-tuple-element.74) | data formatting | bytes 786432
  135.1 1.9 %copy.109 = f32[3,128,256]{2,1,0:T(8,128)} copy(f32[3,128,256]{1,2,0:T(8,128)} %get-tuple-element.68) | data formatting | bytes 786432
  137.0 40.1 %all-to-all-done.5 = bf16[16,1,3,128,256]{4,3,2,1,0:T(8,128)(2,1)S(1)} async-done(((bf16[16,1,3,128,256]{4,3,2,1,0:T(8,128)(2,1)}), bf16[16,1,3,128,256]{4,3,2,1,0:T(8,128)(2,1)S(1)}, u32[]{:S(2)}, u32[]{:S(2)}) %all-to-all-start.5) | async-done | bytes 3145760 | tf_op jit(solution)/shard_map/all_to_all | solution.py:20
  177.2 1.9 %copy.107 = bf16[16,1,3,128,256]{4,3,0,2,1:T(8,128)(2,1)} copy(bf16[16,1,3,128,256]{4,3,2,1,0:T(8,128)(2,1)S(1)} %all-to-all-done.5) | data formatting | bytes 6291456 | tf_op jit(solution)/shard_map/all_to_all | solution.py:20
  (16 shorter events, 0.1 us)
Async XLA Ops:
  0.6 10.7 %copy-start = (bf16[3,128,256]{2,1,0:T(8,128)(2,1)S(1)}, bf16[3,128,256]{2,1,0:T(8,128)(2,1)}, u32[]{:S(2)}) copy-start(bf16[3,128,256]{2,1,0:T(8,128)(2,1)} %param.16) | copy-start | bytes 589828
  3.3 15.5 %all-to-all-start.1 = ((f32[16,1,1,32]{3,2,1,0:T(1,128)}), f32[16,1,1,32]{3,2,1,0:T(1,128)S(1)}, u32[]{:S(2)}, u32[]{:S(2)}) async-start(f32[16,1,1,32]{3,2,1,0:T(1,128)} %broadcast_in_dim.18), calls=%async_computation.1 | async-start | bytes 16384 | tf_op jit(solution)/shard_map/all_to_all | solution.py:20
  20.4 26.8 %all-to-all-start = ((bf16[16,3,128,128]{2,3,1,0:T(8,128)(2,1)}), bf16[16,3,128,128]{2,3,1,0:T(8,128)(2,1)}, u32[]{:S(2)}, u32[]{:S(2)}) async-start(bf16[16,3,128,128]{2,3,1,0:T(8,128)(2,1)} %broadcast_in_dim.17), calls=%async_computation | async-start | bytes 3145728 | tf_op jit(solution)/shard_map/all_to_all | solution.py:20
  47.2 14.2 %collective-permute-start = (bf16[16,3,128,128]{2,3,1,0:T(8,128)(2,1)}, bf16[16,3,128,128]{2,3,1,0:T(8,128)(2,1)}, u32[]{:S(2)}, u32[]{:S(2)}) collective-permute-start(bf16[16,3,128,128]{2,3,1,0:T(8,128)(2,1)} %all-to-all-done), channel_id=1, source_target_pairs={{0,1},{1,0},{2,3},{3,2},{4,5},{5,4},{6,7},{7,6},{8,9},{9,8},{10,11... | collective-permute-start | bytes 4718600 | tf_op jit(solution)/shard_map/ppermute | solution.py:89
  54.2 7.2 %slice-start = ((s8[6291456]{0:T(1024)(128)(4,1)}), s8[4194304]{0:T(1024)(128)(4,1)S(1)}, s32[]{:S(2)}) async-start(s8[6291456]{0:T(1024)(128)(4,1)} %bitcast.71), calls=%async_computation.6 | async-start | bytes 8388608
  54.2 7.2 %slice-start.1 = ((s8[6291456]{0:T(1024)(128)(4,1)}), s8[2097152]{0:T(1024)(128)(4,1)S(1)}, s32[]{:S(2)}) async-start(s8[6291456]{0:T(1024)(128)(4,1)} %bitcast.71), calls=%async_computation.7 | async-start | bytes 4194304
  64.2 2.6 %copy-start.4 = (f32[128,256]{1,0:T(8,128)S(1)}, f32[128,256]{1,0:T(8,128)}, u32[]{:S(2)}) copy-start(f32[128,256]{1,0:T(8,128)} %reshape.68) | copy-start | bytes 393220
  66.9 25.0 %copy-start.5 = (f32[3,128,256]{2,1,0:T(8,128)S(1)}, f32[3,128,256]{2,1,0:T(8,128)}, u32[]{:S(2)}) copy-start(f32[3,128,256]{2,1,0:T(8,128)} %param.15) | copy-start | bytes 1179652
  88.0 19.1 %all-to-all-start.3 = ((f32[16,1,56,256]{3,2,1,0:T(8,128)}), f32[16,1,56,256]{3,2,1,0:T(8,128)S(1)}, u32[]{:S(2)}, u32[]{:S(2)}) async-start(f32[16,1,56,256]{3,2,1,0:T(8,128)} %broadcast_in_dim.19), calls=%async_computation.3 | async-start | bytes 1835008 | tf_op jit(solution)/shard_map/all_to_all | solution.py:20
  107.1 2.6 %copy-start.1 = (f32[16,1,56,256]{3,2,1,0:T(8,128)}, f32[16,1,56,256]{3,2,1,0:T(8,128)S(1)}, u32[]{:S(2)}) copy-start(f32[16,1,56,256]{3,2,1,0:T(8,128)S(1)} %all-to-all-done.3) | copy-start | bytes 2752516
  109.7 15.5 %copy-start.2 = (f32[3,256,256]{2,1,0:T(8,128)}, f32[3,256,256]{2,1,0:T(8,128)S(1)}, u32[]{:S(2)}) copy-start(f32[3,256,256]{2,1,0:T(8,128)S(1)} %get-tuple-element.70) | copy-start | bytes 2359300
  109.7 15.5 %copy-start.3 = (f32[3,256,256]{2,1,0:T(8,128)}, f32[3,256,256]{2,1,0:T(8,128)S(1)}, u32[]{:S(2)}) copy-start(f32[3,256,256]{2,1,0:T(8,128)S(1)} %get-tuple-element.71) | copy-start | bytes 2359300
  125.1 52.0 %all-to-all-start.5 = ((bf16[16,1,3,128,256]{4,3,2,1,0:T(8,128)(2,1)}), bf16[16,1,3,128,256]{4,3,2,1,0:T(8,128)(2,1)S(1)}, u32[]{:S(2)}, u32[]{:S(2)}) async-start(bf16[16,1,3,128,256]{4,3,2,1,0:T(8,128)(2,1)} %broadcast_in_dim.21), calls=%async_computation.5 | async-start | bytes 6291456 | tf_op jit(solution)/shard_map/all_to_all | solution.py:20

commit v2 on v1

v2 whole, which is shorter than its diff:
```python
import jax
import jax.numpy as jnp
from jax import lax
from jax.experimental import pallas as pl
from jax.experimental.pallas import tpu as pltpu
from jax.sharding import Mesh
from jax.sharding import PartitionSpec as P

BETA_ONE = 0.8
BETA_TWO = 0.9
LEARN = 0.001
FS = ("z", "x")
TP = ("y", "c")


def from_everyone(x, axis):
    copies = jnp.broadcast_to(x, (lax.axis_size(axis), *x.shape))
    return lax.all_to_all(copies, axis, split_axis=0, concat_axis=0, tiled=True)


VMEM = pl.BlockSpec(memory_space=pltpu.VMEM)
SMEM = pl.BlockSpec(memory_space=pltpu.SMEM)
ROOM = pltpu.CompilerParams(vmem_limit_bytes=48 * 2**20)


def cost(flops, moved):
    return pl.CostEstimate(flops=flops, bytes_accessed=moved, transcendentals=0)


def halves(x):
    upper = x.astype(jnp.bfloat16)
    return upper, (x - upper.astype(jnp.float32)).astype(jnp.bfloat16)


def pack_kernel(place_ref, factor_ref, log_ref, cot_ref, out_ref):
    peers, lines, lanes = out_ref.shape
    heads, length = log_ref.shape
    roles, rows, _ = factor_ref.shape
    column = lax.broadcasted_iota(jnp.int32, (heads, lanes), 1)
    row = lax.broadcasted_iota(jnp.int32, (heads, lanes), 0)
    ends = jnp.sum(jnp.where(column == row, jnp.sum(cot_ref[...], axis=1, keepdims=True), 0.0), axis=0, keepdims=True)
    last = log_ref[:, length - 1 :]
    ends = ends + jnp.sum(jnp.where(column == row + heads, last, 0.0), axis=0, keepdims=True)
    upper, lower = halves(ends)
    rest = ends - upper.astype(jnp.float32)
    rest = rest - lower.astype(jnp.float32)
    line = lax.broadcasted_iota(jnp.int32, (lines - roles * rows, lanes), 0)
    tail = jnp.where(line == 0, upper.astype(jnp.float32), 0.0)
    tail = jnp.where(line == 1, lower.astype(jnp.float32), tail)
    tail = jnp.where(line == 2, rest, tail).astype(jnp.bfloat16)
    for peer in range(peers):
        for role in range(roles):
            out_ref[peer, role * rows : (role + 1) * rows, :] = factor_ref[role]
        out_ref[peer, roles * rows :, :] = tail


def packed(place, factors, log_cache, cache_cot, peers):
    roles, rows, rank = factors.shape
    heads, length = log_cache.shape
    shape = (peers, roles * rows + 16, rank // 2)
    whole = lambda i, place: (0, 0)
    return pl.pallas_call(
        pack_kernel,
        out_shape=jax.ShapeDtypeStruct(shape, jnp.bfloat16),
        grid_spec=pltpu.PrefetchScalarGridSpec(
            num_scalar_prefetch=1,
            grid=(1,),
            in_specs=[
                pl.BlockSpec((roles, rows, rank // 2), lambda i, place: (0, 0, place[2])),
                pl.BlockSpec((heads, length), whole),
                pl.BlockSpec((heads, length), whole),
            ],
            out_specs=pl.BlockSpec(shape, lambda i, place: (0, 0, 0)),
        ),
        compiler_params=ROOM,
        cost_estimate=cost(10**6, 2 * 10**6),
        name="packed",
    )(place, factors, log_cache, cache_cot)


def gate_kernel(place_ref, log_ref, cot_ref, ends_ref, input_ref, out_ref):
    me = place_ref[0]
    heads, length = log_ref.shape
    ends = ends_ref[...].astype(jnp.float32)
    ends = ends[:, 0, :] + ends[:, 1, :] + ends[:, 2, :]
    source = lax.broadcasted_iota(jnp.int32, ends.shape, 0)
    after = jnp.sum(jnp.where(source > me, ends, 0.0), axis=0, keepdims=True)
    before = jnp.sum(jnp.where(source == me - 1, ends, 0.0), axis=0, keepdims=True)
    lane = lax.broadcasted_iota(jnp.int32, (heads, ends.shape[1]), 1)
    row = lax.broadcasted_iota(jnp.int32, (heads, ends.shape[1]), 0)
    carried = jnp.sum(jnp.where(lane == row, after, 0.0), axis=1, keepdims=True)
    edge = jnp.sum(jnp.where(lane == row + heads, before, 0.0), axis=1, keepdims=True)
    place = lax.broadcasted_iota(jnp.int32, (heads, length), 1)
    total = cot_ref[...]
    step = 1
    while step < length:
        total = total + jnp.where(place < length - step, pltpu.roll(total, length - step, 1), 0.0)
        step *= 2
    log = log_ref[...]
    previous = jnp.where(place == 0, edge, pltpu.roll(log, 1, 1))
    delta = log - previous
    closed = -jnp.tanh(0.5 * delta) * (jnp.exp(delta) + 1.0)
    gate_cot = ((total + carried) * closed).astype(jnp.bfloat16)
    out_ref[...] = jnp.dot(gate_cot, input_ref[...], preferred_element_type=jnp.float32)


def gate_columns(place, log_cache, cache_cot, ends, saved_input, width):
    heads, length = log_cache.shape
    peers, lines, lanes = ends.shape
    whole = lambda i, place: (0, 0)
    return pl.pallas_call(
        gate_kernel,
        out_shape=jax.ShapeDtypeStruct((heads, width), jnp.float32),
        grid_spec=pltpu.PrefetchScalarGridSpec(
            num_scalar_prefetch=1,
            grid=(1,),
            in_specs=[
                pl.BlockSpec((heads, length), whole),
                pl.BlockSpec((heads, length), whole),
                pl.BlockSpec((peers, 16, lanes), lambda i, place: (0, lines // 16 - 1, 0)),
                pl.BlockSpec((length, width), lambda i, place: (0, place[1])),
            ],
            out_specs=pl.BlockSpec((heads, width), whole),
        ),
        compiler_params=ROOM,
        cost_estimate=cost(4 * 10**9, 4 * 10**6),
        name="gate_columns",
    )(place, log_cache, cache_cot, ends, saved_input)


def low_kernel(grad_ref, near_ref, far_ref, out_ref):
    role = pl.program_id(0)
    peers, rows, half = near_ref.shape
    sides = [ref[...].reshape(peers * rows, half) for ref in (near_ref, far_ref)]
    pieces = jnp.concatenate(sides, axis=1)
    upper, lower = halves(grad_ref[0])
    low = jnp.dot(upper, pieces, preferred_element_type=jnp.float32)
    low = low + jnp.dot(lower, pieces, preferred_element_type=jnp.float32)
    low = low.T
    lines = half // peers
    for side in range(2):
        part = low[side * half : (side + 1) * half].reshape(peers, lines, -1)
        start = pl.multiple_of(side * 3 * lines + role * lines, lines)
        out_ref[:, pl.ds(start, lines), :] = part


def low_parts(grad, near, far):
    roles, width, depth = grad.shape
    peers, _, half = near.shape
    rows = depth // peers
    lines = 2 * roles * half // peers
    factor_spec = pl.BlockSpec((peers, rows, half), lambda r: (0, r, 0))
    return pl.pallas_call(
        low_kernel,
        out_shape=jax.ShapeDtypeStruct((peers, lines, width), jnp.float32),
        grid=(roles,),
        in_specs=[
            pl.BlockSpec((1, width, depth), lambda r: (r, 0, 0)),
            factor_spec,
            factor_spec,
        ],
        out_specs=pl.BlockSpec((peers, lines, width), lambda r: (0, 0, 0)),
        compiler_params=ROOM,
        cost_estimate=cost(4 * roles * width * depth * 2 * half, 11 * 10**6),
        name="low_parts",
    )(grad, near, far)


def sum_kernel(arrived_ref, gate_ref, out_ref):
    peers, lines, _ = arrived_ref.shape
    total = jnp.sum(arrived_ref[...], axis=0)
    gate = gate_ref[...]
    for peer in range(peers):
        out_ref[peer, :lines, :] = total
        out_ref[peer, lines:, :] = gate


def summed(arrived, gate):
    peers, lines, width = arrived.shape
    return pl.pallas_call(
        sum_kernel,
        out_shape=jax.ShapeDtypeStruct((peers, lines + gate.shape[0], width), jnp.float32),
        in_specs=[VMEM, VMEM],
        out_specs=VMEM,
        compiler_params=ROOM,
        cost_estimate=cost(10**6, 2 * 10**6),
        name="summed",
    )(arrived, gate)


def moment_kernel(
    place_ref, sums_ref, first_ref, second_ref, first_new_ref, second_new_ref, upper_ref,
    lower_ref, shared_ref,
):
    core = place_ref[2]
    roles, rank, width = first_ref.shape
    peers, _, _ = sums_ref.shape
    half = rank // 2
    block = half // peers
    squares = jnp.zeros((half, width), jnp.float32)
    for side in range(2):
        for role in range(roles):
            at = (side * roles + role) * block
            low = sums_ref[:, at : at + block, :].reshape(half, width)
            at = pl.ds(pl.multiple_of((core ^ side) * half, half), half)
            first_new = BETA_ONE * first_ref[role, at] + (1.0 - BETA_ONE) * low
            second_new = BETA_TWO * second_ref[role, at] + (1.0 - BETA_TWO) * low * low
            direction = first_new / jnp.sqrt(second_new)
            first_new_ref[role, at] = first_new
            second_new_ref[role, at] = second_new
            squares = squares + direction * direction
            upper_ref[role, at], lower_ref[role, at] = halves(direction)
    squares = jnp.sum(squares, axis=(0, 1), keepdims=True)
    gate = jnp.sum(sums_ref[:, 2 * roles * block :, :], axis=0)
    heads = gate.shape[0]
    for copy in range(shared_ref.shape[0]):
        shared_ref[copy, :heads, :] = gate
        shared_ref[copy, heads:, :] = jnp.broadcast_to(squares, (8, width))


def moments(place, sums, first_moment, second_moment, copies):
    shape = first_moment.shape
    heads = sums.shape[1] - 2 * shape[0] * (shape[1] // 2 // sums.shape[0])
    like = lambda dtype: jax.ShapeDtypeStruct(shape, dtype)
    return pl.pallas_call(
        moment_kernel,
        out_shape=[
            like(jnp.float32),
            like(jnp.float32),
            like(jnp.bfloat16),
            like(jnp.bfloat16),
            jax.ShapeDtypeStruct((copies, heads + 8, shape[2]), jnp.float32),
        ],
        in_specs=[SMEM, VMEM, VMEM, VMEM],
        out_specs=[VMEM] * 5,
        compiler_params=ROOM,
        cost_estimate=cost(10**7, 6 * 10**6),
        name="moments",
    )(place, sums, first_moment, second_moment)


def product_kernel(factor_ref, upper_ref, lower_ref, out_ref):
    for role in range(factor_ref.shape[0]):
        out_ref[role] = jnp.dot(
            factor_ref[role], upper_ref[role], preferred_element_type=jnp.float32
        ) + jnp.dot(factor_ref[role], lower_ref[role], preferred_element_type=jnp.float32)


def products(factors, upper, lower):
    roles, rows, rank = factors.shape
    width = upper.shape[2]
    return pl.pallas_call(
        product_kernel,
        out_shape=jax.ShapeDtypeStruct((roles, rows, width), jnp.float32),
        in_specs=[VMEM] * 3,
        out_specs=VMEM,
        compiler_params=ROOM,
        cost_estimate=cost(4 * roles * rows * rank * width, 2 * 10**6),
        name="products",
    )(factors, upper, lower)


def local(
    saved_input,
    proj_cot,
    log_cache,
    cache_cot,
    proj_master,
    factors,
    first_moment,
    second_moment,
    gate_master,
    gate_first,
    gate_second,
):
    roles, rows, _ = factors.shape
    heads = log_cache.shape[0]
    width = proj_cot.shape[2]
    peers = lax.axis_size(FS)
    core = lax.axis_index("c")
    place = jnp.stack([lax.axis_index(FS), lax.axis_index(TP), core]).astype(jnp.int32)

    near = packed(place, factors, log_cache, cache_cot, peers)
    near = lax.all_to_all(near, FS, split_axis=0, concat_axis=0, tiled=True)
    far = lax.ppermute(near, "c", [(0, 1), (1, 0)])
    grad = jnp.einsum("td,rtw->rwd", saved_input, proj_cot, preferred_element_type=jnp.float32)
    parts = low_parts(grad, near, far)
    arrived = lax.all_to_all(parts, FS, split_axis=0, concat_axis=0, tiled=True)
    gate_part = gate_columns(place, log_cache, cache_cot, near, saved_input, width)
    sums = lax.all_to_all(summed(arrived, gate_part), FS, split_axis=0, concat_axis=0, tiled=True)

    first_new, second_new, upper, lower, shared = moments(
        place, sums, first_moment, second_moment, lax.axis_size(TP)
    )
    shared = lax.all_to_all(shared, TP, split_axis=0, concat_axis=0, tiled=True)
    squares = jnp.sum(shared[:, heads, 0])
    entries = first_new.size * lax.axis_size(TP)
    scale = lax.rsqrt(squares / entries + 1e-06)
    product = products(factors, upper, lower)
    proj_step = scale * product
    proj_new = proj_master - LEARN * proj_step
    proj_copy = from_everyone(proj_new.astype(jnp.bfloat16)[None], FS)
    proj_copy = proj_copy.reshape(peers, roles, rows, width)
    proj_copy = jnp.moveaxis(proj_copy, 0, 1).reshape(roles, peers * rows, width)
    gate_grad = jnp.moveaxis(shared[:, :heads], 0, 1).reshape(heads, -1)
    gate_first_new = BETA_ONE * gate_first + (1.0 - BETA_ONE) * gate_grad
    gate_second_new = BETA_TWO * gate_second + (1.0 - BETA_TWO) * gate_grad * gate_grad
    gate_new = gate_master - LEARN * gate_first_new / jnp.sqrt(gate_second_new)
    return (
        proj_step,
        proj_new,
        proj_copy,
        first_new,
        second_new,
        gate_new,
        gate_new.astype(jnp.bfloat16),
        gate_first_new,
        gate_second_new,
    )


def solution(mesh):
    fine = Mesh(mesh.devices.reshape(4, 4, 4, 2), (*FS, *TP))
    placed = (
        P(FS, None),
        P(None, FS, TP),
        P(None, FS),
        P(None, FS),
        P(None, FS, TP),
        P(None, FS, None),
        P(None, None, TP),
        P(None, None, TP),
        P(),
        P(),
        P(),
    )

    return jax.shard_map(
        local,
        mesh=fine,
        in_specs=placed,
        out_specs=(
            P(None, FS, TP),
            P(None, FS, TP),
            P(None, None, TP),
            P(None, None, TP),
            P(None, None, TP),
            P(),
            P(),
            P(),
            P(),
        ),
        check_vma=False,
    )
```

time: 180 us -> 169 us (0.939)
  matrix products: 36.7 us -> 14.6 us
  blocking collectives: 29.7 us -> 51.6 us
  Pallas kernels: 2.28 us -> 12.1 us
  starting transfers between devices: 20 us -> 11.8 us
  local copies, waits for them, and re-layouts: 16.8 us -> 8.78 us
  waiting for transfers between devices: 65.9 us -> 64.1 us
    dot_general x7 -> x1, matrix products: 36.7 us -> 14.6 us  [local(): jnp.einsum('td,rtw->rwd', saved_input, proj_cot, preferred_element_type=j...]
    all_to_all x2, blocking collectives: 29.7 us -> 51.6 us  [the longest x1 31.4 us: local(): near = lax.all_to_all(near, FS, split_axis=0, concat_axis=0, tiled=True)]
    all_to_all x4 -> x1, waiting for transfers between devices: 65.9 us -> 45.8 us  [from_everyone(): return lax.all_to_all(copies, axis, split_axis=0, concat_axis=0, tiled=True)]
    all_to_all x0 -> x2, waiting for transfers between devices: none -> 18.3 us  [the longest x1 11.8 us: local(): arrived = lax.all_to_all(parts, FS, split_axis=0, concat_axis=0, tiled=True)]
    all_to_all x4 -> x1, starting transfers between devices: 20 us -> 3.74 us  [from_everyone(): return lax.all_to_all(copies, axis, split_axis=0, concat_axis=0, tiled=True)]
    pallas_call x1 -> x6, Pallas kernels: 2.28 us -> 12.1 us  [the longest x1 5.7 us: low_parts(): pl.pallas_call(low_kernel, out_shape=jax.ShapeDtypeStruct((peers, lines,...]
    all_to_all x0 -> x2, starting transfers between devices: none -> 8.04 us  [the longest x1 4.43 us: local(): shared = lax.all_to_all(shared, TP, split_axis=0, concat_axis=0, tiled=True)]
    broadcast_in_dim x5 -> x1, local copies, waits for them, and re-layouts: 5.79 us -> 2.04 us  [from_everyone(): copies = jnp.broadcast_to(x, (lax.axis_size(axis), *x.shape))]
  transfers between devices with their start and end apart: 5 -> 4, of which waited for: 4 -> 3; matrix products, arithmetic and copies ran while one was open for 22% -> 10% of each run, Pallas kernels for 1% -> 2%
where the time goes in v2:
time: 169 us
  waiting for transfers between devices  64.1 us (38%)
  blocking collectives  51.6 us (31%)
  matrix products  14.6 us (9%)
  Pallas kernels  12.1 us (7%)
  starting transfers between devices  11.8 us (7%)
  local copies, waits for them, and re-layouts  8.78 us (5%)
  other arithmetic  4.4 us (3%)
    all_to_all x1, waiting for transfers between devices, from_everyone(): return lax.all_to_all(copies, axis, split_axis=0, concat_axis=0, tiled=True)  45.8 us
    all_to_all x1, blocking collectives, local(): near = lax.all_to_all(near, FS, split_axis=0, concat_axis=0, tiled=True)  31.4 us
    all_to_all x1, blocking collectives, local(): lax.all_to_all(summed(arrived, gate_part), FS, split_axis=0, concat_axis=...  20.1 us
    dot_general x1, matrix products, local(): jnp.einsum('td,rtw->rwd', saved_input, proj_cot, preferred_element_type=j...  14.6 us
    all_to_all x1, waiting for transfers between devices, local(): arrived = lax.all_to_all(parts, FS, split_axis=0, concat_axis=0, tiled=True)  11.8 us
    all_to_all x1, waiting for transfers between devices, local(): shared = lax.all_to_all(shared, TP, split_axis=0, concat_axis=0, tiled=True)  6.52 us
    pallas_call x1, Pallas kernels, low_parts(): pl.pallas_call(low_kernel, out_shape=jax.ShapeDtypeStruct((peers, lines,...  5.7 us
    unnamed x21, local copies, waits for them, and re-layouts  4.87 us
  transfers between devices with their start and end apart: 4, of which 3 were waited for; matrix products, arithmetic and copies ran while one was open for 10% of the time, Pallas kernels for 2%

profile of v2, /device:TPU:0, one launch (start us, length us, event | category | flops | bytes accessed | tf_op | source)
XLA Modules:
  0.0 168.8 jit_solution(1882424859124303188)
XLA Ops:
  0.7 0.1 pad_add_fusion.place_ref
  0.7 0.0 copy-start.2
  0.7 0.9 copy-done.2
  1.7 0.0 copy-start.4
  1.7 0.9 copy-done.4
  2.6 0.0 copy-start.6
  2.6 0.9 copy-done.6
  3.5 0.0 copy-start.9
  3.5 0.8 packed.1
  4.3 31.4 %all_to_all.25.near_ref.ends_ref = bf16[16,400,128]{2,1,0:T(8,128)(2,1)S(1)} all-to-all(bf16[16,400,128]{2,1,0:T(8,128)(2,1)S(1)} %packed.1), channel_id=1, replica_groups=mesh['z'=4,'x'=4,'y'=4,'c'=2] {'z','x'}, dimensions={0} | all-to-all | bytes 3276800 | tf_op jit(solution)/shard_map/all_to_all | solution.py:284
  35.7 0.0 collective-permute-start
  35.7 0.0 copy-done.9
  35.7 14.6 %fusion.grad_ref = f32[3,256,2048]{2,1,0:T(8,128)} fusion(bf16[3,3072,256]{2,1,0:T(8,128)(2,1)S(1)} %copy-done.9, bf16[3072,2048]{1,0:T(8,128)(2,1)} %input_ref.1), kind=kOutput, calls=%fused_computation | convolution fusion | flops 9663676416 | bytes 23592960 | tf_op jit(solution)/shard_map/td,rtw->rwd/dot_general | solution.py:286
  50.4 0.0 copy-start.5
  50.4 0.0 collective-permute-done.far_ref
  50.4 5.7 %low_parts.1 = f32[16,48,256]{2,1,0:T(8,128)} custom-call(f32[3,256,2048]{2,1,0:T(8,128)} %fusion.grad_ref, bf16[16,400,128]{2,1,0:T(8,128)(2,1)S(1)} %all_to_all.25.near_ref.ends_ref, bf16[16,400,128]{2,1,0:T(8,128)(2,1)S(1)} %collective-permute-done.far_ref), custom_call_target="tpu_custom_call" | custom-call | flops 1610612736 | bytes 11000000 | tf_op jit(solution)/shard_map/low_parts/pallas_call | solution.py:153
  56.1 3.6 %all-to-all-start.1 = ((f32[16,48,256]{2,1,0:T(8,128)}), f32[16,48,256]{2,1,0:T(8,128)S(1)}, u32[]{:S(2)}, u32[]{:S(2)}) async-start(f32[16,48,256]{2,1,0:T(8,128)} %low_parts.1), calls=%async_computation.1 | async-start | bytes 1572864 | tf_op jit(solution)/shard_map/all_to_all | solution.py:288
  59.7 0.0 copy-done.5
  59.7 0.0 copy-start.7
  59.7 0.9 copy-done.7
  60.6 0.0 copy-start
  60.6 2.8 %gate_columns.1.gate_ref = f32[16,256]{1,0:T(8,128)S(1)} custom-call(s32[3]{0:T(128)S(1)} %pad_add_fusion.place_ref, f32[16,3072]{1,0:T(8,128)S(1)} %copy-done.5, f32[16,3072]{1,0:T(8,128)S(1)} %copy-done.7, bf16[16,400,128]{2,1,0:T(8,128)(2,1)S(1)} %all_to_all.25.near_ref.ends_ref, bf16[3072,2048]{1,0:T(8,128)(2,1)} %input_ref.1), custom_call_target="tpu_custom_call" | custom-call | flops 4000000000 | bytes 4000000 | tf_op jit(solution)/shard_map/gate_columns/pallas_call | solution.py:111
  63.5 0.0 copy-start.3
  63.5 11.8 %all-to-all-done.1.arrived_ref = f32[16,48,256]{2,1,0:T(8,128)S(1)} async-done(((f32[16,48,256]{2,1,0:T(8,128)}), f32[16,48,256]{2,1,0:T(8,128)S(1)}, u32[]{:S(2)}, u32[]{:S(2)}) %all-to-all-start.1) | async-done | bytes 786464 | tf_op jit(solution)/shard_map/all_to_all | solution.py:288
  75.3 0.1 summed.1
  75.4 20.1 %all_to_all.26.sums_ref = f32[16,64,256]{2,1,0:T(8,128)S(1)} all-to-all(f32[16,64,256]{2,1,0:T(8,128)S(1)} %summed.1), channel_id=1, replica_groups=mesh['z'=4,'x'=4,'y'=4,'c'=2] {'z','x'}, dimensions={0} | all-to-all | bytes 2097152 | tf_op jit(solution)/shard_map/all_to_all | solution.py:290
  95.5 0.0 copy-done
  95.5 0.0 copy-start.1
  95.6 1.1 copy-done.1
  96.7 2.4 %moments.1 = (f32[3,256,256]{2,1,0:T(8,128)}, f32[3,256,256]{2,1,0:T(8,128)}, bf16[3,256,256]{2,1,0:T(8,128)(2,1)S(1)}, bf16[3,256,256]{2,1,0:T(8,128)(2,1)S(1)}, f32[8,24,256]{2,1,0:T(8,128)}) custom-call(s32[3]{0:T(128)S(1)} %pad_add_fusion.place_ref, f32[16,64,256]{2,1,0:T(8,128)S(1)} %all_to_all.26.sums_ref, f32[3,256,256]{2,1,0:T(8,128)S(1)} %copy-done, ...), custom_call_target="tpu_custom_call" | custom-call | flops 10000000 | bytes 6000000 | tf_op jit(solution)/shard_map/moments/pallas_call | solution.py:225
  99.0 4.4 %all-to-all-start.3 = ((f32[8,24,256]{2,1,0:T(8,128)}), f32[8,24,256]{2,1,0:T(8,128)S(1)}, u32[]{:S(2)}, u32[]{:S(2)}) async-start(f32[8,24,256]{2,1,0:T(8,128)} %get-tuple-element.14), calls=%async_computation.3 | async-start | bytes 393216 | tf_op jit(solution)/shard_map/all_to_all | solution.py:295
  103.5 0.0 copy-done.3
  103.5 0.3 products.1
  103.8 6.5 %all-to-all-done.3 = f32[8,24,256]{2,1,0:T(8,128)S(1)} async-done(((f32[8,24,256]{2,1,0:T(8,128)}), f32[8,24,256]{2,1,0:T(8,128)S(1)}, u32[]{:S(2)}, u32[]{:S(2)}) %all-to-all-start.3) | async-done | bytes 196640 | tf_op jit(solution)/shard_map/all_to_all | solution.py:295
  110.3 0.6 slice_reduce_fusion
  111.6 2.0 %fusion.5 = (bf16[3,128,256]{2,1,0:T(8,128)(2,1)S(1)}, f32[3,128,256]{2,1,0:T(8,128)}, f32[3,128,256]{2,1,0:T(8,128)}) fusion(f32[3,128,256]{2,1,0:T(8,128)} %param.15, f32[3,128,256]{2,1,0:T(8,128)S(1)} %products.1, f32[]{:T(128)S(6)} %rsqrt.4), kind=kLoop, calls=%fused_computation.12 | loop fusion | flops 393216 | bytes 1769476 | tf_op jit(solution)/shard_map/convert_element_type | solution.py:302
  113.5 0.0 copy-start.8
  113.5 2.0 %broadcast_in_dim.4 = bf16[16,1,3,128,256]{4,3,2,1,0:T(8,128)(2,1)} broadcast(bf16[3,128,256]{2,1,0:T(8,128)(2,1)S(1)} %get-tuple-element.23), dimensions={2,3,4} | broadcast | bytes 3342336 | tf_op jit(solution)/shard_map/broadcast_in_dim | solution.py:17
  115.6 3.7 %all-to-all-start.4 = ((bf16[16,1,3,128,256]{4,3,2,1,0:T(8,128)(2,1)}), bf16[16,1,3,128,256]{4,3,2,1,0:T(8,128)(2,1)S(1)}, u32[]{:S(2)}, u32[]{:S(2)}) async-start(bf16[16,1,3,128,256]{4,3,2,1,0:T(8,128)(2,1)} %broadcast_in_dim.4), calls=%async_computation.4 | async-start | bytes 6291456 | tf_op jit(solution)/shard_map/all_to_all | solution.py:18
  119.4 0.0 copy-done.8
  119.4 1.8 %fusion.3 = (bf16[16,2048]{1,0:T(8,128)(2,1)}, f32[16,2048]{1,0:T(8,128)}, f32[16,2048]{1,0:T(8,128)}, f32[16,2048]{1,0:T(8,128)}) fusion(f32[16,2048]{1,0:T(8,128)S(1)} %copy-done.8, f32[16,2048]{1,0:T(8,128)S(1)} %bitcast.17, f32[16,2048]{1,0:T(8,128)} %param.20, f32[16,2048]{1,0:T(8,128)} %param.21), kind=kLoop, calls=%fused_computation.11 | loop fusion | flops 360448 | bytes 983040 | tf_op jit(solution)/shard_map/convert_element_type | solution.py:316
  121.1 45.8 %all-to-all-done.4 = bf16[16,1,3,128,256]{4,3,2,1,0:T(8,128)(2,1)S(1)} async-done(((bf16[16,1,3,128,256]{4,3,2,1,0:T(8,128)(2,1)}), bf16[16,1,3,128,256]{4,3,2,1,0:T(8,128)(2,1)S(1)}, u32[]{:S(2)}, u32[]{:S(2)}) %all-to-all-start.4) | async-done | bytes 3145760 | tf_op jit(solution)/shard_map/all_to_all | solution.py:18
  166.9 1.9 %copy.26 = bf16[16,1,3,128,256]{4,3,0,2,1:T(8,128)(2,1)} copy(bf16[16,1,3,128,256]{4,3,2,1,0:T(8,128)(2,1)S(1)} %all-to-all-done.4) | data formatting | bytes 6291456 | tf_op jit(solution)/shard_map/all_to_all | solution.py:18
  (2 shorter events, 0.0 us)
Async XLA Ops:
  0.7 0.9 copy-start.2
  1.7 0.9 copy-start.4
  2.6 0.9 copy-start.6
  3.5 32.2 %copy-start.9 = (bf16[3,3072,256]{2,1,0:T(8,128)(2,1)S(1)}, bf16[3,3072,256]{2,1,0:T(8,128)(2,1)}, u32[]{:S(2)}) copy-start(bf16[3,3072,256]{2,1,0:T(8,128)(2,1)} %param.12) | copy-start | bytes 14155780
  35.7 14.6 %collective-permute-start = (bf16[16,400,128]{2,1,0:T(8,128)(2,1)S(1)}, bf16[16,400,128]{2,1,0:T(8,128)(2,1)S(1)}, u32[]{:S(2)}, u32[]{:S(2)}) collective-permute-start(bf16[16,400,128]{2,1,0:T(8,128)(2,1)S(1)} %all_to_all.25.near_ref.ends_ref), channel_id=1, source_target_pairs={{0,1},{1,0},{2,3},{3,2},{4,5},{5,4},{6,7},{7,6},{8,9},{9,8},{10,11... | collective-permute-start | bytes 4915208 | tf_op jit(solution)/shard_map/ppermute | solution.py:285
  50.4 9.3 %copy-start.5 = (f32[16,3072]{1,0:T(8,128)S(1)}, f32[16,3072]{1,0:T(8,128)}, u32[]{:S(2)}) copy-start(f32[16,3072]{1,0:T(8,128)} %log_ref.3) | copy-start | bytes 589828
  56.1 19.2 %all-to-all-start.1 = ((f32[16,48,256]{2,1,0:T(8,128)}), f32[16,48,256]{2,1,0:T(8,128)S(1)}, u32[]{:S(2)}, u32[]{:S(2)}) async-start(f32[16,48,256]{2,1,0:T(8,128)} %low_parts.1), calls=%async_computation.1 | async-start | bytes 1572864 | tf_op jit(solution)/shard_map/all_to_all | solution.py:288
  59.7 0.9 copy-start.7
  60.6 34.9 %copy-start = (f32[3,256,256]{2,1,0:T(8,128)S(1)}, f32[3,256,256]{2,1,0:T(8,128)}, u32[]{:S(2)}) copy-start(f32[3,256,256]{2,1,0:T(8,128)} %first_ref.1) | copy-start | bytes 2359300
  63.5 40.0 %copy-start.3 = (bf16[3,128,256]{2,1,0:T(8,128)(2,1)S(1)}, bf16[3,128,256]{2,1,0:T(8,128)(2,1)}, u32[]{:S(2)}) copy-start(bf16[3,128,256]{2,1,0:T(8,128)(2,1)} %factor_ref.3) | copy-start | bytes 589828
  95.5 1.1 copy-start.1
  99.0 11.2 %all-to-all-start.3 = ((f32[8,24,256]{2,1,0:T(8,128)}), f32[8,24,256]{2,1,0:T(8,128)S(1)}, u32[]{:S(2)}, u32[]{:S(2)}) async-start(f32[8,24,256]{2,1,0:T(8,128)} %get-tuple-element.14), calls=%async_computation.3 | async-start | bytes 393216 | tf_op jit(solution)/shard_map/all_to_all | solution.py:295
  113.5 5.8 %copy-start.8 = (f32[16,2048]{1,0:T(8,128)S(1)}, f32[16,2048]{1,0:T(8,128)}, u32[]{:S(2)}) copy-start(f32[16,2048]{1,0:T(8,128)} %param.19) | copy-start | bytes 393220
  115.6 51.3 %all-to-all-start.4 = ((bf16[16,1,3,128,256]{4,3,2,1,0:T(8,128)(2,1)}), bf16[16,1,3,128,256]{4,3,2,1,0:T(8,128)(2,1)S(1)}, u32[]{:S(2)}, u32[]{:S(2)}) async-start(bf16[16,1,3,128,256]{4,3,2,1,0:T(8,128)(2,1)} %broadcast_in_dim.4), calls=%async_computation.4 | async-start | bytes 6291456 | tf_op jit(solution)/shard_map/all_to_all | solution.py:18

commit v3 on v2

v3 whole, which is shorter than its diff:
```python
import functools

import jax
import jax.numpy as jnp
from jax import lax
from jax.experimental import pallas as pl
from jax.experimental.pallas import tpu as pltpu
from jax.sharding import Mesh
from jax.sharding import PartitionSpec as P

BETA_ONE = 0.8
BETA_TWO = 0.9
LEARN = 0.001
FS = ("z", "x")
TP = ("y", "c")


VMEM = pl.BlockSpec(memory_space=pltpu.VMEM)
SMEM = pl.BlockSpec(memory_space=pltpu.SMEM)
HBM = pl.BlockSpec(memory_space=pltpu.HBM)


def room(mebibytes):
    return pltpu.CompilerParams(vmem_limit_bytes=mebibytes * 2**20)


def held(space, *arrays):
    return [pltpu.with_memory_space_constraint(a, space) for a in arrays]


def cost(flops, moved):
    return pl.CostEstimate(flops=flops, bytes_accessed=moved, transcendentals=0)


def halves(x):
    upper = x.astype(jnp.bfloat16)
    return upper, (x - upper.astype(jnp.float32)).astype(jnp.bfloat16)


def started(pairs, sems):
    copies = [pltpu.make_async_copy(a, b, sems.at[n]) for n, (a, b) in enumerate(pairs)]
    for copy in copies:
        copy.start()
    return copies


def finished(copies):
    for copy in copies:
        copy.wait()


def pack_kernel(
    place_ref, factor_ref, log_ref, cot_ref, out_ref, last, cot, block, read_sems, write_sems
):
    peers, lines, lanes = out_ref.shape
    heads, length = log_ref.shape
    roles, rows, _ = factor_ref.shape
    at = pl.ds(pl.multiple_of(place_ref[2] * lanes, lanes), lanes)
    reads = [(factor_ref.at[r, :, at], block.at[pl.ds(r * rows, rows)]) for r in range(roles)]
    reads += [(log_ref.at[:, pl.ds(length - lanes, lanes)], last), (cot_ref, cot)]
    finished(started(reads, read_sems))
    column = lax.broadcasted_iota(jnp.int32, (heads, lanes), 1)
    row = lax.broadcasted_iota(jnp.int32, (heads, lanes), 0)
    totals = jnp.sum(cot[...], axis=1, keepdims=True)
    ends = jnp.where(column == row, totals, 0.0)
    ends = ends + jnp.where(column == row + heads, last[:, lanes - 1 :], 0.0)
    ends = jnp.sum(ends, axis=0, keepdims=True)
    upper, lower = halves(ends)
    rest = ends - upper.astype(jnp.float32)
    rest = rest - lower.astype(jnp.float32)
    line = lax.broadcasted_iota(jnp.int32, (lines - roles * rows, lanes), 0)
    tail = jnp.where(line == 0, upper.astype(jnp.float32), 0.0)
    tail = jnp.where(line == 1, lower.astype(jnp.float32), tail)
    tail = jnp.where(line == 2, rest, tail).astype(jnp.bfloat16)
    block[roles * rows :, :] = tail
    finished(started([(block, out_ref.at[peer]) for peer in range(peers)], write_sems))


def packed(place, factors, log_cache, cache_cot, peers):
    roles, rows, rank = factors.shape
    heads, length = log_cache.shape
    lanes = rank // 2
    lines = roles * rows + 16
    return pl.pallas_call(
        pack_kernel,
        out_shape=pltpu.HBM((peers, lines, lanes), jnp.bfloat16),
        in_specs=[SMEM, HBM, HBM, HBM],
        out_specs=HBM,
        scratch_shapes=[
            pltpu.VMEM((heads, lanes), jnp.float32),
            pltpu.VMEM((heads, length), jnp.float32),
            pltpu.VMEM((lines, lanes), jnp.bfloat16),
            pltpu.SemaphoreType.DMA((roles + 2,)),
            pltpu.SemaphoreType.DMA((peers,)),
        ],
        compiler_params=room(8),
        cost_estimate=cost(10**6, 2 * 10**6),
        name="packed",
    )(place, *held(pltpu.HBM, factors, log_cache, cache_cot))


def gate_kernel(
    place_ref, log_hbm, cot_hbm, ends_hbm, input_hbm, out_ref, log_ref, cot_ref, ends_ref,
    input_ref, sems,
):
    lines, width = ends_hbm.shape[1], input_ref.shape[1]
    at = pl.ds(pl.multiple_of(place_ref[1] * width, width), width)
    reads = [
        (log_hbm, log_ref),
        (cot_hbm, cot_ref),
        (ends_hbm.at[:, pl.ds(lines - 16, 16)], ends_ref),
        (input_hbm.at[:, at], input_ref),
    ]
    reads = started(reads, sems)
    finished(reads[:3])
    me = place_ref[0]
    heads, length = log_ref.shape
    ends = ends_ref[...].astype(jnp.float32)
    ends = ends[:, 0, :] + ends[:, 1, :] + ends[:, 2, :]
    source = lax.broadcasted_iota(jnp.int32, ends.shape, 0)
    after = jnp.sum(jnp.where(source > me, ends, 0.0), axis=0, keepdims=True)
    before = jnp.sum(jnp.where(source == me - 1, ends, 0.0), axis=0, keepdims=True)
    lane = lax.broadcasted_iota(jnp.int32, (heads, ends.shape[1]), 1)
    row = lax.broadcasted_iota(jnp.int32, (heads, ends.shape[1]), 0)
    carried = jnp.sum(jnp.where(lane == row, after, 0.0), axis=1, keepdims=True)
    edge = jnp.sum(jnp.where(lane == row + heads, before, 0.0), axis=1, keepdims=True)
    place = lax.broadcasted_iota(jnp.int32, (heads, length), 1)
    total = cot_ref[...]
    step = 1
    while step < length:
        total = total + jnp.where(place < length - step, pltpu.roll(total, length - step, 1), 0.0)
        step *= 2
    log = log_ref[...]
    previous = jnp.where(place == 0, edge, pltpu.roll(log, 1, 1))
    delta = log - previous
    closed = -jnp.tanh(0.5 * delta) * (jnp.exp(delta) + 1.0)
    gate_cot = ((total + carried) * closed).astype(jnp.bfloat16)
    finished(reads[3:])
    out_ref[...] = jnp.dot(gate_cot, input_ref[...], preferred_element_type=jnp.float32)


def gate_columns(place, log_cache, cache_cot, ends, saved_input, width):
    heads, length = log_cache.shape
    peers, _, lanes = ends.shape
    return pl.pallas_call(
        gate_kernel,
        out_shape=jax.ShapeDtypeStruct((heads, width), jnp.float32),
        in_specs=[SMEM, HBM, HBM, HBM, HBM],
        out_specs=VMEM,
        scratch_shapes=[
            pltpu.VMEM((heads, length), jnp.float32),
            pltpu.VMEM((heads, length), jnp.float32),
            pltpu.VMEM((peers, 16, lanes), jnp.bfloat16),
            pltpu.VMEM((length, width), jnp.bfloat16),
            pltpu.SemaphoreType.DMA((4,)),
        ],
        compiler_params=room(10),
        cost_estimate=cost(4 * 10**9, 4 * 10**6),
        name="gate_columns",
    )(place, *held(pltpu.HBM, log_cache, cache_cot, ends, saved_input))


def low_kernel(grad_ref, near_ref, far_ref, out_ref):
    role = pl.program_id(0)
    peers, rows, half = near_ref.shape
    sides = [ref[...].reshape(peers * rows, half) for ref in (near_ref, far_ref)]
    pieces = jnp.concatenate(sides, axis=1)
    upper, lower = halves(grad_ref[0])
    low = jnp.dot(upper, pieces, preferred_element_type=jnp.float32)
    low = low + jnp.dot(lower, pieces, preferred_element_type=jnp.float32)
    low = low.T
    lines = half // peers
    for side in range(2):
        part = low[side * half : (side + 1) * half].reshape(peers, lines, -1)
        start = pl.multiple_of(side * 3 * lines + role * lines, lines)
        out_ref[:, pl.ds(start, lines), :] = part


def low_parts(grad, near, far):
    roles, width, depth = grad.shape
    peers, _, half = near.shape
    rows = depth // peers
    lines = 2 * roles * half // peers
    factor_spec = pl.BlockSpec((peers, rows, half), lambda r: (0, r, 0))
    return pl.pallas_call(
        low_kernel,
        out_shape=pltpu.HBM((peers, lines, width), jnp.float32),
        grid=(roles,),
        in_specs=[
            pl.BlockSpec((1, width, depth), lambda r: (r, 0, 0)),
            factor_spec,
            factor_spec,
        ],
        out_specs=pl.BlockSpec((peers, lines, width), lambda r: (0, 0, 0)),
        compiler_params=room(20),
        cost_estimate=cost(4 * roles * width * depth * 2 * half, 11 * 10**6),
        name="low_parts",
    )(*held(pltpu.HBM, grad), near, far)


def sum_kernel(arrived_ref, gate_ref, out_ref, block, sems):
    peers, lines, _ = arrived_ref.shape
    block[:lines, :] = jnp.sum(arrived_ref[...], axis=0)
    block[lines:, :] = gate_ref[...]
    finished(started([(block, out_ref.at[peer]) for peer in range(peers)], sems))


def summed(arrived, gate):
    peers, lines, width = arrived.shape
    lines = lines + gate.shape[0]
    return pl.pallas_call(
        sum_kernel,
        out_shape=pltpu.HBM((peers, lines, width), jnp.float32),
        in_specs=[VMEM, VMEM],
        out_specs=HBM,
        scratch_shapes=[
            pltpu.VMEM((lines, width), jnp.float32),
            pltpu.SemaphoreType.DMA((peers,)),
        ],
        compiler_params=room(8),
        cost_estimate=cost(10**6, 2 * 10**6),
        name="summed",
    )(arrived, gate)


def moment_kernel(
    place_ref, sums_ref, first_hbm, second_hbm, first_new_hbm, second_new_hbm, upper_ref,
    lower_ref, shared_hbm, first_ref, second_ref, first_new_ref, second_new_ref, message, sems,
):
    core = place_ref[2]
    finished(started([(first_hbm, first_ref), (second_hbm, second_ref)], sems))
    roles, rank, width = first_ref.shape
    peers, _, _ = sums_ref.shape
    half = rank // 2
    block = half // peers
    squares = jnp.zeros((half, width), jnp.float32)
    for side in range(2):
        for role in range(roles):
            at = (side * roles + role) * block
            low = sums_ref[:, at : at + block, :].reshape(half, width)
            at = pl.ds(pl.multiple_of((core ^ side) * half, half), half)
            first_new = BETA_ONE * first_ref[role, at] + (1.0 - BETA_ONE) * low
            second_new = BETA_TWO * second_ref[role, at] + (1.0 - BETA_TWO) * low * low
            direction = first_new / jnp.sqrt(second_new)
            first_new_ref[role, at] = first_new
            second_new_ref[role, at] = second_new
            squares = squares + direction * direction
            upper_ref[role, at], lower_ref[role, at] = halves(direction)
    squares = jnp.sum(squares, axis=(0, 1), keepdims=True)
    gate = jnp.sum(sums_ref[:, 2 * roles * block :, :], axis=0)
    heads = gate.shape[0]
    message[:heads, :] = gate
    message[heads:, :] = jnp.broadcast_to(squares, (8, width))
    writes = [(message, shared_hbm.at[copy]) for copy in range(shared_hbm.shape[0])]
    writes += [(first_new_ref, first_new_hbm), (second_new_ref, second_new_hbm)]
    finished(started(writes, sems))


def moments(place, sums, first_moment, second_moment, copies):
    shape = first_moment.shape
    heads = sums.shape[1] - 2 * shape[0] * (shape[1] // 2 // sums.shape[0])
    return pl.pallas_call(
        moment_kernel,
        out_shape=[
            pltpu.HBM(shape, jnp.float32),
            pltpu.HBM(shape, jnp.float32),
            pltpu.VMEM(shape, jnp.bfloat16),
            pltpu.VMEM(shape, jnp.bfloat16),
            pltpu.HBM((copies, heads + 8, shape[2]), jnp.float32),
        ],
        in_specs=[SMEM, VMEM, HBM, HBM],
        out_specs=[HBM, HBM, VMEM, VMEM, HBM],
        scratch_shapes=[pltpu.VMEM(shape, jnp.float32)] * 4
        + [
            pltpu.VMEM((heads + 8, shape[2]), jnp.float32),
            pltpu.SemaphoreType.DMA((copies + 2,)),
        ],
        compiler_params=room(12),
        cost_estimate=cost(10**7, 6 * 10**6),
        name="moments",
    )(place, sums, *held(pltpu.HBM, first_moment, second_moment))


def product_kernel(place_ref, near_ref, far_ref, upper_ref, lower_ref, out_ref):
    roles, depth, _ = out_ref.shape
    peers, _, half = near_ref.shape
    rows = depth // peers
    core = place_ref[2]
    for role in range(roles):
        total = None
        for side, ref in enumerate((near_ref, far_ref)):
            pieces = ref[:, role * rows : (role + 1) * rows, :].reshape(depth, half)
            at = pl.ds(pl.multiple_of((core ^ side) * half, half), half)
            for part in (upper_ref, lower_ref):
                term = jnp.dot(pieces, part[role, at], preferred_element_type=jnp.float32)
                total = term if total is None else total + term
        out_ref[role] = total


def products(place, near, far, upper, lower, rows):
    roles, rank, width = upper.shape
    depth = near.shape[0] * rows
    return pl.pallas_call(
        product_kernel,
        out_shape=pltpu.VMEM((roles, depth, width), jnp.float32),
        in_specs=[SMEM, VMEM, VMEM, VMEM, VMEM],
        out_specs=VMEM,
        compiler_params=room(20),
        cost_estimate=cost(4 * roles * depth * rank * width, 10**7),
        name="products",
    )(place, near, far, *held(pltpu.VMEM, upper, lower))


def final_kernel(entries, place_ref, shared_ref, product_ref, *refs):
    pieces, refs = refs[:10], refs[10:]
    inputs, outputs, refs = refs[:4], refs[4:11], refs[11:]
    kept, made, read_sems, write_sems = refs[:4], refs[4:11], refs[11], refs[12]
    master_ref, gate_master_ref, gate_first_ref, gate_second_ref = kept
    step_ref, new_ref, copy_ref, *gate_refs = made
    reads = started(zip(inputs, kept), read_sems)
    heads = gate_master_ref.shape[0]
    roles, rows, width = master_ref.shape
    squares = jnp.sum(shared_ref[:, heads, 0:1], axis=0, keepdims=True)
    scale = 1.0 / jnp.sqrt(squares / entries + 1e-06)
    along = place_ref[3], place_ref[4]
    side = rows // 2
    writes = []
    for role in range(roles):
        for part in range(2):
            for first in range(4):
                for second in range(4):
                    offsets = (first, second) if part == 0 else (second, first)
                    source = [(along[n] + 4 - offsets[n]) % 4 for n in range(2)]
                    source = source[0] * 4 + source[1]
                    if second == 2:
                        ref, index = pieces[part * 5 + 3 + first // 2], first % 2
                    else:
                        ref, index = pieces[part * 5 + (0, 1, None, 2)[second]], first
                    at = pl.ds(pl.multiple_of(source * rows + part * side, side), side)
                    step = scale * product_ref[role, at]
                    new = ref[index, role] - LEARN * step
                    copy_ref[role, at] = new.astype(jnp.bfloat16)
        writes += started([(copy_ref.at[role], outputs[2].at[role])], write_sems.at[pl.ds(role, 1)])
    finished(reads)
    at = pl.ds(pl.multiple_of(place_ref[0] * rows, rows), rows)
    for role in range(roles):
        step = scale * product_ref[role, at]
        step_ref[role] = step
        new_ref[role] = master_ref[role] - LEARN * step
    for peer in range(shared_ref.shape[0]):
        at = slice(peer * width, (peer + 1) * width)
        grad = shared_ref[peer, :heads]
        first = BETA_ONE * gate_first_ref[:, at] + (1.0 - BETA_ONE) * grad
        second = BETA_TWO * gate_second_ref[:, at] + (1.0 - BETA_TWO) * grad * grad
        new = gate_master_ref[:, at] - LEARN * first / jnp.sqrt(second)
        gate_refs[0][:, at] = new
        gate_refs[1][:, at] = new.astype(jnp.bfloat16)
        gate_refs[2][:, at] = first
        gate_refs[3][:, at] = second
    rest = [(made[n], outputs[n]) for n in (0, 1, 3, 4, 5, 6)]
    finished(writes + started(rest, write_sems.at[pl.ds(roles, 6)]))


def finals(entries, place, shared, product, pieces, master, gates):
    roles = master.shape[0]
    outs = [
        (master.shape, jnp.float32),
        (master.shape, jnp.float32),
        (product.shape, jnp.bfloat16),
        (gates[0].shape, jnp.float32),
        (gates[0].shape, jnp.bfloat16),
        (gates[0].shape, jnp.float32),
        (gates[0].shape, jnp.float32),
    ]
    kept = [(a.shape, a.dtype) for a in (master, *gates)]
    return pl.pallas_call(
        functools.partial(final_kernel, entries),
        out_shape=[pltpu.HBM(*out) for out in outs],
        in_specs=[SMEM, VMEM, VMEM] + [VMEM] * 10 + [HBM] * 4,
        out_specs=[HBM] * 7,
        scratch_shapes=[pltpu.VMEM(*a) for a in kept + outs]
        + [pltpu.SemaphoreType.DMA((4,)), pltpu.SemaphoreType.DMA((roles + 6,))],
        compiler_params=room(20),
        cost_estimate=cost(10**7, 16 * 10**6),
        name="finals",
    )(place, shared, *held(pltpu.VMEM, product), *pieces, *held(pltpu.HBM, master, *gates))


def shift(x, axis, by):
    return lax.ppermute(x, axis, [(i, (i + by) % 4) for i in range(4)])


def local(
    saved_input,
    proj_cot,
    log_cache,
    cache_cot,
    proj_master,
    factors,
    first_moment,
    second_moment,
    gate_master,
    gate_first,
    gate_second,
):
    roles, rows, _ = factors.shape
    width = proj_cot.shape[2]
    peers = lax.axis_size(FS)
    place = [lax.axis_index(name) for name in (FS, TP, "c", "z", "x")]
    place = jnp.stack(place).astype(jnp.int32)

    near = packed(place, factors, log_cache, cache_cot, peers)
    near = lax.all_to_all(near, FS, split_axis=0, concat_axis=0, tiled=True)
    far = lax.ppermute(near, "c", [(0, 1), (1, 0)])
    sides = proj_master.reshape(roles, 2, rows // 2, width)
    sides = [(sides[:, part][None], axis) for part, axis in enumerate(FS)]
    sides = [[side] + [shift(side, axis, by) for by in (1, 2, 3)] for side, axis in sides]
    sides = [jnp.concatenate(side) for side in sides]
    ahead = [shift(side, axis, 1) for side, axis in zip(sides, FS[::-1])]
    behind = [shift(side, axis, 3) for side, axis in zip(sides, FS[::-1])]
    opposite = [shift(side[:2], axis, 1) for side, axis in zip(ahead, FS[::-1])]
    other = [shift(side[2:], axis, 3) for side, axis in zip(behind, FS[::-1])]
    pieces = [x for group in zip(sides, ahead, behind, opposite, other) for x in group]
    grad = jnp.einsum("td,rtw->rwd", saved_input, proj_cot, preferred_element_type=jnp.float32)
    parts = low_parts(grad, near, far)
    arrived = lax.all_to_all(parts, FS, split_axis=0, concat_axis=0, tiled=True)
    gate_part = gate_columns(place, log_cache, cache_cot, near, saved_input, width)
    sums = lax.all_to_all(summed(arrived, gate_part), FS, split_axis=0, concat_axis=0, tiled=True)

    first_new, second_new, upper, lower, shared = moments(
        place, sums, first_moment, second_moment, lax.axis_size(TP)
    )
    shared = lax.all_to_all(shared, TP, split_axis=0, concat_axis=0, tiled=True)
    product = products(place, near, far, upper, lower, rows)
    entries = first_new.size * lax.axis_size(TP)
    gates = (gate_master, gate_first, gate_second)
    step, new, copy, *gates = finals(entries, place, shared, product, pieces, proj_master, gates)
    return step, new, copy, first_new, second_new, *gates


def solution(mesh):
    fine = Mesh(mesh.devices.reshape(4, 4, 4, 2), (*FS, *TP))
    placed = (
        P(FS, None),
        P(None, FS, TP),
        P(None, FS),
        P(None, FS),
        P(None, FS, TP),
        P(None, FS, None),
        P(None, None, TP),
        P(None, None, TP),
        P(),
        P(),
        P(),
    )

    return jax.shard_map(
        local,
        mesh=fine,
        in_specs=placed,
        out_specs=(
            P(None, FS, TP),
            P(None, FS, TP),
            P(None, None, TP),
            P(None, None, TP),
            P(None, None, TP),
            P(),
            P(),
            P(),
            P(),
        ),
        check_vma=False,
    )
```

time: 169 us -> 154 us (0.911); the launches traced: 169 us -> 152 us
  waiting for transfers between devices: 64.1 us -> 21.3 us
  starting transfers between devices: 11.8 us -> 36 us
  blocking collectives: 51.6 us -> 31.5 us
  Pallas kernels: 12.1 us -> 28.9 us
  local copies, waits for them, and re-layouts: 8.78 us -> 16.2 us
  other arithmetic: 4.4 us -> 1.92 us
    all_to_all x1, waiting for transfers between devices: 45.8 us -> 0.01 us  [local(): lax.all_to_all(summed(arrived, gate_part), FS, split_axis=0, concat_axis=...]
    ppermute x0 -> x14, waiting for transfers between devices: none -> 21.3 us  [shift(): return lax.ppermute(x, axis, [(i, (i + by) % 4) for i in range(4)])]
    all_to_all x1 -> x0, blocking collectives: 20.1 us -> none  [local(): lax.all_to_all(summed(arrived, gate_part), FS, split_axis=0, concat_axis=...]
    ppermute x0 -> x14, starting transfers between devices: none -> 19 us  [shift(): return lax.ppermute(x, axis, [(i, (i + by) % 4) for i in range(4)])]
    pallas_call x5 -> x6, Pallas kernels: 9.22 us -> 26.4 us  [the longest x1 6.27 us: finals(): pl.pallas_call(functools.partial(final_kernel, entries), out_shape=[pltpu...]
    all_to_all x1, waiting for transfers between devices: 11.8 us -> 0.01 us  [local(): arrived = lax.all_to_all(parts, FS, split_axis=0, concat_axis=0, tiled=True)]
    slice x0 -> x4, local copies, waits for them, and re-layouts: none -> 7.17 us  [the longest x2 3.61 us: local(): other = [shift(side[2:], axis, 3) for side, axis in zip(behind, FS[::-1])]]
    all_to_all x1, waiting for transfers between devices: 6.52 us -> 0.01 us  [local(): shared = lax.all_to_all(shared, TP, split_axis=0, concat_axis=0, tiled=True)]
  transfers between devices with their start and end apart: 4 -> 18, of which waited for: 3 -> 5; matrix products, arithmetic and copies ran while one was open for 10% -> 16% of each run, Pallas kernels for 2% -> 13%
where the time goes in v3:
time: 154 us; the launch traced here: 152 us
  starting transfers between devices  36 us (23%)
  blocking collectives  31.5 us (20%)
  Pallas kernels  28.9 us (19%)
  waiting for transfers between devices  21.3 us (14%)
  local copies, waits for them, and re-layouts  16.2 us (11%)
  matrix products  15 us (10%)
  other arithmetic  1.92 us (1%)
    all_to_all x1, blocking collectives, local(): near = lax.all_to_all(near, FS, split_axis=0, concat_axis=0, tiled=True)  31.5 us
    ppermute x14, waiting for transfers between devices, shift(): return lax.ppermute(x, axis, [(i, (i + by) % 4) for i in range(4)])  21.3 us
    ppermute x14, starting transfers between devices, shift(): return lax.ppermute(x, axis, [(i, (i + by) % 4) for i in range(4)])  19 us
    dot_general x1, matrix products, local(): jnp.einsum('td,rtw->rwd', saved_input, proj_cot, preferred_element_type=j...  15 us
    unnamed x20, local copies, waits for them, and re-layouts  8.9 us
    all_to_all x1, starting transfers between devices, local(): lax.all_to_all(summed(arrived, gate_part), FS, split_axis=0, concat_axis=...  6.84 us
    pallas_call x1, Pallas kernels, finals(): pl.pallas_call(functools.partial(final_kernel, entries), out_shape=[pltpu...  6.27 us
    all_to_all x1, starting transfers between devices, local(): arrived = lax.all_to_all(parts, FS, split_axis=0, concat_axis=0, tiled=True)  5.73 us
  transfers between devices with their start and end apart: 18, of which 5 were waited for; matrix products, arithmetic and copies ran while one was open for 16% of the time, Pallas kernels for 13%

profile of v3, /device:TPU:0, one launch (start us, length us, event | category | flops | bytes accessed | tf_op | source)
XLA Modules:
  0.0 151.8 jit_solution(3596871996059410464)
XLA Ops:
  0.6 0.0 copy-start.8
  0.7 0.1 stack.23.place_ref
  0.8 3.3 %packed.1 = bf16[16,400,128]{2,1,0:T(8,128)(2,1)} custom-call(s32[5]{0:T(128)S(1)} %stack.23.place_ref, bf16[3,128,256]{2,1,0:T(8,128)(2,1)} %factor_ref.1, f32[16,3072]{1,0:T(8,128)} %log_hbm.1, f32[16,3072]{1,0:T(8,128)} %cot_hbm.1), custom_call_target="tpu_custom_call" | custom-call | flops 1000000 | bytes 2000000 | tf_op jit(solution)/shard_map/packed/pallas_call | solution.py:84
  4.0 31.5 %all_to_all.20.near_ref.ends_hbm = bf16[16,400,128]{2,1,0:T(8,128)(2,1)S(1)} all-to-all(bf16[16,400,128]{2,1,0:T(8,128)(2,1)} %packed.1), channel_id=1, replica_groups=mesh['z'=4,'x'=4,'y'=4,'c'=2] {'z','x'}, dimensions={0} | all-to-all | bytes 3276800 | tf_op jit(solution)/shard_map/all_to_all | solution.py:413
  35.5 0.0 collective-permute-start
  35.6 1.2 collective-permute-start.3
  36.8 1.5 collective-permute-start.2
  38.2 0.0 collective-permute-start.1
  38.2 15.0 %fusion.grad_ref = f32[3,256,2048]{2,1,0:T(8,128)} fusion(bf16[3,3072,256]{2,1,0:T(8,128)(2,1)S(1)} %copy-done.9, bf16[3072,2048]{1,0:T(8,128)(2,1)} %input_hbm.1), kind=kOutput, calls=%fused_computation | convolution fusion | flops 9663676416 | bytes 23592960 | tf_op jit(solution)/shard_map/td,rtw->rwd/dot_general | solution.py:424
  53.2 0.0 collective-permute-done.far_ref
  53.2 5.7 %low_parts.1 = f32[16,48,256]{2,1,0:T(8,128)} custom-call(f32[3,256,2048]{2,1,0:T(8,128)} %fusion.grad_ref, bf16[16,400,128]{2,1,0:T(8,128)(2,1)S(1)} %all_to_all.20.near_ref.ends_hbm, bf16[16,400,128]{2,1,0:T(8,128)(2,1)S(1)} %collective-permute-done.far_ref), custom_call_target="tpu_custom_call" | custom-call | flops 1610612736 | bytes 11000000 | tf_op jit(solution)/shard_map/low_parts/pallas_call | solution.py:185
  58.9 5.7 %all-to-all-start.1 = ((f32[16,48,256]{2,1,0:T(8,128)}), f32[16,48,256]{2,1,0:T(8,128)}, u32[]{:S(2)}, u32[]{:S(2)}) async-start(f32[16,48,256]{2,1,0:T(8,128)} %low_parts.1), calls=%async_computation.1 | async-start | bytes 1572864 | tf_op jit(solution)/shard_map/all_to_all | solution.py:426
  64.6 3.1 %collective-permute-start.10 = (f32[1,3,64,256]{3,2,1,0:T(8,128)S(1)}, f32[1,3,64,256]{3,2,1,0:T(8,128)S(1)}, u32[]{:S(2)}, u32[]{:S(2)}) collective-permute-start(f32[1,3,64,256]{3,2,1,0:T(8,128)S(1)} %get-tuple-element.33), channel_id=1, source_target_pairs={{0,24},{8,0},{16,8},{24,16},{1,25},{9,1},{17,9},{25,17},{2,26},{10... | collective-permute-start | bytes 589832 | tf_op jit(solution)/shard_map/ppermute | solution.py:390
  67.7 0.9 collective-permute-start.9
  68.6 0.0 collective-permute-done.3
  68.6 0.9 collective-permute-start.8
  69.4 0.0 collective-permute-done.2
  69.4 1.0 pad_maximum_fusion.refs_0_
  70.4 2.4 %collective-permute-start.5 = (f32[4,3,64,256]{3,2,1,0:T(8,128)}, f32[4,3,64,256]{3,2,1,0:T(8,128)}, u32[]{:S(2)}, u32[]{:S(2)}) collective-permute-start(f32[4,3,64,256]{3,2,1,0:T(8,128)} %pad_maximum_fusion.refs_0_), channel_id=1, source_target_pairs={{0,24},{8,0},{16,8},{24,16},{1,25},{9,1},{17,9},{25,17},{2,26},{10... | collective-permute-start | bytes 2359304 | tf_op jit(solution)/shard_map/ppermute | solution.py:390
  72.8 8.1 %collective-permute-done.10 = f32[1,3,64,256]{3,2,1,0:T(8,128)S(1)} collective-permute-done((f32[1,3,64,256]{3,2,1,0:T(8,128)S(1)}, f32[1,3,64,256]{3,2,1,0:T(8,128)S(1)}, u32[]{:S(2)}, u32[]{:S(2)}) %collective-permute-start.10) | collective-permute-done | bytes 196640 | tf_op jit(solution)/shard_map/ppermute | solution.py:390
  80.9 1.5 %collective-permute-done.9 = f32[1,3,64,256]{3,2,1,0:T(8,128)S(1)} collective-permute-done((f32[1,3,64,256]{3,2,1,0:T(8,128)S(1)}, f32[1,3,64,256]{3,2,1,0:T(8,128)S(1)}, u32[]{:S(2)}, u32[]{:S(2)}) %collective-permute-start.9) | collective-permute-done | bytes 196640 | tf_op jit(solution)/shard_map/ppermute | solution.py:390
  82.4 2.7 %collective-permute-done.8 = f32[1,3,64,256]{3,2,1,0:T(8,128)S(1)} collective-permute-done((f32[1,3,64,256]{3,2,1,0:T(8,128)S(1)}, f32[1,3,64,256]{3,2,1,0:T(8,128)S(1)}, u32[]{:S(2)}, u32[]{:S(2)}) %collective-permute-start.8) | collective-permute-done | bytes 196640 | tf_op jit(solution)/shard_map/ppermute | solution.py:390
  85.1 0.9 pad_maximum_fusion.1.refs_5_
  86.0 2.7 %collective-permute-start.12 = (f32[4,3,64,256]{3,2,1,0:T(8,128)}, f32[4,3,64,256]{3,2,1,0:T(8,128)}, u32[]{:S(2)}, u32[]{:S(2)}) collective-permute-start(f32[4,3,64,256]{3,2,1,0:T(8,128)} %pad_maximum_fusion.1.refs_5_), channel_id=1, source_target_pairs={{0,96},{32,0},{64,32},{96,64},{1,97},{33,1},{65,33},{97,65},{2,98}... | collective-permute-start | bytes 2359304 | tf_op jit(solution)/shard_map/ppermute | solution.py:390
  88.7 2.5 %gate_columns.1.gate_ref = f32[16,256]{1,0:T(8,128)S(1)} custom-call(s32[5]{0:T(128)S(1)} %stack.23.place_ref, f32[16,3072]{1,0:T(8,128)} %log_hbm.1, f32[16,3072]{1,0:T(8,128)} %cot_hbm.1, bf16[16,400,128]{2,1,0:T(8,128)(2,1)} %copy-done.2, bf16[3072,2048]{1,0:T(8,128)(2,1)} %input_hbm.1), custom_call_target="tpu_custom_call" | custom-call | flops 4000000000 | bytes 4000000 | tf_op jit(solution)/shard_map/gate_columns/pallas_call | solution.py:145
  91.3 0.0 copy-start.3
  91.3 2.4 %summed.1 = f32[16,64,256]{2,1,0:T(8,128)} custom-call(f32[16,48,256]{2,1,0:T(8,128)} %all-to-all-done.1.arrived_ref, f32[16,256]{1,0:T(8,128)S(1)} %gate_columns.1.gate_ref), custom_call_target="tpu_custom_call" | custom-call | flops 1000000 | bytes 2000000 | tf_op jit(solution)/shard_map/summed/pallas_call | solution.py:211
  93.7 6.8 %all-to-all-start.2 = ((f32[16,64,256]{2,1,0:T(8,128)}), f32[16,64,256]{2,1,0:T(8,128)}, u32[]{:S(2)}, u32[]{:S(2)}) async-start(f32[16,64,256]{2,1,0:T(8,128)} %summed.1), calls=%async_computation.2 | async-start | bytes 2097152 | tf_op jit(solution)/shard_map/all_to_all | solution.py:428
  100.6 0.3 collective-permute-done.5.refs_2_
  100.9 1.8 %slice.26 = f32[2,3,64,256]{3,2,1,0:T(8,128)} slice(f32[4,3,64,256]{3,2,1,0:T(8,128)} %collective-permute-done.5.refs_2_), slice={[2:4], [0:3], [0:64], [0:256]} | slice | bytes 786432 | tf_op jit(solution)/shard_map/slice | solution.py:422
  102.7 2.8 %collective-permute-start.7 = (f32[2,3,64,256]{3,2,1,0:T(8,128)}, f32[2,3,64,256]{3,2,1,0:T(8,128)}, u32[]{:S(2)}, u32[]{:S(2)}) collective-permute-start(f32[2,3,64,256]{3,2,1,0:T(8,128)} %slice.26), channel_id=1, source_target_pairs={{0,24},{8,0},{16,8},{24,16},{1,25},{9,1},{17,9},{25,17},{2,26},{10... | collective-permute-start | bytes 1179656 | tf_op jit(solution)/shard_map/ppermute | solution.py:390
  105.5 1.8 %slice.25 = f32[2,3,64,256]{3,2,1,0:T(8,128)} slice(f32[4,3,64,256]{3,2,1,0:T(8,128)} %collective-permute-done.4.refs_1_), slice={[0:2], [0:3], [0:64], [0:256]} | slice | bytes 786432 | tf_op jit(solution)/shard_map/slice | solution.py:421
  107.3 8.6 %collective-permute-done.12.refs_7_ = f32[4,3,64,256]{3,2,1,0:T(8,128)} collective-permute-done((f32[4,3,64,256]{3,2,1,0:T(8,128)}, f32[4,3,64,256]{3,2,1,0:T(8,128)}, u32[]{:S(2)}, u32[]{:S(2)}) %collective-permute-start.12) | collective-permute-done | bytes 786464 | tf_op jit(solution)/shard_map/ppermute | solution.py:390
  115.9 1.8 %slice.29 = f32[2,3,64,256]{3,2,1,0:T(8,128)} slice(f32[4,3,64,256]{3,2,1,0:T(8,128)} %collective-permute-done.12.refs_7_), slice={[2:4], [0:3], [0:64], [0:256]} | slice | bytes 786432 | tf_op jit(solution)/shard_map/slice | solution.py:422
  117.7 3.7 %collective-permute-start.14 = (f32[2,3,64,256]{3,2,1,0:T(8,128)}, f32[2,3,64,256]{3,2,1,0:T(8,128)}, u32[]{:S(2)}, u32[]{:S(2)}) collective-permute-start(f32[2,3,64,256]{3,2,1,0:T(8,128)} %slice.29), channel_id=1, source_target_pairs={{0,96},{32,0},{64,32},{96,64},{1,97},{33,1},{65,33},{97,65},{2,98}... | collective-permute-start | bytes 1179656 | tf_op jit(solution)/shard_map/ppermute | solution.py:390
  121.4 1.8 %slice.28 = f32[2,3,64,256]{3,2,1,0:T(8,128)} slice(f32[4,3,64,256]{3,2,1,0:T(8,128)} %collective-permute-done.11.refs_6_), slice={[0:2], [0:3], [0:64], [0:256]} | slice | bytes 786432 | tf_op jit(solution)/shard_map/slice | solution.py:421
  123.2 4.7 %moments.1 = (f32[3,256,256]{2,1,0:T(8,128)}, f32[3,256,256]{2,1,0:T(8,128)}, bf16[3,256,256]{2,1,0:T(8,128)(2,1)S(1)}, bf16[3,256,256]{2,1,0:T(8,128)(2,1)S(1)}, f32[8,24,256]{2,1,0:T(8,128)}) custom-call(s32[5]{0:T(128)S(1)} %stack.23.place_ref, f32[16,64,256]{2,1,0:T(8,128)} %all-to-all-done.2.sums_ref, f32[3,256,256]{2,1,0:T(8,128)} %first_hbm.1, ...), custom_call_target="tpu_custom_call" | custom-call | flops 10000000 | bytes 6000000 | tf_op jit(solution)/shard_map/moments/pallas_call | solution.py:262
  127.9 0.0 copy-start.4
  127.9 0.7 copy-done.4
  128.7 0.7 copy-done.6
  129.4 4.5 %all-to-all-start.3 = ((f32[8,24,256]{2,1,0:T(8,128)}), f32[8,24,256]{2,1,0:T(8,128)S(1)}, u32[]{:S(2)}, u32[]{:S(2)}) async-start(f32[8,24,256]{2,1,0:T(8,128)} %get-tuple-element.21), calls=%async_computation.3 | async-start | bytes 393216 | tf_op jit(solution)/shard_map/all_to_all | solution.py:433
  133.9 0.0 copy-start.5
  133.9 1.0 copy-done.5
  134.9 1.0 copy-done.7
  135.9 4.0 %products.1.product_ref = f32[3,2048,256]{2,1,0:T(8,128)S(1)} custom-call(s32[5]{0:T(128)S(1)} %stack.23.place_ref, bf16[16,400,128]{2,1,0:T(8,128)(2,1)S(1)} %copy-done.3, bf16[16,400,128]{2,1,0:T(8,128)(2,1)S(1)} %collective-permute-done.far_ref, bf16[3,256,256]{2,1,0:T(8,128)(2,1)S(1)} %copy-done.5, bf16[3,256,256]{2,1,0:T(8,128)(2,1)S(1)} %copy-done.7), custom_call_target="tpu_custom_call" | custom-call | flops 1610612736 | bytes 10000000 | tf_op jit(solution)/shard_map/products/pallas_call | solution.py:303
  139.9 2.6 %copy-done = f32[3,2048,256]{2,1,0:T(8,128)} copy-done((f32[3,2048,256]{2,1,0:T(8,128)}, f32[3,2048,256]{2,1,0:T(8,128)S(1)}, u32[]{:S(2)}) %copy-start) | copy-done | bytes 6291480
  142.6 2.8 %copy-done.1 = f32[3,2048,256]{2,1,0:T(8,128)S(1)} copy-done((f32[3,2048,256]{2,1,0:T(8,128)S(1)}, f32[3,2048,256]{2,1,0:T(8,128)}, u32[]{:S(2)}) %copy-start.1) | copy-done | bytes 6291480
  145.3 6.3 %finals.1 = (f32[3,128,256]{2,1,0:T(8,128)}, f32[3,128,256]{2,1,0:T(8,128)}, bf16[3,2048,256]{2,1,0:T(8,128)(2,1)}, f32[16,2048]{1,0:T(8,128)}, bf16[16,2048]{1,...) custom-call(s32[5]{0:T(128)S(1)} %stack.23.place_ref, f32[8,24,256]{2,1,0:T(8,128)S(1)} %all-to-all-done.3.shared_ref, ...), custom_call_target="tpu_custom_call" | custom-call | flops 10000000 | bytes 16000000 | tf_op jit(solution)/shard_map/finals/pallas_call | solution.py:376
  (25 shorter events, 0.1 us)
Async XLA Ops:
  0.6 34.9 %copy-start.8 = (f32[3,128,256]{2,1,0:T(8,128)S(1)}, f32[3,128,256]{2,1,0:T(8,128)}, u32[]{:S(2)}) copy-start(f32[3,128,256]{2,1,0:T(8,128)} %refs_10_.1) | copy-start | bytes 1179652
  0.7 37.5 %copy-start.9 = (bf16[3,3072,256]{2,1,0:T(8,128)(2,1)S(1)}, bf16[3,3072,256]{2,1,0:T(8,128)(2,1)}, u32[]{:S(2)}) copy-start(bf16[3,3072,256]{2,1,0:T(8,128)(2,1)} %param.12) | copy-start | bytes 14155780
  35.5 17.7 %copy-start.2 = (bf16[16,400,128]{2,1,0:T(8,128)(2,1)}, bf16[16,400,128]{2,1,0:T(8,128)(2,1)S(1)}, u32[]{:S(2)}) copy-start(bf16[16,400,128]{2,1,0:T(8,128)(2,1)S(1)} %all_to_all.20.near_ref.ends_hbm) | copy-start | bytes 4915204
  35.5 17.7 %collective-permute-start = (bf16[16,400,128]{2,1,0:T(8,128)(2,1)S(1)}, bf16[16,400,128]{2,1,0:T(8,128)(2,1)S(1)}, u32[]{:S(2)}, u32[]{:S(2)}) collective-permute-start(bf16[16,400,128]{2,1,0:T(8,128)(2,1)S(1)} %all_to_all.20.near_ref.ends_hbm), channel_id=1, source_target_pairs={{0,1},{1,0},{2,3},{3,2},{4,5},{5,4},{6,7},{7,6},{8,9},{9,8},{10,11... | collective-permute-start | bytes 4915208 | tf_op jit(solution)/shard_map/ppermute | solution.py:414
  35.6 33.0 %collective-permute-start.3 = (f32[1,3,64,256]{3,2,1,0:T(8,128)S(1)}, f32[1,3,64,256]{3,2,1,0:T(8,128)S(1)}, u32[]{:S(2)}, u32[]{:S(2)}) collective-permute-start(f32[1,3,64,256]{3,2,1,0:T(8,128)S(1)} %get-tuple-element.34), channel_id=1, source_target_pairs={{0,96},{32,0},{64,32},{96,64},{1,97},{33,1},{65,33},{97,65},{2,98}... | collective-permute-start | bytes 589832 | tf_op jit(solution)/shard_map/ppermute | solution.py:390
  36.8 32.7 %collective-permute-start.2 = (f32[1,3,64,256]{3,2,1,0:T(8,128)S(1)}, f32[1,3,64,256]{3,2,1,0:T(8,128)S(1)}, u32[]{:S(2)}, u32[]{:S(2)}) collective-permute-start(f32[1,3,64,256]{3,2,1,0:T(8,128)S(1)} %get-tuple-element.34), channel_id=1, source_target_pairs={{0,64},{32,96},{64,0},{96,32},{1,65},{33,97},{65,1},{97,33},{2,66}... | collective-permute-start | bytes 589832 | tf_op jit(solution)/shard_map/ppermute | solution.py:390
  38.2 31.2 %collective-permute-start.1 = (f32[1,3,64,256]{3,2,1,0:T(8,128)S(1)}, f32[1,3,64,256]{3,2,1,0:T(8,128)S(1)}, u32[]{:S(2)}, u32[]{:S(2)}) collective-permute-start(f32[1,3,64,256]{3,2,1,0:T(8,128)S(1)} %get-tuple-element.34), channel_id=1, source_target_pairs={{0,32},{32,64},{64,96},{96,0},{1,33},{33,65},{65,97},{97,1},{2,34}... | collective-permute-start | bytes 589832 | tf_op jit(solution)/shard_map/ppermute | solution.py:390
  58.9 32.4 %all-to-all-start.1 = ((f32[16,48,256]{2,1,0:T(8,128)}), f32[16,48,256]{2,1,0:T(8,128)}, u32[]{:S(2)}, u32[]{:S(2)}) async-start(f32[16,48,256]{2,1,0:T(8,128)} %low_parts.1), calls=%async_computation.1 | async-start | bytes 1572864 | tf_op jit(solution)/shard_map/all_to_all | solution.py:426
  64.6 16.3 %collective-permute-start.10 = (f32[1,3,64,256]{3,2,1,0:T(8,128)S(1)}, f32[1,3,64,256]{3,2,1,0:T(8,128)S(1)}, u32[]{:S(2)}, u32[]{:S(2)}) collective-permute-start(f32[1,3,64,256]{3,2,1,0:T(8,128)S(1)} %get-tuple-element.33), channel_id=1, source_target_pairs={{0,24},{8,0},{16,8},{24,16},{1,25},{9,1},{17,9},{25,17},{2,26},{10... | collective-permute-start | bytes 589832 | tf_op jit(solution)/shard_map/ppermute | solution.py:390
  67.7 14.7 %collective-permute-start.9 = (f32[1,3,64,256]{3,2,1,0:T(8,128)S(1)}, f32[1,3,64,256]{3,2,1,0:T(8,128)S(1)}, u32[]{:S(2)}, u32[]{:S(2)}) collective-permute-start(f32[1,3,64,256]{3,2,1,0:T(8,128)S(1)} %get-tuple-element.33), channel_id=1, source_target_pairs={{0,16},{8,24},{16,0},{24,8},{1,17},{9,25},{17,1},{25,9},{2,18},{10... | collective-permute-start | bytes 589832 | tf_op jit(solution)/shard_map/ppermute | solution.py:390
  68.6 16.5 %collective-permute-start.8 = (f32[1,3,64,256]{3,2,1,0:T(8,128)S(1)}, f32[1,3,64,256]{3,2,1,0:T(8,128)S(1)}, u32[]{:S(2)}, u32[]{:S(2)}) collective-permute-start(f32[1,3,64,256]{3,2,1,0:T(8,128)S(1)} %get-tuple-element.33), channel_id=1, source_target_pairs={{0,8},{8,16},{16,24},{24,0},{1,9},{9,17},{17,25},{25,1},{2,10},{10... | collective-permute-start | bytes 589832 | tf_op jit(solution)/shard_map/ppermute | solution.py:390
  70.4 30.4 %collective-permute-start.5 = (f32[4,3,64,256]{3,2,1,0:T(8,128)}, f32[4,3,64,256]{3,2,1,0:T(8,128)}, u32[]{:S(2)}, u32[]{:S(2)}) collective-permute-start(f32[4,3,64,256]{3,2,1,0:T(8,128)} %pad_maximum_fusion.refs_0_), channel_id=1, source_target_pairs={{0,24},{8,0},{16,8},{24,16},{1,25},{9,1},{17,9},{25,17},{2,26},{10... | collective-permute-start | bytes 2359304 | tf_op jit(solution)/shard_map/ppermute | solution.py:390
  72.8 32.7 %collective-permute-start.4 = (f32[4,3,64,256]{3,2,1,0:T(8,128)}, f32[4,3,64,256]{3,2,1,0:T(8,128)}, u32[]{:S(2)}, u32[]{:S(2)}) collective-permute-start(f32[4,3,64,256]{3,2,1,0:T(8,128)} %pad_maximum_fusion.refs_0_), channel_id=1, source_target_pairs={{0,8},{8,16},{16,24},{24,0},{1,9},{9,17},{17,25},{25,1},{2,10},{10... | collective-permute-start | bytes 2359304 | tf_op jit(solution)/shard_map/ppermute | solution.py:390
  86.0 29.9 %collective-permute-start.12 = (f32[4,3,64,256]{3,2,1,0:T(8,128)}, f32[4,3,64,256]{3,2,1,0:T(8,128)}, u32[]{:S(2)}, u32[]{:S(2)}) collective-permute-start(f32[4,3,64,256]{3,2,1,0:T(8,128)} %pad_maximum_fusion.1.refs_5_), channel_id=1, source_target_pairs={{0,96},{32,0},{64,32},{96,64},{1,97},{33,1},{65,33},{97,65},{2,98}... | collective-permute-start | bytes 2359304 | tf_op jit(solution)/shard_map/ppermute | solution.py:390
  88.7 32.6 %collective-permute-start.11 = (f32[4,3,64,256]{3,2,1,0:T(8,128)}, f32[4,3,64,256]{3,2,1,0:T(8,128)}, u32[]{:S(2)}, u32[]{:S(2)}) collective-permute-start(f32[4,3,64,256]{3,2,1,0:T(8,128)} %pad_maximum_fusion.1.refs_5_), channel_id=1, source_target_pairs={{0,32},{32,64},{64,96},{96,0},{1,33},{33,65},{65,97},{97,1},{2,34}... | collective-permute-start | bytes 2359304 | tf_op jit(solution)/shard_map/ppermute | solution.py:390
  91.3 42.6 %copy-start.3 = (bf16[16,400,128]{2,1,0:T(8,128)(2,1)S(1)}, bf16[16,400,128]{2,1,0:T(8,128)(2,1)}, u32[]{:S(2)}) copy-start(bf16[16,400,128]{2,1,0:T(8,128)(2,1)} %copy-done.2) | copy-start | bytes 4915204
  93.7 29.4 %all-to-all-start.2 = ((f32[16,64,256]{2,1,0:T(8,128)}), f32[16,64,256]{2,1,0:T(8,128)}, u32[]{:S(2)}, u32[]{:S(2)}) async-start(f32[16,64,256]{2,1,0:T(8,128)} %summed.1), calls=%async_computation.2 | async-start | bytes 2097152 | tf_op jit(solution)/shard_map/all_to_all | solution.py:428
  102.7 39.8 %collective-permute-start.7 = (f32[2,3,64,256]{3,2,1,0:T(8,128)}, f32[2,3,64,256]{3,2,1,0:T(8,128)}, u32[]{:S(2)}, u32[]{:S(2)}) collective-permute-start(f32[2,3,64,256]{3,2,1,0:T(8,128)} %slice.26), channel_id=1, source_target_pairs={{0,24},{8,0},{16,8},{24,16},{1,25},{9,1},{17,9},{25,17},{2,26},{10... | collective-permute-start | bytes 1179656 | tf_op jit(solution)/shard_map/ppermute | solution.py:390
  107.3 35.2 %collective-permute-start.6 = (f32[2,3,64,256]{3,2,1,0:T(8,128)}, f32[2,3,64,256]{3,2,1,0:T(8,128)}, u32[]{:S(2)}, u32[]{:S(2)}) collective-permute-start(f32[2,3,64,256]{3,2,1,0:T(8,128)} %slice.25), channel_id=1, source_target_pairs={{0,8},{8,16},{16,24},{24,0},{1,9},{9,17},{17,25},{25,1},{2,10},{10... | collective-permute-start | bytes 1179656 | tf_op jit(solution)/shard_map/ppermute | solution.py:390
  117.7 24.8 %collective-permute-start.14 = (f32[2,3,64,256]{3,2,1,0:T(8,128)}, f32[2,3,64,256]{3,2,1,0:T(8,128)}, u32[]{:S(2)}, u32[]{:S(2)}) collective-permute-start(f32[2,3,64,256]{3,2,1,0:T(8,128)} %slice.29), channel_id=1, source_target_pairs={{0,96},{32,0},{64,32},{96,64},{1,97},{33,1},{65,33},{97,65},{2,98}... | collective-permute-start | bytes 1179656 | tf_op jit(solution)/shard_map/ppermute | solution.py:390
  123.2 19.4 %collective-permute-start.13 = (f32[2,3,64,256]{3,2,1,0:T(8,128)}, f32[2,3,64,256]{3,2,1,0:T(8,128)}, u32[]{:S(2)}, u32[]{:S(2)}) collective-permute-start(f32[2,3,64,256]{3,2,1,0:T(8,128)} %slice.28), channel_id=1, source_target_pairs={{0,32},{32,64},{64,96},{96,0},{1,33},{33,65},{65,97},{97,1},{2,34}... | collective-permute-start | bytes 1179656 | tf_op jit(solution)/shard_map/ppermute | solution.py:390
  127.9 0.7 copy-start.4
  128.7 0.7 copy-start.6
  129.4 13.1 %all-to-all-start.3 = ((f32[8,24,256]{2,1,0:T(8,128)}), f32[8,24,256]{2,1,0:T(8,128)S(1)}, u32[]{:S(2)}, u32[]{:S(2)}) async-start(f32[8,24,256]{2,1,0:T(8,128)} %get-tuple-element.21), calls=%async_computation.3 | async-start | bytes 393216 | tf_op jit(solution)/shard_map/all_to_all | solution.py:433
  133.9 1.0 copy-start.5
  134.9 1.0 copy-start.7
  139.9 2.6 %copy-start = (f32[3,2048,256]{2,1,0:T(8,128)}, f32[3,2048,256]{2,1,0:T(8,128)S(1)}, u32[]{:S(2)}) copy-start(f32[3,2048,256]{2,1,0:T(8,128)S(1)} %products.1.product_ref) | copy-start | bytes 18874372
  142.5 2.8 %copy-start.1 = (f32[3,2048,256]{2,1,0:T(8,128)S(1)}, f32[3,2048,256]{2,1,0:T(8,128)}, u32[]{:S(2)}) copy-start(f32[3,2048,256]{2,1,0:T(8,128)} %copy-done) | copy-start | bytes 18874372

commit v4 on v3

--- a/solution.py
+++ b/solution.py
@@ -160,7 +160,7 @@
     )(place, *held(pltpu.HBM, log_cache, cache_cot, ends, saved_input))
 
 
-def low_kernel(grad_ref, near_ref, far_ref, out_ref):
+def low_kernel(grad_ref, near_ref, far_ref, gate_ref, out_ref):
     role = pl.program_id(0)
     peers, rows, half = near_ref.shape
     sides = [ref[...].reshape(peers * rows, half) for ref in (near_ref, far_ref)]
@@ -175,12 +175,18 @@
         start = pl.multiple_of(side * 3 * lines + role * lines, lines)
         out_ref[:, pl.ds(start, lines), :] = part
 
-
-def low_parts(grad, near, far):
+    @pl.when(role == 0)
+    def _():
+        out_ref[:, 6 * lines :, :] = jnp.zeros_like(out_ref[:, 6 * lines :, :])
+        for head in range(gate_ref.shape[0]):
+            out_ref[head, 6 * lines : 6 * lines + 1, :] = gate_ref[head : head + 1, :]
+
+
+def low_parts(grad, near, far, gate):
     roles, width, depth = grad.shape
     peers, _, half = near.shape
     rows = depth // peers
-    lines = 2 * roles * half // peers
+    lines = 2 * roles * half // peers + 8
     factor_spec = pl.BlockSpec((peers, rows, half), lambda r: (0, r, 0))
     return pl.pallas_call(
         low_kernel,
@@ -190,90 +196,105 @@
             pl.BlockSpec((1, width, depth), lambda r: (r, 0, 0)),
             factor_spec,
             factor_spec,
+            pl.BlockSpec(gate.shape, lambda r: (0, 0)),
         ],
         out_specs=pl.BlockSpec((peers, lines, width), lambda r: (0, 0, 0)),
         compiler_params=room(20),
         cost_estimate=cost(4 * roles * width * depth * 2 * half, 11 * 10**6),
         name="low_parts",
-    )(*held(pltpu.HBM, grad), near, far)
-
-
-def sum_kernel(arrived_ref, gate_ref, out_ref, block, sems):
-    peers, lines, _ = arrived_ref.shape
-    block[:lines, :] = jnp.sum(arrived_ref[...], axis=0)
-    block[lines:, :] = gate_ref[...]
+    )(*held(pltpu.HBM, grad, near, far), gate)
+
+
+def sum_kernel(arrived_ref, out_ref, block, sems):
+    block[...] = jnp.sum(arrived_ref[...], axis=0)
+    peers = out_ref.shape[0]
     finished(started([(block, out_ref.at[peer]) for peer in range(peers)], sems))
 
 
-def summed(arrived, gate):
-    peers, lines, width = arrived.shape
-    lines = lines + gate.shape[0]
+def summed(arrived):
     return pl.pallas_call(
         sum_kernel,
-        out_shape=pltpu.HBM((peers, lines, width), jnp.float32),
-        in_specs=[VMEM, VMEM],
+        out_shape=pltpu.HBM(arrived.shape, jnp.float32),
+        in_specs=[VMEM],
         out_specs=HBM,
         scratch_shapes=[
-            pltpu.VMEM((lines, width), jnp.float32),
-            pltpu.SemaphoreType.DMA((peers,)),
+            pltpu.VMEM(arrived.shape[1:], jnp.float32),
+            pltpu.SemaphoreType.DMA((arrived.shape[0],)),
         ],
         compiler_params=room(8),
         cost_estimate=cost(10**6, 2 * 10**6),
         name="summed",
-    )(arrived, gate)
+    )(arrived)
 
 
 def moment_kernel(
-    place_ref, sums_ref, first_hbm, second_hbm, first_new_hbm, second_new_hbm, upper_ref,
-    lower_ref, shared_hbm, first_ref, second_ref, first_new_ref, second_new_ref, message, sems,
+    place_ref, sums_ref, first_hbm, second_hbm, first_new_hbm, second_new_hbm, upper_hbm,
+    lower_hbm, shared_hbm, first_ref, second_ref, upper_ref, lower_ref, message, read_sems,
+    write_sems,
 ):
     core = place_ref[2]
-    finished(started([(first_hbm, first_ref), (second_hbm, second_ref)], sems))
     roles, rank, width = first_ref.shape
-    peers, _, _ = sums_ref.shape
+    peers = sums_ref.shape[0]
     half = rank // 2
     block = half // peers
+    reads = [
+        started(
+            [(first_hbm.at[role], first_ref.at[role]), (second_hbm.at[role], second_ref.at[role])],
+            read_sems.at[role],
+        )
+        for role in range(roles)
+    ]
     squares = jnp.zeros((half, width), jnp.float32)
-    for side in range(2):
-        for role in range(roles):
+    writes = []
+    for role in range(roles):
+        finished(reads[role])
+        for side in range(2):
             at = (side * roles + role) * block
             low = sums_ref[:, at : at + block, :].reshape(half, width)
             at = pl.ds(pl.multiple_of((core ^ side) * half, half), half)
             first_new = BETA_ONE * first_ref[role, at] + (1.0 - BETA_ONE) * low
             second_new = BETA_TWO * second_ref[role, at] + (1.0 - BETA_TWO) * low * low
             direction = first_new / jnp.sqrt(second_new)
-            first_new_ref[role, at] = first_new
-            second_new_ref[role, at] = second_new
+            first_ref[role, at] = first_new
+            second_ref[role, at] = second_new
             squares = squares + direction * direction
-            upper_ref[role, at], lower_ref[role, at] = halves(direction)
+            upper, lower = halves(direction)
+            upper_ref[role, side * half : (side + 1) * half] = upper
+            lower_ref[role, side * half : (side + 1) * half] = lower
+        made = [first_ref, second_ref, upper_ref, lower_ref]
+        kept = [first_new_hbm, second_new_hbm, upper_hbm, lower_hbm]
+        pairs = [(a.at[role], b.at[role]) for a, b in zip(made, kept)]
+        writes += started(pairs, write_sems.at[pl.ds(role * 4, 4)])
     squares = jnp.sum(squares, axis=(0, 1), keepdims=True)
-    gate = jnp.sum(sums_ref[:, 2 * roles * block :, :], axis=0)
-    heads = gate.shape[0]
-    message[:heads, :] = gate
+    heads = peers
+    for head in range(heads):
+        message[head : head + 1, :] = sums_ref[head, 6 * block : 6 * block + 1, :]
     message[heads:, :] = jnp.broadcast_to(squares, (8, width))
-    writes = [(message, shared_hbm.at[copy]) for copy in range(shared_hbm.shape[0])]
-    writes += [(first_new_ref, first_new_hbm), (second_new_ref, second_new_hbm)]
-    finished(started(writes, sems))
+    copies = shared_hbm.shape[0]
+    pairs = [(message, shared_hbm.at[copy]) for copy in range(copies)]
+    finished(writes + started(pairs, write_sems.at[pl.ds(roles * 4, copies)]))
 
 
 def moments(place, sums, first_moment, second_moment, copies):
     shape = first_moment.shape
-    heads = sums.shape[1] - 2 * shape[0] * (shape[1] // 2 // sums.shape[0])
+    heads = sums.shape[0]
     return pl.pallas_call(
         moment_kernel,
         out_shape=[
             pltpu.HBM(shape, jnp.float32),
             pltpu.HBM(shape, jnp.float32),
-            pltpu.VMEM(shape, jnp.bfloat16),
-            pltpu.VMEM(shape, jnp.bfloat16),
+            pltpu.HBM(shape, jnp.bfloat16),
+            pltpu.HBM(shape, jnp.bfloat16),
             pltpu.HBM((copies, heads + 8, shape[2]), jnp.float32),
         ],
         in_specs=[SMEM, VMEM, HBM, HBM],
-        out_specs=[HBM, HBM, VMEM, VMEM, HBM],
-        scratch_shapes=[pltpu.VMEM(shape, jnp.float32)] * 4
+        out_specs=[HBM] * 5,
+        scratch_shapes=[pltpu.VMEM(shape, jnp.float32)] * 2
+        + [pltpu.VMEM(shape, jnp.bfloat16)] * 2
         + [
             pltpu.VMEM((heads + 8, shape[2]), jnp.float32),
-            pltpu.SemaphoreType.DMA((copies + 2,)),
+            pltpu.SemaphoreType.DMA((shape[0], 2)),
+            pltpu.SemaphoreType.DMA((shape[0] * 4 + copies,)),
         ],
         compiler_params=room(12),
         cost_estimate=cost(10**7, 6 * 10**6),
@@ -281,72 +302,81 @@
     )(place, sums, *held(pltpu.HBM, first_moment, second_moment))
 
 
-def product_kernel(place_ref, near_ref, far_ref, upper_ref, lower_ref, out_ref):
-    roles, depth, _ = out_ref.shape
-    peers, _, half = near_ref.shape
-    rows = depth // peers
-    core = place_ref[2]
+def product_kernel(
+    near_hbm, far_hbm, upper_hbm, lower_hbm, out_hbm, factor_ref, direction_ref, product_ref,
+    read_sems, write_sems,
+):
+    roles, peers, rows, rank = factor_ref.shape
+    half = rank // 2
+
+    def operands(role):
+        lines = pl.ds(role * rows, rows)
+        pairs = [
+            (ref.at[:, lines, :], factor_ref.at[role, :, :, pl.ds(side * half, half)])
+            for side, ref in enumerate((near_hbm, far_hbm))
+        ]
+        directions = enumerate((upper_hbm, lower_hbm))
+        pairs += [(ref.at[role], direction_ref.at[role, n]) for n, ref in directions]
+        return started(pairs, read_sems.at[role])
+
+    reads = [operands(role) for role in range(roles)]
+    writes = []
     for role in range(roles):
-        total = None
-        for side, ref in enumerate((near_ref, far_ref)):
-            pieces = ref[:, role * rows : (role + 1) * rows, :].reshape(depth, half)
-            at = pl.ds(pl.multiple_of((core ^ side) * half, half), half)
-            for part in (upper_ref, lower_ref):
-                term = jnp.dot(pieces, part[role, at], preferred_element_type=jnp.float32)
-                total = term if total is None else total + term
-        out_ref[role] = total
-
-
-def products(place, near, far, upper, lower, rows):
+        finished(reads[role])
+        factor = factor_ref[role].reshape(peers * rows, rank)
+        product_ref[role] = jnp.dot(
+            factor, direction_ref[role, 0], preferred_element_type=jnp.float32
+        ) + jnp.dot(factor, direction_ref[role, 1], preferred_element_type=jnp.float32)
+        pairs = [(product_ref.at[role], out_hbm.at[role])]
+        writes += started(pairs, write_sems.at[pl.ds(role, 1)])
+    finished(writes)
+
+
+def products(near, far, upper, lower, rows):
     roles, rank, width = upper.shape
-    depth = near.shape[0] * rows
+    peers = near.shape[0]
+    shape = (roles, peers * rows, width)
     return pl.pallas_call(
         product_kernel,
-        out_shape=pltpu.VMEM((roles, depth, width), jnp.float32),
-        in_specs=[SMEM, VMEM, VMEM, VMEM, VMEM],
-        out_specs=VMEM,
+        out_shape=pltpu.HBM(shape, jnp.float32),
+        in_specs=[HBM] * 4,
+        out_specs=HBM,
+        scratch_shapes=[
+            pltpu.VMEM((roles, peers, rows, rank), jnp.bfloat16),
+            pltpu.VMEM((roles, 2, rank, width), jnp.bfloat16),
+            pltpu.VMEM(shape, jnp.float32),
+            pltpu.SemaphoreType.DMA((roles, 4)),
+            pltpu.SemaphoreType.DMA((roles,)),
+        ],
         compiler_params=room(20),
-        cost_estimate=cost(4 * roles * depth * rank * width, 10**7),
+        cost_estimate=cost(4 * roles * peers * rows * rank * width, 10**7),
         name="products",
-    )(place, near, far, *held(pltpu.VMEM, upper, lower))
-
-
-def final_kernel(entries, place_ref, shared_ref, product_ref, *refs):
-    pieces, refs = refs[:10], refs[10:]
-    inputs, outputs, refs = refs[:4], refs[4:11], refs[11:]
-    kept, made, read_sems, write_sems = refs[:4], refs[4:11], refs[11], refs[12]
-    master_ref, gate_master_ref, gate_first_ref, gate_second_ref = kept
+    )(*held(pltpu.HBM, near, far, upper, lower))
+
+
+def final_kernel(entries, place_ref, product_hbm, *refs):
+    pieces, inputs, outputs, refs = refs[:18], refs[18:23], refs[23:30], refs[30:]
+    product_ref, piece_refs, refs = refs[0], refs[1:19], refs[19:]
+    kept, made, (piece_sems, rest_sems, write_sems) = refs[:5], refs[5:12], refs[12:]
+    shared_ref, master_ref, gate_master_ref, gate_first_ref, gate_second_ref = kept
     step_ref, new_ref, copy_ref, *gate_refs = made
-    reads = started(zip(inputs, kept), read_sems)
     heads = gate_master_ref.shape[0]
     roles, rows, width = master_ref.shape
+    rest = started(zip(inputs, kept), rest_sems)
+    waits = []
+    for role in range(roles):
+        pairs = [(product_hbm.at[role], product_ref.at[role])]
+        chosen, index = (range(0, 5), role) if role + 1 < roles else (range(5, 9), 0)
+        for n in [part * 9 + n for part in range(2) for n in chosen]:
+            pairs.append((pieces[n].at[:, index], piece_refs[n].at[:, index]))
+        waits.append(started(pairs, piece_sems.at[role]))
+    along = place_ref[3], place_ref[4]
+    side = rows // 2
+    own = pl.ds(pl.multiple_of(place_ref[0] * rows, rows), rows)
+    finished(rest)
     squares = jnp.sum(shared_ref[:, heads, 0:1], axis=0, keepdims=True)
     scale = 1.0 / jnp.sqrt(squares / entries + 1e-06)
-    along = place_ref[3], place_ref[4]
-    side = rows // 2
     writes = []
-    for role in range(roles):
-        for part in range(2):
-            for first in range(4):
-                for second in range(4):
-                    offsets = (first, second) if part == 0 else (second, first)
-                    source = [(along[n] + 4 - offsets[n]) % 4 for n in range(2)]
-                    source = source[0] * 4 + source[1]
-                    if second == 2:
-                        ref, index = pieces[part * 5 + 3 + first // 2], first % 2
-                    else:
-                        ref, index = pieces[part * 5 + (0, 1, None, 2)[second]], first
-                    at = pl.ds(pl.multiple_of(source * rows + part * side, side), side)
-                    step = scale * product_ref[role, at]
-                    new = ref[index, role] - LEARN * step
-                    copy_ref[role, at] = new.astype(jnp.bfloat16)
-        writes += started([(copy_ref.at[role], outputs[2].at[role])], write_sems.at[pl.ds(role, 1)])
-    finished(reads)
-    at = pl.ds(pl.multiple_of(place_ref[0] * rows, rows), rows)
-    for role in range(roles):
-        step = scale * product_ref[role, at]
-        step_ref[role] = step
-        new_ref[role] = master_ref[role] - LEARN * step
     for peer in range(shared_ref.shape[0]):
         at = slice(peer * width, (peer + 1) * width)
         grad = shared_ref[peer, :heads]
@@ -357,11 +387,34 @@
         gate_refs[1][:, at] = new.astype(jnp.bfloat16)
         gate_refs[2][:, at] = first
         gate_refs[3][:, at] = second
-    rest = [(made[n], outputs[n]) for n in (0, 1, 3, 4, 5, 6)]
-    finished(writes + started(rest, write_sems.at[pl.ds(roles, 6)]))
-
-
-def finals(entries, place, shared, product, pieces, master, gates):
+    writes += started(zip(made[3:], outputs[3:]), write_sems.at[pl.ds(roles * 3, 4)])
+    for role in range(roles):
+        finished(waits[role])
+        for part in range(2):
+            for first in range(4):
+                for second in range(4):
+                    offsets = (first, second) if part == 0 else (second, first)
+                    source = [(along[n] + 4 - offsets[n]) % 4 for n in range(2)]
+                    source = source[0] * 4 + source[1]
+                    at = pl.ds(pl.multiple_of(source * rows + part * side, side), side)
+                    index = first
+                    if role + 1 == roles:
+                        ref = piece_refs[part * 9 + 5 + second][index, 0]
+                    else:
+                        place = (0, 1, 3 + first // 2, 2)[second]
+                        index = first % 2 if second == 2 else first
+                        ref = piece_refs[part * 9 + place][index, role]
+                    new = ref - LEARN * (scale * product_ref[role, at])
+                    copy_ref[role, at] = new.astype(jnp.bfloat16)
+        step = scale * product_ref[role, own]
+        step_ref[role] = step
+        new_ref[role] = master_ref[role] - LEARN * step
+        pairs = [(made[n].at[role], outputs[n].at[role]) for n in range(3)]
+        writes += started(pairs, write_sems.at[pl.ds(role * 3, 3)])
+    finished(writes)
+
+
+def finals(entries, place, product, pieces, shared, master, gates):
     roles = master.shape[0]
     outs = [
         (master.shape, jnp.float32),
@@ -372,18 +425,58 @@
         (gates[0].shape, jnp.float32),
         (gates[0].shape, jnp.float32),
     ]
-    kept = [(a.shape, a.dtype) for a in (master, *gates)]
+    inputs = (shared, master, *gates)
+    kept = [(a.shape, a.dtype) for a in (product, *pieces, *inputs)]
+    dma = pltpu.SemaphoreType.DMA
     return pl.pallas_call(
         functools.partial(final_kernel, entries),
         out_shape=[pltpu.HBM(*out) for out in outs],
-        in_specs=[SMEM, VMEM, VMEM] + [VMEM] * 10 + [HBM] * 4,
+        in_specs=[SMEM] + [HBM] * len(kept),
         out_specs=[HBM] * 7,
         scratch_shapes=[pltpu.VMEM(*a) for a in kept + outs]
-        + [pltpu.SemaphoreType.DMA((4,)), pltpu.SemaphoreType.DMA((roles + 6,))],
-        compiler_params=room(20),
+        + [dma((roles, 11)), dma((5,)), dma((roles * 3 + 4,))],
+        compiler_params=room(32),
         cost_estimate=cost(10**7, 16 * 10**6),
         name="finals",
-    )(place, shared, *held(pltpu.VMEM, product), *pieces, *held(pltpu.HBM, master, *gates))
+    )(place, *held(pltpu.HBM, product, *pieces, *inputs))
+
+
+def join_kernel(master_hbm, *refs):
+    pieces, outs, blocks, (read_sems, write_sems) = refs[:6], refs[6:10], refs[10:12], refs[12:]
+    early = outs[0].shape[1]
+    side = master_hbm.shape[1] // 2
+    pairs = []
+    for part, block in enumerate(blocks):
+        pairs.append((master_hbm.at[:, pl.ds(part * side, side)], block.at[0]))
+        pairs += [(pieces[part * 3 + n].at[0], block.at[n + 1]) for n in range(3)]
+    reads, writes = started(pairs, read_sems), []
+    for n, read in enumerate(reads):
+        read.wait()
+        block = blocks[n // 4].at[n % 4]
+        pairs = [
+            (block.at[pl.ds(0, early)], outs[n // 4].at[n % 4]),
+            (block.at[pl.ds(early, block.shape[0] - early)], outs[2 + n // 4].at[n % 4]),
+        ]
+        writes += started(pairs, write_sems.at[pl.ds(n * 2, 2)])
+    finished(writes)
+
+
+def joined(master, pieces, early):
+    shape = (4, *pieces[0].shape[1:])
+    return pl.pallas_call(
+        join_kernel,
+        out_shape=[
+            pltpu.HBM((4, count, *shape[2:]), jnp.float32)
+            for count in (early, early, shape[1] - early, shape[1] - early)
+        ],
+        in_specs=[HBM] * 7,
+        out_specs=[HBM] * 4,
+        scratch_shapes=[pltpu.VMEM(shape, jnp.float32)] * 2
+        + [pltpu.SemaphoreType.DMA((8,)), pltpu.SemaphoreType.DMA((16,))],
+        compiler_params=room(4),
+        cost_estimate=cost(10**6, 6 * 10**6),
+        name="joined",
+    )(*held(pltpu.HBM, master, *pieces))
 
 
 def shift(x, axis, by):
@@ -413,28 +506,35 @@
     near = lax.all_to_all(near, FS, split_axis=0, concat_axis=0, tiled=True)
     far = lax.ppermute(near, "c", [(0, 1), (1, 0)])
     sides = proj_master.reshape(roles, 2, rows // 2, width)
-    sides = [(sides[:, part][None], axis) for part, axis in enumerate(FS)]
-    sides = [[side] + [shift(side, axis, by) for by in (1, 2, 3)] for side, axis in sides]
-    sides = [jnp.concatenate(side) for side in sides]
-    ahead = [shift(side, axis, 1) for side, axis in zip(sides, FS[::-1])]
-    behind = [shift(side, axis, 3) for side, axis in zip(sides, FS[::-1])]
-    opposite = [shift(side[:2], axis, 1) for side, axis in zip(ahead, FS[::-1])]
-    other = [shift(side[2:], axis, 3) for side, axis in zip(behind, FS[::-1])]
-    pieces = [x for group in zip(sides, ahead, behind, opposite, other) for x in group]
+    spread = [
+        shift(sides[:, part][None], axis, by) for part, axis in enumerate(FS) for by in (1, 2, 3)
+    ]
+    axes = FS[::-1]
+    *early, first_late, second_late = joined(proj_master, spread, roles - 1)
+    late = (first_late, second_late)
+    ahead = [shift(side, axis, 1) for side, axis in zip(early, axes)]
+    behind = [shift(side, axis, 3) for side, axis in zip(early, axes)]
+    opposite = [shift(side[:2], axis, 1) for side, axis in zip(ahead, axes)]
+    other = [shift(side[2:], axis, 3) for side, axis in zip(behind, axes)]
+    late = [[side] + [shift(side, axis, by) for by in (1, 2, 3)] for side, axis in zip(late, axes)]
+    pieces = [
+        [*group, *rest] for *group, rest in zip(early, ahead, behind, opposite, other, late)
+    ]
+    pieces = [piece for group in pieces for piece in group]
     grad = jnp.einsum("td,rtw->rwd", saved_input, proj_cot, preferred_element_type=jnp.float32)
-    parts = low_parts(grad, near, far)
+    gate_part = gate_columns(place, log_cache, cache_cot, near, saved_input, width)
+    parts = low_parts(grad, near, far, gate_part)
     arrived = lax.all_to_all(parts, FS, split_axis=0, concat_axis=0, tiled=True)
-    gate_part = gate_columns(place, log_cache, cache_cot, near, saved_input, width)
-    sums = lax.all_to_all(summed(arrived, gate_part), FS, split_axis=0, concat_axis=0, tiled=True)
+    sums = lax.all_to_all(summed(arrived), FS, split_axis=0, concat_axis=0, tiled=True)
 
     first_new, second_new, upper, lower, shared = moments(
         place, sums, first_moment, second_moment, lax.axis_size(TP)
     )
     shared = lax.all_to_all(shared, TP, split_axis=0, concat_axis=0, tiled=True)
-    product = products(place, near, far, upper, lower, rows)
+    product = products(near, far, upper, lower, rows)
     entries = first_new.size * lax.axis_size(TP)
     gates = (gate_master, gate_first, gate_second)
-    step, new, copy, *gates = finals(entries, place, shared, product, pieces, proj_master, gates)
+    step, new, copy, *gates = finals(entries, place, product, pieces, shared, proj_master, gates)
     return step, new, copy, first_new, second_new, *gates
 
 

time: 154 us -> 158 us (1.026)
  local copies, waits for them, and re-layouts: 16.2 us -> 5 us
  starting transfers between devices: 36 us -> 45.4 us
  Pallas kernels: 28.9 us -> 33 us
  waiting for transfers between devices: 21.3 us -> 24.9 us
  other arithmetic: 1.92 us -> 0 us
    ppermute x14 -> x20, starting transfers between devices: 19 us -> 30.9 us  [shift(): return lax.ppermute(x, axis, [(i, (i + by) % 4) for i in range(4)])]
    slice x4, local copies, waits for them, and re-layouts: 7.17 us -> 1.54 us  [the longest x2 0.81 us: local(): other = [shift(side[2:], axis, 3) for side, axis in zip(behind, axes)]]
    unnamed x20 -> x40, local copies, waits for them, and re-layouts: 8.9 us -> 3.35 us
    pallas_call x2 -> x3, Pallas kernels: 6.41 us -> 9.48 us  [the longest x1 5.91 us: products(): pl.pallas_call(product_kernel, out_shape=pltpu.HBM(shape, jnp.float32), i...]
    ppermute x14 -> x20, waiting for transfers between devices: 21.3 us -> 24 us  [shift(): return lax.ppermute(x, axis, [(i, (i + by) % 4) for i in range(4)])]
    all_to_all x1, starting transfers between devices: 5.73 us -> 3.63 us  [local(): arrived = lax.all_to_all(parts, FS, split_axis=0, concat_axis=0, tiled=True)]
    concatenate x2 -> x0, other arithmetic: 1.92 us -> none  [local(): sides = [jnp.concatenate(side) for side in sides]]
    pallas_call x1, Pallas kernels: 6.27 us -> 8.07 us  [finals(): pl.pallas_call(functools.partial(final_kernel, entries), out_shape=[pltpu...]
  transfers between devices with their start and end apart: 18 -> 24, of which waited for: 5 -> 8; matrix products, arithmetic and copies ran while one was open for 16% -> 11% of each run, Pallas kernels for 13% -> 10%
where the time goes in v4:
time: 158 us; the launch traced here: 157 us
  starting transfers between devices  45.4 us (29%)
  Pallas kernels  33 us (21%)
  blocking collectives  31.5 us (20%)
  waiting for transfers between devices  24.9 us (16%)
  matrix products  15.7 us (10%)
  local copies, waits for them, and re-layouts  5 us (3%)
    all_to_all x1, blocking collectives, local(): near = lax.all_to_all(near, FS, split_axis=0, concat_axis=0, tiled=True)  31.5 us
    ppermute x20, starting transfers between devices, shift(): return lax.ppermute(x, axis, [(i, (i + by) % 4) for i in range(4)])  30.9 us
    ppermute x20, waiting for transfers between devices, shift(): return lax.ppermute(x, axis, [(i, (i + by) % 4) for i in range(4)])  24 us
    dot_general x1, matrix products, local(): jnp.einsum('td,rtw->rwd', saved_input, proj_cot, preferred_element_type=j...  15.7 us
    pallas_call x1, Pallas kernels, finals(): pl.pallas_call(functools.partial(final_kernel, entries), out_shape=[pltpu...  8.07 us
    all_to_all x1, starting transfers between devices, local(): lax.all_to_all(summed(arrived), FS, split_axis=0, concat_axis=0, tiled=True)  6.31 us
    pallas_call x1, Pallas kernels, low_parts(): pl.pallas_call(low_kernel, out_shape=pltpu.HBM((peers, lines, width), jnp...  6.24 us
    pallas_call x1, Pallas kernels, products(): pl.pallas_call(product_kernel, out_shape=pltpu.HBM(shape, jnp.float32), i...  5.91 us
  transfers between devices with their start and end apart: 24, of which 8 were waited for; matrix products, arithmetic and copies ran while one was open for 11% of the time, Pallas kernels for 10%

profile of v4, /device:TPU:0, one launch (start us, length us, event | category | flops | bytes accessed | tf_op | source)
XLA Modules:
  0.0 156.5 jit_solution(10966646949918639487)
XLA Ops:
  0.7 0.1 stack.23.place_ref
  0.7 3.3 %packed.1 = bf16[16,400,128]{2,1,0:T(8,128)(2,1)} custom-call(s32[5]{0:T(128)S(1)} %stack.23.place_ref, bf16[3,128,256]{2,1,0:T(8,128)(2,1)} %factor_ref.1, f32[16,3072]{1,0:T(8,128)} %log_hbm.1, f32[16,3072]{1,0:T(8,128)} %cot_hbm.1), custom_call_target="tpu_custom_call" | custom-call | flops 1000000 | bytes 2000000 | tf_op jit(solution)/shard_map/packed/pallas_call | solution.py:84
  4.0 31.5 %all_to_all.20.ends_hbm.near_ref.near_hbm = bf16[16,400,128]{2,1,0:T(8,128)(2,1)S(1)} all-to-all(bf16[16,400,128]{2,1,0:T(8,128)(2,1)} %packed.1), channel_id=1, replica_groups=mesh['z'=4,'x'=4,'y'=4,'c'=2] {'z','x'}, dimensions={0} | all-to-all | bytes 3276800 | tf_op jit(solution)/shard_map/all_to_all | solution.py:506
  35.5 15.7 %fusion.grad_ref = f32[3,256,2048]{2,1,0:T(8,128)} fusion(bf16[3,3072,256]{2,1,0:T(8,128)(2,1)S(1)} %copy-done.19, bf16[3072,2048]{1,0:T(8,128)(2,1)} %input_hbm.1), kind=kOutput, calls=%fused_computation | convolution fusion | flops 9663676416 | bytes 23592960 | tf_op jit(solution)/shard_map/td,rtw->rwd/dot_general | solution.py:524
  51.2 2.5 %gate_columns.1.gate_ref = f32[16,256]{1,0:T(8,128)S(1)} custom-call(s32[5]{0:T(128)S(1)} %stack.23.place_ref, f32[16,3072]{1,0:T(8,128)} %log_hbm.1, f32[16,3072]{1,0:T(8,128)} %cot_hbm.1, bf16[16,400,128]{2,1,0:T(8,128)(2,1)} %copy-done, bf16[3072,2048]{1,0:T(8,128)(2,1)} %input_hbm.1), custom_call_target="tpu_custom_call" | custom-call | flops 4000000000 | bytes 4000000 | tf_op jit(solution)/shard_map/gate_columns/pallas_call | solution.py:145
  53.8 1.2 copy-done.1
  55.0 6.2 %low_parts.1 = f32[16,56,256]{2,1,0:T(8,128)} custom-call(f32[3,256,2048]{2,1,0:T(8,128)} %fusion.grad_ref, bf16[16,400,128]{2,1,0:T(8,128)(2,1)} %copy-done, bf16[16,400,128]{2,1,0:T(8,128)(2,1)} %copy-done.1, f32[16,256]{1,0:T(8,128)S(1)} %gate_columns.1.gate_ref), custom_call_target="tpu_custom_call" | custom-call | flops 1610612736 | bytes 11000000 | tf_op jit(solution)/shard_map/low_parts/pallas_call | solution.py:191
  61.2 3.6 %all-to-all-start.1 = ((f32[16,56,256]{2,1,0:T(8,128)}), f32[16,56,256]{2,1,0:T(8,128)S(1)}, u32[]{:S(2)}, u32[]{:S(2)}) async-start(f32[16,56,256]{2,1,0:T(8,128)} %low_parts.1), calls=%async_computation.1 | async-start | bytes 1835008 | tf_op jit(solution)/shard_map/all_to_all | solution.py:527
  64.9 3.1 %collective-permute-start.6 = (f32[1,3,64,256]{3,2,1,0:T(8,128)S(1)}, f32[1,3,64,256]{3,2,1,0:T(8,128)S(1)}, u32[]{:S(2)}, u32[]{:S(2)}) collective-permute-start(f32[1,3,64,256]{3,2,1,0:T(8,128)S(1)} %get-tuple-element.41), channel_id=1, source_target_pairs={{0,24},{8,0},{16,8},{24,16},{1,25},{9,1},{17,9},{25,17},{2,26},{10... | collective-permute-start | bytes 589832 | tf_op jit(solution)/shard_map/ppermute | solution.py:483
  68.0 0.8 collective-permute-start.5
  68.8 0.9 collective-permute-start.4
  69.7 2.8 %collective-permute-start.3 = (f32[1,3,64,256]{3,2,1,0:T(8,128)S(1)}, f32[1,3,64,256]{3,2,1,0:T(8,128)S(1)}, u32[]{:S(2)}, u32[]{:S(2)}) collective-permute-start(f32[1,3,64,256]{3,2,1,0:T(8,128)S(1)} %get-tuple-element.42), channel_id=1, source_target_pairs={{0,96},{32,0},{64,32},{96,64},{1,97},{33,1},{65,33},{97,65},{2,98}... | collective-permute-start | bytes 589832 | tf_op jit(solution)/shard_map/ppermute | solution.py:483
  72.4 0.8 collective-permute-start.2
  73.2 9.2 %collective-permute-done.6.refs_5_ = f32[1,3,64,256]{3,2,1,0:T(8,128)S(1)} collective-permute-done((f32[1,3,64,256]{3,2,1,0:T(8,128)S(1)}, f32[1,3,64,256]{3,2,1,0:T(8,128)S(1)}, u32[]{:S(2)}, u32[]{:S(2)}) %collective-permute-start.6) | collective-permute-done | bytes 196640 | tf_op jit(solution)/shard_map/ppermute | solution.py:483
  82.4 1.5 collective-permute-start.1
  83.9 0.1 collective-permute-done.5.refs_4_
  84.0 2.8 %collective-permute-done.4.refs_3_ = f32[1,3,64,256]{3,2,1,0:T(8,128)S(1)} collective-permute-done((f32[1,3,64,256]{3,2,1,0:T(8,128)S(1)}, f32[1,3,64,256]{3,2,1,0:T(8,128)S(1)}, u32[]{:S(2)}, u32[]{:S(2)}) %collective-permute-start.4) | collective-permute-done | bytes 196640 | tf_op jit(solution)/shard_map/ppermute | solution.py:483
  86.8 0.0 copy-start.17
  86.8 2.5 %collective-permute-done.1.refs_0_ = f32[1,3,64,256]{3,2,1,0:T(8,128)S(1)} collective-permute-done((f32[1,3,64,256]{3,2,1,0:T(8,128)S(1)}, f32[1,3,64,256]{3,2,1,0:T(8,128)S(1)}, u32[]{:S(2)}, u32[]{:S(2)}) %collective-permute-start.1) | collective-permute-done | bytes 196640 | tf_op jit(solution)/shard_map/ppermute | solution.py:483
  89.3 0.0 copy-start.18
  89.3 0.7 copy-done.18
  90.0 2.4 %joined.1 = (f32[4,2,64,256]{3,2,1,0:T(8,128)}, f32[4,2,64,256]{3,2,1,0:T(8,128)}, f32[4,1,64,256]{3,2,1,0:T(8,128)}, f32[4,1,64,256]{3,2,1,0:T(8,128)}) custom-call(f32[3,128,256]{2,1,0:T(8,128)} %refs_19_.1, f32[1,3,64,256]{3,2,1,0:T(8,128)} %copy-done.18, f32[1,3,64,256]{3,2,1,0:T(8,128)} %copy-done.17, f32[1,3,64,256]{3,2,1,0:T(8,128)} %copy-done.16, ...), custom_call_target="tpu_custom_call" | custom-call | flops 1000000 | bytes 6000000 | tf_op jit(solution)/shard_map/joined/pallas_call | solution.py:466
  92.4 1.1 collective-permute-start.8
  93.5 1.0 collective-permute-start.7
  94.5 1.5 collective-permute-start.15
  96.0 0.5 collective-permute-start.14
  96.5 1.2 summed.1
  97.7 6.3 %all-to-all-start.2 = ((f32[16,56,256]{2,1,0:T(8,128)}), f32[16,56,256]{2,1,0:T(8,128)S(1)}, u32[]{:S(2)}, u32[]{:S(2)}) async-start(f32[16,56,256]{2,1,0:T(8,128)} %summed.1), calls=%async_computation.2 | async-start | bytes 1835008 | tf_op jit(solution)/shard_map/all_to_all | solution.py:528
  104.1 3.1 %collective-permute-start.13 = (f32[4,1,64,256]{3,2,1,0:T(8,128)}, f32[4,1,64,256]{3,2,1,0:T(8,128)S(1)}, u32[]{:S(2)}, u32[]{:S(2)}) collective-permute-start(f32[4,1,64,256]{3,2,1,0:T(8,128)} %get-tuple-element.28.refs_5_), channel_id=1, source_target_pairs={{0,24},{8,0},{16,8},{24,16},{1,25},{9,1},{17,9},{25,17},{2,26},{10... | collective-permute-start | bytes 786440 | tf_op jit(solution)/shard_map/ppermute | solution.py:483
  107.2 0.9 collective-permute-start.12
  108.1 2.6 %collective-permute-done.7.refs_1_ = f32[4,2,64,256]{3,2,1,0:T(8,128)S(1)} collective-permute-done((f32[4,2,64,256]{3,2,1,0:T(8,128)}, f32[4,2,64,256]{3,2,1,0:T(8,128)S(1)}, u32[]{:S(2)}, u32[]{:S(2)}) %collective-permute-start.7) | collective-permute-done | bytes 524320 | tf_op jit(solution)/shard_map/ppermute | solution.py:483
  110.6 0.4 collective-permute-start.11
  111.0 4.3 %collective-permute-done.15.refs_11_ = f32[4,2,64,256]{3,2,1,0:T(8,128)S(1)} collective-permute-done((f32[4,2,64,256]{3,2,1,0:T(8,128)}, f32[4,2,64,256]{3,2,1,0:T(8,128)S(1)}, u32[]{:S(2)}, u32[]{:S(2)}) %collective-permute-start.15) | collective-permute-done | bytes 524320 | tf_op jit(solution)/shard_map/ppermute | solution.py:483
  115.3 3.7 %collective-permute-start.20 = (f32[4,1,64,256]{3,2,1,0:T(8,128)}, f32[4,1,64,256]{3,2,1,0:T(8,128)S(1)}, u32[]{:S(2)}, u32[]{:S(2)}) collective-permute-start(f32[4,1,64,256]{3,2,1,0:T(8,128)} %get-tuple-element.30.refs_14_), channel_id=1, source_target_pairs={{0,96},{32,0},{64,32},{96,64},{1,97},{33,1},{65,33},{97,65},{2,98}... | collective-permute-start | bytes 786440 | tf_op jit(solution)/shard_map/ppermute | solution.py:483
  119.1 2.6 %collective-permute-done.14.refs_10_ = f32[4,2,64,256]{3,2,1,0:T(8,128)S(1)} collective-permute-done((f32[4,2,64,256]{3,2,1,0:T(8,128)}, f32[4,2,64,256]{3,2,1,0:T(8,128)S(1)}, u32[]{:S(2)}, u32[]{:S(2)}) %collective-permute-start.14) | collective-permute-done | bytes 524320 | tf_op jit(solution)/shard_map/ppermute | solution.py:483
  121.7 0.8 slice.31
  122.5 0.7 slice.30
  123.2 3.0 %collective-permute-start.18 = (f32[4,1,64,256]{3,2,1,0:T(8,128)}, f32[4,1,64,256]{3,2,1,0:T(8,128)}, u32[]{:S(2)}, u32[]{:S(2)}) collective-permute-start(f32[4,1,64,256]{3,2,1,0:T(8,128)} %get-tuple-element.30.refs_14_), channel_id=1, source_target_pairs={{0,32},{32,64},{64,96},{96,0},{1,33},{33,65},{65,97},{97,1},{2,34}... | collective-permute-start | bytes 786440 | tf_op jit(solution)/shard_map/ppermute | solution.py:483
  126.3 3.7 %collective-permute-start.10 = (f32[2,2,64,256]{3,2,1,0:T(8,128)}, f32[2,2,64,256]{3,2,1,0:T(8,128)}, u32[]{:S(2)}, u32[]{:S(2)}) collective-permute-start(f32[2,2,64,256]{3,2,1,0:T(8,128)} %slice.31), channel_id=1, source_target_pairs={{0,24},{8,0},{16,8},{24,16},{1,25},{9,1},{17,9},{25,17},{2,26},{10... | collective-permute-start | bytes 786440 | tf_op jit(solution)/shard_map/ppermute | solution.py:483
  130.0 1.6 collective-permute-start.17
  131.6 0.7 copy-done.12
  132.4 0.5 collective-permute-start.16
  132.9 3.4 %moments.1 = (f32[3,256,256]{2,1,0:T(8,128)}, f32[3,256,256]{2,1,0:T(8,128)}, bf16[3,256,256]{2,1,0:T(8,128)(2,1)}, bf16[3,256,256]{2,1,0:T(8,128)(2,1)}, f32[8,24,256]{2,1,0:T(8,128)}) custom-call(s32[5]{0:T(128)S(1)} %stack.23.place_ref, f32[16,56,256]{2,1,0:T(8,128)S(1)} %all-to-all-done.2.sums_ref, f32[3,256,256]{2,1,0:T(8,128)} %first_hbm.1, ...), custom_call_target="tpu_custom_call" | custom-call | flops 10000000 | bytes 6000000 | tf_op jit(solution)/shard_map/moments/pallas_call | solution.py:281
  136.3 4.5 %all-to-all-start.3 = ((f32[8,24,256]{2,1,0:T(8,128)}), f32[8,24,256]{2,1,0:T(8,128)S(1)}, u32[]{:S(2)}, u32[]{:S(2)}) async-start(f32[8,24,256]{2,1,0:T(8,128)} %get-tuple-element.31), calls=%async_computation.3 | async-start | bytes 393216 | tf_op jit(solution)/shard_map/all_to_all | solution.py:533
  140.8 5.9 %products.1.product_hbm = f32[3,2048,256]{2,1,0:T(8,128)} custom-call(bf16[16,400,128]{2,1,0:T(8,128)(2,1)} %copy-done, bf16[16,400,128]{2,1,0:T(8,128)(2,1)} %copy-done.1, bf16[3,256,256]{2,1,0:T(8,128)(2,1)} %get-tuple-element.25.upper_hbm, bf16[3,256,256]{2,1,0:T(8,128)(2,1)} %get-tuple-element.26.lower_hbm), custom_call_target="tpu_custom_call" | custom-call | flops 1610612736 | bytes 10000000 | tf_op jit(solution)/shard_map/products/pallas_call | solution.py:339
  146.8 0.8 all-to-all-done.3.refs_18_
  147.6 0.7 copy-done.7
  148.3 8.1 %finals.1 = (f32[3,128,256]{2,1,0:T(8,128)}, f32[3,128,256]{2,1,0:T(8,128)}, bf16[3,2048,256]{2,1,0:T(8,128)(2,1)}, f32[16,2048]{1,0:T(8,128)}, bf16[16,2048]{1,...) custom-call(s32[5]{0:T(128)S(1)} %stack.23.place_ref, f32[3,2048,256]{2,1,0:T(8,128)} %products.1.product_hbm, ...), custom_call_target="tpu_custom_call" | custom-call | flops 10000000 | bytes 16000000 | tf_op jit(solution)/shard_map/finals/pallas_call | solution.py:431
  (56 shorter events, 0.2 us)
Async XLA Ops:
  0.7 34.8 %copy-start.19 = (bf16[3,3072,256]{2,1,0:T(8,128)(2,1)S(1)}, bf16[3,3072,256]{2,1,0:T(8,128)(2,1)}, u32[]{:S(2)}) copy-start(bf16[3,3072,256]{2,1,0:T(8,128)(2,1)} %param.12) | copy-start | bytes 14155780
  35.5 15.7 %copy-start = (bf16[16,400,128]{2,1,0:T(8,128)(2,1)}, bf16[16,400,128]{2,1,0:T(8,128)(2,1)S(1)}, u32[]{:S(2)}) copy-start(bf16[16,400,128]{2,1,0:T(8,128)(2,1)S(1)} %all_to_all.20.ends_hbm.near_ref.near_hbm) | copy-start | bytes 4915204
  35.5 18.3 %collective-permute-start = (bf16[16,400,128]{2,1,0:T(8,128)(2,1)S(1)}, bf16[16,400,128]{2,1,0:T(8,128)(2,1)S(1)}, u32[]{:S(2)}, u32[]{:S(2)}) collective-permute-start(bf16[16,400,128]{2,1,0:T(8,128)(2,1)S(1)} %all_to_all.20.ends_hbm.near_ref.near_hbm), channel_id=1, source_target_pairs={{0,1},{1,0},{2,3},{3,2},{4,5},{5,4},{6,7},{7,6},{8,9},{9,8},{10,11... | collective-permute-start | bytes 4915208 | tf_op jit(solution)/shard_map/ppermute | solution.py:507
  53.7 11.1 %copy-start.2 = (f32[3,128,256]{2,1,0:T(8,128)S(1)}, f32[3,128,256]{2,1,0:T(8,128)}, u32[]{:S(2)}) copy-start(f32[3,128,256]{2,1,0:T(8,128)} %refs_19_.1) | copy-start | bytes 1179652
  53.8 1.2 copy-start.1
  61.2 35.3 %all-to-all-start.1 = ((f32[16,56,256]{2,1,0:T(8,128)}), f32[16,56,256]{2,1,0:T(8,128)S(1)}, u32[]{:S(2)}, u32[]{:S(2)}) async-start(f32[16,56,256]{2,1,0:T(8,128)} %low_parts.1), calls=%async_computation.1 | async-start | bytes 1835008 | tf_op jit(solution)/shard_map/all_to_all | solution.py:527
  64.9 17.5 %collective-permute-start.6 = (f32[1,3,64,256]{3,2,1,0:T(8,128)S(1)}, f32[1,3,64,256]{3,2,1,0:T(8,128)S(1)}, u32[]{:S(2)}, u32[]{:S(2)}) collective-permute-start(f32[1,3,64,256]{3,2,1,0:T(8,128)S(1)} %get-tuple-element.41), channel_id=1, source_target_pairs={{0,24},{8,0},{16,8},{24,16},{1,25},{9,1},{17,9},{25,17},{2,26},{10... | collective-permute-start | bytes 589832 | tf_op jit(solution)/shard_map/ppermute | solution.py:483
  68.0 16.0 %collective-permute-start.5 = (f32[1,3,64,256]{3,2,1,0:T(8,128)S(1)}, f32[1,3,64,256]{3,2,1,0:T(8,128)S(1)}, u32[]{:S(2)}, u32[]{:S(2)}) collective-permute-start(f32[1,3,64,256]{3,2,1,0:T(8,128)S(1)} %get-tuple-element.41), channel_id=1, source_target_pairs={{0,16},{8,24},{16,0},{24,8},{1,17},{9,25},{17,1},{25,9},{2,18},{10... | collective-permute-start | bytes 589832 | tf_op jit(solution)/shard_map/ppermute | solution.py:483
  68.8 18.0 %collective-permute-start.4 = (f32[1,3,64,256]{3,2,1,0:T(8,128)S(1)}, f32[1,3,64,256]{3,2,1,0:T(8,128)S(1)}, u32[]{:S(2)}, u32[]{:S(2)}) collective-permute-start(f32[1,3,64,256]{3,2,1,0:T(8,128)S(1)} %get-tuple-element.41), channel_id=1, source_target_pairs={{0,8},{8,16},{16,24},{24,0},{1,9},{9,17},{17,25},{25,1},{2,10},{10... | collective-permute-start | bytes 589832 | tf_op jit(solution)/shard_map/ppermute | solution.py:483
  69.7 17.1 %collective-permute-start.3 = (f32[1,3,64,256]{3,2,1,0:T(8,128)S(1)}, f32[1,3,64,256]{3,2,1,0:T(8,128)S(1)}, u32[]{:S(2)}, u32[]{:S(2)}) collective-permute-start(f32[1,3,64,256]{3,2,1,0:T(8,128)S(1)} %get-tuple-element.42), channel_id=1, source_target_pairs={{0,96},{32,0},{64,32},{96,64},{1,97},{33,1},{65,33},{97,65},{2,98}... | collective-permute-start | bytes 589832 | tf_op jit(solution)/shard_map/ppermute | solution.py:483
  72.4 14.4 %collective-permute-start.2 = (f32[1,3,64,256]{3,2,1,0:T(8,128)S(1)}, f32[1,3,64,256]{3,2,1,0:T(8,128)S(1)}, u32[]{:S(2)}, u32[]{:S(2)}) collective-permute-start(f32[1,3,64,256]{3,2,1,0:T(8,128)S(1)} %get-tuple-element.42), channel_id=1, source_target_pairs={{0,64},{32,96},{64,0},{96,32},{1,65},{33,97},{65,1},{97,33},{2,66}... | collective-permute-start | bytes 589832 | tf_op jit(solution)/shard_map/ppermute | solution.py:483
  82.4 6.9 %copy-start.13 = (f32[1,3,64,256]{3,2,1,0:T(8,128)}, f32[1,3,64,256]{3,2,1,0:T(8,128)S(1)}, u32[]{:S(2)}) copy-start(f32[1,3,64,256]{3,2,1,0:T(8,128)S(1)} %collective-permute-done.6.refs_5_) | copy-start | bytes 589828
  82.4 6.9 %collective-permute-start.1 = (f32[1,3,64,256]{3,2,1,0:T(8,128)S(1)}, f32[1,3,64,256]{3,2,1,0:T(8,128)S(1)}, u32[]{:S(2)}, u32[]{:S(2)}) collective-permute-start(f32[1,3,64,256]{3,2,1,0:T(8,128)S(1)} %get-tuple-element.42), channel_id=1, source_target_pairs={{0,32},{32,64},{64,96},{96,0},{1,33},{33,65},{65,97},{97,1},{2,34}... | collective-permute-start | bytes 589832 | tf_op jit(solution)/shard_map/ppermute | solution.py:483
  84.0 5.3 %copy-start.14 = (f32[1,3,64,256]{3,2,1,0:T(8,128)}, f32[1,3,64,256]{3,2,1,0:T(8,128)S(1)}, u32[]{:S(2)}) copy-start(f32[1,3,64,256]{3,2,1,0:T(8,128)S(1)} %collective-permute-done.5.refs_4_) | copy-start | bytes 589828
  86.8 2.5 %copy-start.15 = (f32[1,3,64,256]{3,2,1,0:T(8,128)}, f32[1,3,64,256]{3,2,1,0:T(8,128)S(1)}, u32[]{:S(2)}) copy-start(f32[1,3,64,256]{3,2,1,0:T(8,128)S(1)} %collective-permute-done.4.refs_3_) | copy-start | bytes 589828
  86.8 2.5 %copy-start.16 = (f32[1,3,64,256]{3,2,1,0:T(8,128)}, f32[1,3,64,256]{3,2,1,0:T(8,128)S(1)}, u32[]{:S(2)}) copy-start(f32[1,3,64,256]{3,2,1,0:T(8,128)S(1)} %collective-permute-done.3.refs_2_) | copy-start | bytes 589828
  86.8 2.5 %copy-start.17 = (f32[1,3,64,256]{3,2,1,0:T(8,128)}, f32[1,3,64,256]{3,2,1,0:T(8,128)S(1)}, u32[]{:S(2)}) copy-start(f32[1,3,64,256]{3,2,1,0:T(8,128)S(1)} %collective-permute-done.2.refs_1_) | copy-start | bytes 589828
  89.3 0.7 copy-start.18
  92.4 14.8 %collective-permute-start.8 = (f32[4,2,64,256]{3,2,1,0:T(8,128)}, f32[4,2,64,256]{3,2,1,0:T(8,128)S(1)}, u32[]{:S(2)}, u32[]{:S(2)}) collective-permute-start(f32[4,2,64,256]{3,2,1,0:T(8,128)} %get-tuple-element.27.refs_0_), channel_id=1, source_target_pairs={{0,24},{8,0},{16,8},{24,16},{1,25},{9,1},{17,9},{25,17},{2,26},{10... | collective-permute-start | bytes 1572872 | tf_op jit(solution)/shard_map/ppermute | solution.py:483
  93.5 17.1 %collective-permute-start.7 = (f32[4,2,64,256]{3,2,1,0:T(8,128)}, f32[4,2,64,256]{3,2,1,0:T(8,128)S(1)}, u32[]{:S(2)}, u32[]{:S(2)}) collective-permute-start(f32[4,2,64,256]{3,2,1,0:T(8,128)} %get-tuple-element.27.refs_0_), channel_id=1, source_target_pairs={{0,8},{8,16},{16,24},{24,0},{1,9},{9,17},{17,25},{25,1},{2,10},{10... | collective-permute-start | bytes 1572872 | tf_op jit(solution)/shard_map/ppermute | solution.py:483
  94.5 20.9 %collective-permute-start.15 = (f32[4,2,64,256]{3,2,1,0:T(8,128)}, f32[4,2,64,256]{3,2,1,0:T(8,128)S(1)}, u32[]{:S(2)}, u32[]{:S(2)}) collective-permute-start(f32[4,2,64,256]{3,2,1,0:T(8,128)} %get-tuple-element.29.refs_9_), channel_id=1, source_target_pairs={{0,96},{32,0},{64,32},{96,64},{1,97},{33,1},{65,33},{97,65},{2,98}... | collective-permute-start | bytes 1572872 | tf_op jit(solution)/shard_map/ppermute | solution.py:483
  96.0 25.6 %collective-permute-start.14 = (f32[4,2,64,256]{3,2,1,0:T(8,128)}, f32[4,2,64,256]{3,2,1,0:T(8,128)S(1)}, u32[]{:S(2)}, u32[]{:S(2)}) collective-permute-start(f32[4,2,64,256]{3,2,1,0:T(8,128)} %get-tuple-element.29.refs_9_), channel_id=1, source_target_pairs={{0,32},{32,64},{64,96},{96,0},{1,33},{33,65},{65,97},{97,1},{2,34}... | collective-permute-start | bytes 1572872 | tf_op jit(solution)/shard_map/ppermute | solution.py:483
  97.7 35.2 %all-to-all-start.2 = ((f32[16,56,256]{2,1,0:T(8,128)}), f32[16,56,256]{2,1,0:T(8,128)S(1)}, u32[]{:S(2)}, u32[]{:S(2)}) async-start(f32[16,56,256]{2,1,0:T(8,128)} %summed.1), calls=%async_computation.2 | async-start | bytes 1835008 | tf_op jit(solution)/shard_map/all_to_all | solution.py:528
  104.1 19.2 %collective-permute-start.13 = (f32[4,1,64,256]{3,2,1,0:T(8,128)}, f32[4,1,64,256]{3,2,1,0:T(8,128)S(1)}, u32[]{:S(2)}, u32[]{:S(2)}) collective-permute-start(f32[4,1,64,256]{3,2,1,0:T(8,128)} %get-tuple-element.28.refs_5_), channel_id=1, source_target_pairs={{0,24},{8,0},{16,8},{24,16},{1,25},{9,1},{17,9},{25,17},{2,26},{10... | collective-permute-start | bytes 786440 | tf_op jit(solution)/shard_map/ppermute | solution.py:483
  107.2 39.5 %copy-start.3 = (f32[4,2,64,256]{3,2,1,0:T(8,128)}, f32[4,2,64,256]{3,2,1,0:T(8,128)S(1)}, u32[]{:S(2)}) copy-start(f32[4,2,64,256]{3,2,1,0:T(8,128)S(1)} %collective-permute-done.8.refs_2_) | copy-start | bytes 1572868
  107.2 19.1 %collective-permute-start.12 = (f32[4,1,64,256]{3,2,1,0:T(8,128)}, f32[4,1,64,256]{3,2,1,0:T(8,128)S(1)}, u32[]{:S(2)}, u32[]{:S(2)}) collective-permute-start(f32[4,1,64,256]{3,2,1,0:T(8,128)} %get-tuple-element.28.refs_5_), channel_id=1, source_target_pairs={{0,16},{8,24},{16,0},{24,8},{1,17},{9,25},{17,1},{25,9},{2,18},{10... | collective-permute-start | bytes 786440 | tf_op jit(solution)/shard_map/ppermute | solution.py:483
  110.6 36.1 %copy-start.4 = (f32[4,2,64,256]{3,2,1,0:T(8,128)}, f32[4,2,64,256]{3,2,1,0:T(8,128)S(1)}, u32[]{:S(2)}) copy-start(f32[4,2,64,256]{3,2,1,0:T(8,128)S(1)} %collective-permute-done.7.refs_1_) | copy-start | bytes 1572868
  110.6 19.4 %collective-permute-start.11 = (f32[4,1,64,256]{3,2,1,0:T(8,128)}, f32[4,1,64,256]{3,2,1,0:T(8,128)S(1)}, u32[]{:S(2)}, u32[]{:S(2)}) collective-permute-start(f32[4,1,64,256]{3,2,1,0:T(8,128)} %get-tuple-element.28.refs_5_), channel_id=1, source_target_pairs={{0,8},{8,16},{16,24},{24,0},{1,9},{9,17},{17,25},{25,1},{2,10},{10... | collective-permute-start | bytes 786440 | tf_op jit(solution)/shard_map/ppermute | solution.py:483
  115.3 31.4 %copy-start.5 = (f32[4,2,64,256]{3,2,1,0:T(8,128)}, f32[4,2,64,256]{3,2,1,0:T(8,128)S(1)}, u32[]{:S(2)}) copy-start(f32[4,2,64,256]{3,2,1,0:T(8,128)S(1)} %collective-permute-done.15.refs_11_) | copy-start | bytes 1572868
  115.3 14.7 %collective-permute-start.20 = (f32[4,1,64,256]{3,2,1,0:T(8,128)}, f32[4,1,64,256]{3,2,1,0:T(8,128)S(1)}, u32[]{:S(2)}, u32[]{:S(2)}) collective-permute-start(f32[4,1,64,256]{3,2,1,0:T(8,128)} %get-tuple-element.30.refs_14_), channel_id=1, source_target_pairs={{0,96},{32,0},{64,32},{96,64},{1,97},{33,1},{65,33},{97,65},{2,98}... | collective-permute-start | bytes 786440 | tf_op jit(solution)/shard_map/ppermute | solution.py:483
  121.7 25.0 %copy-start.6 = (f32[4,2,64,256]{3,2,1,0:T(8,128)}, f32[4,2,64,256]{3,2,1,0:T(8,128)S(1)}, u32[]{:S(2)}) copy-start(f32[4,2,64,256]{3,2,1,0:T(8,128)S(1)} %collective-permute-done.14.refs_10_) | copy-start | bytes 1572868
  121.7 9.9 %collective-permute-start.19 = (f32[4,1,64,256]{3,2,1,0:T(8,128)}, f32[4,1,64,256]{3,2,1,0:T(8,128)S(1)}, u32[]{:S(2)}, u32[]{:S(2)}) collective-permute-start(f32[4,1,64,256]{3,2,1,0:T(8,128)} %get-tuple-element.30.refs_14_), channel_id=1, source_target_pairs={{0,64},{32,96},{64,0},{96,32},{1,65},{33,97},{65,1},{97,33},{2,66}... | collective-permute-start | bytes 786440 | tf_op jit(solution)/shard_map/ppermute | solution.py:483
  123.2 8.3 %copy-start.8 = (f32[4,1,64,256]{3,2,1,0:T(8,128)}, f32[4,1,64,256]{3,2,1,0:T(8,128)S(1)}, u32[]{:S(2)}) copy-start(f32[4,1,64,256]{3,2,1,0:T(8,128)S(1)} %collective-permute-done.13.refs_8_) | copy-start | bytes 786436
  123.2 23.5 %collective-permute-start.18 = (f32[4,1,64,256]{3,2,1,0:T(8,128)}, f32[4,1,64,256]{3,2,1,0:T(8,128)}, u32[]{:S(2)}, u32[]{:S(2)}) collective-permute-start(f32[4,1,64,256]{3,2,1,0:T(8,128)} %get-tuple-element.30.refs_14_), channel_id=1, source_target_pairs={{0,32},{32,64},{64,96},{96,0},{1,33},{33,65},{65,97},{97,1},{2,34}... | collective-permute-start | bytes 786440 | tf_op jit(solution)/shard_map/ppermute | solution.py:483
  126.3 5.3 %copy-start.9 = (f32[4,1,64,256]{3,2,1,0:T(8,128)}, f32[4,1,64,256]{3,2,1,0:T(8,128)S(1)}, u32[]{:S(2)}) copy-start(f32[4,1,64,256]{3,2,1,0:T(8,128)S(1)} %collective-permute-done.12.refs_7_) | copy-start | bytes 786436
  126.3 20.5 %collective-permute-start.10 = (f32[2,2,64,256]{3,2,1,0:T(8,128)}, f32[2,2,64,256]{3,2,1,0:T(8,128)}, u32[]{:S(2)}, u32[]{:S(2)}) collective-permute-start(f32[2,2,64,256]{3,2,1,0:T(8,128)} %slice.31), channel_id=1, source_target_pairs={{0,24},{8,0},{16,8},{24,16},{1,25},{9,1},{17,9},{25,17},{2,26},{10... | collective-permute-start | bytes 786440 | tf_op jit(solution)/shard_map/ppermute | solution.py:483
  130.0 1.6 %copy-start.10 = (f32[4,1,64,256]{3,2,1,0:T(8,128)}, f32[4,1,64,256]{3,2,1,0:T(8,128)S(1)}, u32[]{:S(2)}) copy-start(f32[4,1,64,256]{3,2,1,0:T(8,128)S(1)} %collective-permute-done.11.refs_6_) | copy-start | bytes 786436
  130.0 16.8 %collective-permute-start.9 = (f32[2,2,64,256]{3,2,1,0:T(8,128)}, f32[2,2,64,256]{3,2,1,0:T(8,128)}, u32[]{:S(2)}, u32[]{:S(2)}) collective-permute-start(f32[2,2,64,256]{3,2,1,0:T(8,128)} %slice.30), channel_id=1, source_target_pairs={{0,8},{8,16},{16,24},{24,0},{1,9},{9,17},{17,25},{25,1},{2,10},{10... | collective-permute-start | bytes 786440 | tf_op jit(solution)/shard_map/ppermute | solution.py:483
  130.0 1.6 %copy-start.11 = (f32[4,1,64,256]{3,2,1,0:T(8,128)}, f32[4,1,64,256]{3,2,1,0:T(8,128)S(1)}, u32[]{:S(2)}) copy-start(f32[4,1,64,256]{3,2,1,0:T(8,128)S(1)} %collective-permute-done.20.refs_17_) | copy-start | bytes 786436
  130.0 16.7 %collective-permute-start.17 = (f32[2,2,64,256]{3,2,1,0:T(8,128)S(1)}, f32[2,2,64,256]{3,2,1,0:T(8,128)}, u32[]{:S(2)}, u32[]{:S(2)}) collective-permute-start(f32[2,2,64,256]{3,2,1,0:T(8,128)S(1)} %slice.33), channel_id=1, source_target_pairs={{0,96},{32,0},{64,32},{96,64},{1,97},{33,1},{65,33},{97,65},{2,98}... | collective-permute-start | bytes 786440 | tf_op jit(solution)/shard_map/ppermute | solution.py:483
  131.6 0.8 copy-start.12
  132.4 14.4 %collective-permute-start.16 = (f32[2,2,64,256]{3,2,1,0:T(8,128)S(1)}, f32[2,2,64,256]{3,2,1,0:T(8,128)}, u32[]{:S(2)}, u32[]{:S(2)}) collective-permute-start(f32[2,2,64,256]{3,2,1,0:T(8,128)S(1)} %slice.32), channel_id=1, source_target_pairs={{0,32},{32,64},{64,96},{96,0},{1,33},{33,65},{65,97},{97,1},{2,34}... | collective-permute-start | bytes 786440 | tf_op jit(solution)/shard_map/ppermute | solution.py:483
  136.3 11.3 %all-to-all-start.3 = ((f32[8,24,256]{2,1,0:T(8,128)}), f32[8,24,256]{2,1,0:T(8,128)S(1)}, u32[]{:S(2)}, u32[]{:S(2)}) async-start(f32[8,24,256]{2,1,0:T(8,128)} %get-tuple-element.31), calls=%async_computation.3 | async-start | bytes 393216 | tf_op jit(solution)/shard_map/all_to_all | solution.py:533
  147.6 0.7 copy-start.7

commit v5 on v4

--- a/solution.py
+++ b/solution.py
@@ -12,6 +12,7 @@
 BETA_TWO = 0.9
 LEARN = 0.001
 FS = ("z", "x")
+NEXT = (1, 2, 10, 11)
 TP = ("y", "c")
 
 
@@ -58,7 +59,12 @@
     at = pl.ds(pl.multiple_of(place_ref[2] * lanes, lanes), lanes)
     reads = [(factor_ref.at[r, :, at], block.at[pl.ds(r * rows, rows)]) for r in range(roles)]
     reads += [(log_ref.at[:, pl.ds(length - lanes, lanes)], last), (cot_ref, cot)]
-    finished(started(reads, read_sems))
+    reads = started(reads, read_sems)
+    finished(reads[:roles])
+    body, rest_of = pl.ds(0, roles * rows), pl.ds(roles * rows, lines - roles * rows)
+    pairs = [(block.at[body], out_ref.at[peer, body]) for peer in range(peers)]
+    writes = started(pairs, write_sems.at[pl.ds(0, peers)])
+    finished(reads[roles:])
     column = lax.broadcasted_iota(jnp.int32, (heads, lanes), 1)
     row = lax.broadcasted_iota(jnp.int32, (heads, lanes), 0)
     totals = jnp.sum(cot[...], axis=1, keepdims=True)
@@ -73,7 +79,8 @@
     tail = jnp.where(line == 1, lower.astype(jnp.float32), tail)
     tail = jnp.where(line == 2, rest, tail).astype(jnp.bfloat16)
     block[roles * rows :, :] = tail
-    finished(started([(block, out_ref.at[peer]) for peer in range(peers)], write_sems))
+    pairs = [(block.at[rest_of], out_ref.at[peer, rest_of]) for peer in range(peers)]
+    finished(writes + started(pairs, write_sems.at[pl.ds(peers, peers)]))
 
 
 def packed(place, factors, log_cache, cache_cot, peers):
@@ -91,7 +98,7 @@
             pltpu.VMEM((heads, length), jnp.float32),
             pltpu.VMEM((lines, lanes), jnp.bfloat16),
             pltpu.SemaphoreType.DMA((roles + 2,)),
-            pltpu.SemaphoreType.DMA((peers,)),
+            pltpu.SemaphoreType.DMA((2 * peers,)),
         ],
         compiler_params=room(8),
         cost_estimate=cost(10**6, 2 * 10**6),
@@ -145,7 +152,7 @@
     return pl.pallas_call(
         gate_kernel,
         out_shape=jax.ShapeDtypeStruct((heads, width), jnp.float32),
-        in_specs=[SMEM, HBM, HBM, HBM, HBM],
+        in_specs=[SMEM, HBM, HBM, pl.BlockSpec(memory_space=pl.ANY), HBM],
         out_specs=VMEM,
         scratch_shapes=[
             pltpu.VMEM((heads, length), jnp.float32),
@@ -157,52 +164,62 @@
         compiler_params=room(10),
         cost_estimate=cost(4 * 10**9, 4 * 10**6),
         name="gate_columns",
-    )(place, *held(pltpu.HBM, log_cache, cache_cot, ends, saved_input))
-
-
-def low_kernel(grad_ref, near_ref, far_ref, gate_ref, out_ref):
-    role = pl.program_id(0)
-    peers, rows, half = near_ref.shape
-    sides = [ref[...].reshape(peers * rows, half) for ref in (near_ref, far_ref)]
-    pieces = jnp.concatenate(sides, axis=1)
-    upper, lower = halves(grad_ref[0])
-    low = jnp.dot(upper, pieces, preferred_element_type=jnp.float32)
-    low = low + jnp.dot(lower, pieces, preferred_element_type=jnp.float32)
-    low = low.T
+    )(place, *held(pltpu.HBM, log_cache, cache_cot), ends, *held(pltpu.HBM, saved_input))
+
+
+def low_kernel(
+    grad_hbm, near_ref, far_ref, gate_ref, out_hbm, grad_ref, out_ref, tail_ref, read_sems,
+    write_sems,
+):
+    roles, width, depth = grad_ref.shape
+    peers, _, half = near_ref.shape
+    rows = depth // peers
     lines = half // peers
-    for side in range(2):
-        part = low[side * half : (side + 1) * half].reshape(peers, lines, -1)
-        start = pl.multiple_of(side * 3 * lines + role * lines, lines)
-        out_ref[:, pl.ds(start, lines), :] = part
-
-    @pl.when(role == 0)
-    def _():
-        out_ref[:, 6 * lines :, :] = jnp.zeros_like(out_ref[:, 6 * lines :, :])
-        for head in range(gate_ref.shape[0]):
-            out_ref[head, 6 * lines : 6 * lines + 1, :] = gate_ref[head : head + 1, :]
+    pairs = [(grad_hbm.at[role], grad_ref.at[role]) for role in range(roles)]
+    reads = started(pairs, read_sems)
+    tail_ref[...] = jnp.zeros_like(tail_ref)
+    for head in range(gate_ref.shape[0]):
+        tail_ref[head, 0:1, :] = gate_ref[head : head + 1, :]
+    writes = [(tail_ref, out_hbm.at[:, pl.ds(2 * roles * lines, tail_ref.shape[1])])]
+    writes = started(writes, write_sems.at[pl.ds(2 * roles, 1)])
+    for role in range(roles):
+        at = slice(role * rows, (role + 1) * rows)
+        sides = [ref[:, at, :].reshape(depth, half) for ref in (near_ref, far_ref)]
+        pieces = jnp.concatenate(sides, axis=1)
+        reads[role].wait()
+        both = jnp.concatenate(halves(grad_ref[role]), axis=0)
+        low = jnp.dot(both, pieces, preferred_element_type=jnp.float32)
+        low = (low[:width] + low[width:]).T
+        pairs = []
+        for side in range(2):
+            part = low[side * half : (side + 1) * half].reshape(peers, lines, width)
+            out_ref[side, role] = part
+            place = pl.ds((side * roles + role) * lines, lines)
+            pairs.append((out_ref.at[side, role], out_hbm.at[:, place]))
+        writes += started(pairs, write_sems.at[pl.ds(2 * role, 2)])
+    finished(writes)
 
 
 def low_parts(grad, near, far, gate):
     roles, width, depth = grad.shape
     peers, _, half = near.shape
-    rows = depth // peers
-    lines = 2 * roles * half // peers + 8
-    factor_spec = pl.BlockSpec((peers, rows, half), lambda r: (0, r, 0))
+    lines = half // peers
     return pl.pallas_call(
         low_kernel,
-        out_shape=pltpu.HBM((peers, lines, width), jnp.float32),
-        grid=(roles,),
-        in_specs=[
-            pl.BlockSpec((1, width, depth), lambda r: (r, 0, 0)),
-            factor_spec,
-            factor_spec,
-            pl.BlockSpec(gate.shape, lambda r: (0, 0)),
-        ],
-        out_specs=pl.BlockSpec((peers, lines, width), lambda r: (0, 0, 0)),
-        compiler_params=room(20),
+        out_shape=pltpu.HBM((peers, 2 * roles * lines + 8, width), jnp.float32),
+        in_specs=[HBM, VMEM, VMEM, VMEM],
+        out_specs=HBM,
+        scratch_shapes=[
+            pltpu.VMEM(grad.shape, jnp.float32),
+            pltpu.VMEM((2, roles, peers, lines, width), jnp.float32),
+            pltpu.VMEM((peers, 8, width), jnp.float32),
+            pltpu.SemaphoreType.DMA((roles,)),
+            pltpu.SemaphoreType.DMA((2 * roles + 1,)),
+        ],
+        compiler_params=room(22),
         cost_estimate=cost(4 * roles * width * depth * 2 * half, 11 * 10**6),
         name="low_parts",
-    )(*held(pltpu.HBM, grad, near, far), gate)
+    )(*held(pltpu.HBM, grad), near, far, gate)
 
 
 def sum_kernel(arrived_ref, out_ref, block, sems):
@@ -355,10 +372,13 @@
 
 
 def final_kernel(entries, place_ref, product_hbm, *refs):
-    pieces, inputs, outputs, refs = refs[:18], refs[18:23], refs[23:30], refs[30:]
-    product_ref, piece_refs, refs = refs[0], refs[1:19], refs[19:]
-    kept, made, (piece_sems, rest_sems, write_sems) = refs[:5], refs[5:12], refs[12:]
-    shared_ref, master_ref, gate_master_ref, gate_first_ref, gate_second_ref = kept
+    pieces, shared_ref, inputs, outputs, refs = refs[:18], refs[18], refs[19:23], refs[23:30], refs[30:]
+    count = 18 - len(NEXT)
+    product_ref, piece_refs, refs = refs[0], list(refs[1 : count + 1]), refs[count + 1 :]
+    kept, made, (piece_sems, rest_sems, write_sems) = refs[:4], refs[4:11], refs[11:]
+    for n in NEXT:
+        piece_refs.insert(n, pieces[n])
+    master_ref, gate_master_ref, gate_first_ref, gate_second_ref = kept
     step_ref, new_ref, copy_ref, *gate_refs = made
     heads = gate_master_ref.shape[0]
     roles, rows, width = master_ref.shape
@@ -367,7 +387,7 @@
     for role in range(roles):
         pairs = [(product_hbm.at[role], product_ref.at[role])]
         chosen, index = (range(0, 5), role) if role + 1 < roles else (range(5, 9), 0)
-        for n in [part * 9 + n for part in range(2) for n in chosen]:
+        for n in [part * 9 + n for part in range(2) for n in chosen if part * 9 + n not in NEXT]:
             pairs.append((pieces[n].at[:, index], piece_refs[n].at[:, index]))
         waits.append(started(pairs, piece_sems.at[role]))
     along = place_ref[3], place_ref[4]
@@ -425,20 +445,23 @@
         (gates[0].shape, jnp.float32),
         (gates[0].shape, jnp.float32),
     ]
-    inputs = (shared, master, *gates)
-    kept = [(a.shape, a.dtype) for a in (product, *pieces, *inputs)]
+    inputs = (master, *gates)
+    copied = [piece for n, piece in enumerate(pieces) if n not in NEXT]
+    kept = [(a.shape, a.dtype) for a in (product, *copied, *inputs)]
+    pieces = [a if n in NEXT else held(pltpu.HBM, a)[0] for n, a in enumerate(pieces)]
+    specs = [VMEM if n in NEXT else HBM for n in range(len(pieces))]
     dma = pltpu.SemaphoreType.DMA
     return pl.pallas_call(
         functools.partial(final_kernel, entries),
         out_shape=[pltpu.HBM(*out) for out in outs],
-        in_specs=[SMEM] + [HBM] * len(kept),
+        in_specs=[SMEM, HBM, *specs, VMEM] + [HBM] * len(inputs),
         out_specs=[HBM] * 7,
         scratch_shapes=[pltpu.VMEM(*a) for a in kept + outs]
-        + [dma((roles, 11)), dma((5,)), dma((roles * 3 + 4,))],
+        + [dma((roles, 11)), dma((4,)), dma((roles * 3 + 4,))],
         compiler_params=room(32),
         cost_estimate=cost(10**7, 16 * 10**6),
         name="finals",
-    )(place, *held(pltpu.HBM, product, *pieces, *inputs))
+    )(place, *held(pltpu.HBM, product), *pieces, shared, *held(pltpu.HBM, *inputs))
 
 
 def join_kernel(master_hbm, *refs):
@@ -514,8 +537,10 @@
     late = (first_late, second_late)
     ahead = [shift(side, axis, 1) for side, axis in zip(early, axes)]
     behind = [shift(side, axis, 3) for side, axis in zip(early, axes)]
-    opposite = [shift(side[:2], axis, 1) for side, axis in zip(ahead, axes)]
-    other = [shift(side[2:], axis, 3) for side, axis in zip(behind, axes)]
+    opposite = [side[:2] for side in ahead]
+    other = [side[2:] for side in behind]
+    opposite = [shift(side, axis, 1) for side, axis in zip(opposite, axes)]
+    other = [shift(side, axis, 3) for side, axis in zip(other, axes)]
     late = [[side] + [shift(side, axis, by) for by in (1, 2, 3)] for side, axis in zip(late, axes)]
     pieces = [
         [*group, *rest] for *group, rest in zip(early, ahead, behind, opposite, other, late)

time: 158 us -> 155 us (0.981)
  local copies, waits for them, and re-layouts: 5 us -> 3.06 us
    unnamed x40 -> x30, local copies, waits for them, and re-layouts: 3.35 us -> 1.44 us
where the time goes in v5:
time: 155 us; the launch traced here: 154 us
  starting transfers between devices  45.3 us (29%)
  Pallas kernels  32.4 us (21%)
  blocking collectives  31.5 us (20%)
  waiting for transfers between devices  25.1 us (16%)
  matrix products  15.6 us (10%)
  local copies, waits for them, and re-layouts  3.06 us (2%)
    all_to_all x1, blocking collectives, local(): near = lax.all_to_all(near, FS, split_axis=0, concat_axis=0, tiled=True)  31.5 us
    ppermute x20, starting transfers between devices, shift(): return lax.ppermute(x, axis, [(i, (i + by) % 4) for i in range(4)])  30.8 us
    ppermute x20, waiting for transfers between devices, shift(): return lax.ppermute(x, axis, [(i, (i + by) % 4) for i in range(4)])  24.2 us
    dot_general x1, matrix products, local(): jnp.einsum('td,rtw->rwd', saved_input, proj_cot, preferred_element_type=j...  15.6 us
    pallas_call x1, Pallas kernels, finals(): pl.pallas_call(functools.partial(final_kernel, entries), out_shape=[pltpu...  7.42 us
    pallas_call x1, Pallas kernels, low_parts(): pl.pallas_call(low_kernel, out_shape=pltpu.HBM((peers, 2 * roles * lines...  6.53 us
    all_to_all x1, starting transfers between devices, local(): lax.all_to_all(summed(arrived), FS, split_axis=0, concat_axis=0, tiled=True)  6.32 us
    pallas_call x1, Pallas kernels, products(): pl.pallas_call(product_kernel, out_shape=pltpu.HBM(shape, jnp.float32), i...  5.91 us
  transfers between devices with their start and end apart: 24, of which 8 were waited for; matrix products, arithmetic and copies ran while one was open for 11% of the time, Pallas kernels for 10%

profile of v5, /device:TPU:0, one launch (start us, length us, event | category | flops | bytes accessed | tf_op | source)
XLA Modules:
  0.0 154.0 jit_solution(1892096496063766380)
XLA Ops:
  0.7 0.1 stack.23.place_ref
  0.7 3.1 %packed.1 = bf16[16,400,128]{2,1,0:T(8,128)(2,1)} custom-call(s32[5]{0:T(128)S(1)} %stack.23.place_ref, bf16[3,128,256]{2,1,0:T(8,128)(2,1)} %factor_ref.1, f32[16,3072]{1,0:T(8,128)} %log_hbm.1, f32[16,3072]{1,0:T(8,128)} %cot_hbm.1), custom_call_target="tpu_custom_call" | custom-call | flops 1000000 | bytes 2000000 | tf_op jit(solution)/shard_map/packed/pallas_call | solution.py:91
  3.8 31.5 %all_to_all.20.ends_hbm.near_ref.near_hbm = bf16[16,400,128]{2,1,0:T(8,128)(2,1)S(1)} all-to-all(bf16[16,400,128]{2,1,0:T(8,128)(2,1)} %packed.1), channel_id=1, replica_groups=mesh['z'=4,'x'=4,'y'=4,'c'=2] {'z','x'}, dimensions={0} | all-to-all | bytes 3276800 | tf_op jit(solution)/shard_map/all_to_all | solution.py:529
  35.3 0.0 collective-permute-start
  35.4 15.6 %fusion.grad_hbm = f32[3,256,2048]{2,1,0:T(8,128)} fusion(bf16[3,3072,256]{2,1,0:T(8,128)(2,1)S(1)} %copy-done.14, bf16[3072,2048]{1,0:T(8,128)(2,1)} %input_hbm.1), kind=kOutput, calls=%fused_computation | convolution fusion | flops 9663676416 | bytes 23592960 | tf_op jit(solution)/shard_map/td,rtw->rwd/dot_general | solution.py:549
  50.9 2.5 %gate_columns.1.gate_ref = f32[16,256]{1,0:T(8,128)S(1)} custom-call(s32[5]{0:T(128)S(1)} %stack.23.place_ref, f32[16,3072]{1,0:T(8,128)} %log_hbm.1, f32[16,3072]{1,0:T(8,128)} %cot_hbm.1, bf16[16,400,128]{2,1,0:T(8,128)(2,1)S(1)} %all_to_all.20.ends_hbm.near_ref.near_hbm, bf16[3072,2048]{1,0:T(8,128)(2,1)} %input_hbm.1), custom_call_target="tpu_custom_call" | custom-call | flops 4000000000 | bytes 4000000 | tf_op jit(solution)/shard_map/gate_columns/pallas_call | solution.py:152
  53.5 0.0 copy-start.2
  53.5 6.5 %low_parts.1 = f32[16,56,256]{2,1,0:T(8,128)} custom-call(f32[3,256,2048]{2,1,0:T(8,128)} %fusion.grad_hbm, bf16[16,400,128]{2,1,0:T(8,128)(2,1)S(1)} %all_to_all.20.ends_hbm.near_ref.near_hbm, bf16[16,400,128]{2,1,0:T(8,128)(2,1)S(1)} %collective-permute-done.far_ref.far_hbm, f32[16,256]{1,0:T(8,128)S(1)} %gate_columns.1.gate_ref), custom_call_target="tpu_custom_call" | custom-call | flops 1610612736 | bytes 11000000 | tf_op jit(solution)/shard_map/low_parts/pallas_call | solution.py:207
  60.1 3.6 %all-to-all-start.1 = ((f32[16,56,256]{2,1,0:T(8,128)}), f32[16,56,256]{2,1,0:T(8,128)S(1)}, u32[]{:S(2)}, u32[]{:S(2)}) async-start(f32[16,56,256]{2,1,0:T(8,128)} %low_parts.1), calls=%async_computation.1 | async-start | bytes 1835008 | tf_op jit(solution)/shard_map/all_to_all | solution.py:552
  63.8 3.1 %collective-permute-start.6 = (f32[1,3,64,256]{3,2,1,0:T(8,128)S(1)}, f32[1,3,64,256]{3,2,1,0:T(8,128)S(1)}, u32[]{:S(2)}, u32[]{:S(2)}) collective-permute-start(f32[1,3,64,256]{3,2,1,0:T(8,128)S(1)} %get-tuple-element.41), channel_id=1, source_target_pairs={{0,24},{8,0},{16,8},{24,16},{1,25},{9,1},{17,9},{25,17},{2,26},{10... | collective-permute-start | bytes 589832 | tf_op jit(solution)/shard_map/ppermute | solution.py:506
  66.9 0.8 collective-permute-start.5
  67.7 0.9 collective-permute-start.4
  68.6 2.8 %collective-permute-start.3 = (f32[1,3,64,256]{3,2,1,0:T(8,128)S(1)}, f32[1,3,64,256]{3,2,1,0:T(8,128)S(1)}, u32[]{:S(2)}, u32[]{:S(2)}) collective-permute-start(f32[1,3,64,256]{3,2,1,0:T(8,128)S(1)} %get-tuple-element.42), channel_id=1, source_target_pairs={{0,96},{32,0},{64,32},{96,64},{1,97},{33,1},{65,33},{97,65},{2,98}... | collective-permute-start | bytes 589832 | tf_op jit(solution)/shard_map/ppermute | solution.py:506
  71.3 0.8 collective-permute-start.2
  72.1 9.2 %collective-permute-done.6.refs_5_ = f32[1,3,64,256]{3,2,1,0:T(8,128)S(1)} collective-permute-done((f32[1,3,64,256]{3,2,1,0:T(8,128)S(1)}, f32[1,3,64,256]{3,2,1,0:T(8,128)S(1)}, u32[]{:S(2)}, u32[]{:S(2)}) %collective-permute-start.6) | collective-permute-done | bytes 196640 | tf_op jit(solution)/shard_map/ppermute | solution.py:506
  81.3 1.5 collective-permute-start.1
  82.8 0.1 collective-permute-done.5.refs_4_
  82.9 2.8 %collective-permute-done.4.refs_3_ = f32[1,3,64,256]{3,2,1,0:T(8,128)S(1)} collective-permute-done((f32[1,3,64,256]{3,2,1,0:T(8,128)S(1)}, f32[1,3,64,256]{3,2,1,0:T(8,128)S(1)}, u32[]{:S(2)}, u32[]{:S(2)}) %collective-permute-start.4) | collective-permute-done | bytes 196640 | tf_op jit(solution)/shard_map/ppermute | solution.py:506
  85.7 0.0 copy-start.12
  85.7 2.5 %collective-permute-done.1.refs_0_ = f32[1,3,64,256]{3,2,1,0:T(8,128)S(1)} collective-permute-done((f32[1,3,64,256]{3,2,1,0:T(8,128)S(1)}, f32[1,3,64,256]{3,2,1,0:T(8,128)S(1)}, u32[]{:S(2)}, u32[]{:S(2)}) %collective-permute-start.1) | collective-permute-done | bytes 196640 | tf_op jit(solution)/shard_map/ppermute | solution.py:506
  88.2 0.0 copy-start.13
  88.2 0.7 copy-done.13
  88.9 2.4 %joined.1 = (f32[4,2,64,256]{3,2,1,0:T(8,128)}, f32[4,2,64,256]{3,2,1,0:T(8,128)}, f32[4,1,64,256]{3,2,1,0:T(8,128)}, f32[4,1,64,256]{3,2,1,0:T(8,128)}) custom-call(f32[3,128,256]{2,1,0:T(8,128)} %refs_19_.1, f32[1,3,64,256]{3,2,1,0:T(8,128)} %copy-done.13, f32[1,3,64,256]{3,2,1,0:T(8,128)} %copy-done.12, f32[1,3,64,256]{3,2,1,0:T(8,128)} %copy-done.11, ...), custom_call_target="tpu_custom_call" | custom-call | flops 1000000 | bytes 6000000 | tf_op jit(solution)/shard_map/joined/pallas_call | solution.py:489
  91.3 1.1 collective-permute-start.8
  92.4 1.0 collective-permute-start.7
  93.4 1.5 %collective-permute-start.15 = (f32[4,2,64,256]{3,2,1,0:T(8,128)}, f32[4,2,64,256]{3,2,1,0:T(8,128)S(1)}, u32[]{:S(2)}, u32[]{:S(2)}) collective-permute-start(f32[4,2,64,256]{3,2,1,0:T(8,128)} %get-tuple-element.29.refs_9_), channel_id=1, source_target_pairs={{0,96},{32,0},{64,32},{96,64},{1,97},{33,1},{65,33},{97,65},{2,98}... | collective-permute-start | bytes 1572872 | tf_op jit(solution)/shard_map/ppermute | solution.py:506
  94.9 0.5 collective-permute-start.14
  95.4 1.1 summed.1
  96.6 6.3 %all-to-all-start.2 = ((f32[16,56,256]{2,1,0:T(8,128)}), f32[16,56,256]{2,1,0:T(8,128)S(1)}, u32[]{:S(2)}, u32[]{:S(2)}) async-start(f32[16,56,256]{2,1,0:T(8,128)} %summed.1), calls=%async_computation.2 | async-start | bytes 1835008 | tf_op jit(solution)/shard_map/all_to_all | solution.py:553
  102.9 3.1 %collective-permute-start.13 = (f32[4,1,64,256]{3,2,1,0:T(8,128)}, f32[4,1,64,256]{3,2,1,0:T(8,128)S(1)}, u32[]{:S(2)}, u32[]{:S(2)}) collective-permute-start(f32[4,1,64,256]{3,2,1,0:T(8,128)} %get-tuple-element.28.refs_5_), channel_id=1, source_target_pairs={{0,24},{8,0},{16,8},{24,16},{1,25},{9,1},{17,9},{25,17},{2,26},{10... | collective-permute-start | bytes 786440 | tf_op jit(solution)/shard_map/ppermute | solution.py:506
  106.0 0.9 collective-permute-start.12
  106.9 2.8 %collective-permute-done.7.refs_1_ = f32[4,2,64,256]{3,2,1,0:T(8,128)S(1)} collective-permute-done((f32[4,2,64,256]{3,2,1,0:T(8,128)}, f32[4,2,64,256]{3,2,1,0:T(8,128)S(1)}, u32[]{:S(2)}, u32[]{:S(2)}) %collective-permute-start.7) | collective-permute-done | bytes 524320 | tf_op jit(solution)/shard_map/ppermute | solution.py:506
  109.7 0.3 collective-permute-start.11
  110.0 4.3 %collective-permute-done.15.refs_11_ = f32[4,2,64,256]{3,2,1,0:T(8,128)S(1)} collective-permute-done((f32[4,2,64,256]{3,2,1,0:T(8,128)}, f32[4,2,64,256]{3,2,1,0:T(8,128)S(1)}, u32[]{:S(2)}, u32[]{:S(2)}) %collective-permute-start.15) | collective-permute-done | bytes 524320 | tf_op jit(solution)/shard_map/ppermute | solution.py:506
  114.2 3.7 %collective-permute-start.20 = (f32[4,1,64,256]{3,2,1,0:T(8,128)}, f32[4,1,64,256]{3,2,1,0:T(8,128)S(1)}, u32[]{:S(2)}, u32[]{:S(2)}) collective-permute-start(f32[4,1,64,256]{3,2,1,0:T(8,128)} %get-tuple-element.30.refs_14_), channel_id=1, source_target_pairs={{0,96},{32,0},{64,32},{96,64},{1,97},{33,1},{65,33},{97,65},{2,98}... | collective-permute-start | bytes 786440 | tf_op jit(solution)/shard_map/ppermute | solution.py:506
  118.0 2.6 %collective-permute-done.14.refs_10_ = f32[4,2,64,256]{3,2,1,0:T(8,128)S(1)} collective-permute-done((f32[4,2,64,256]{3,2,1,0:T(8,128)}, f32[4,2,64,256]{3,2,1,0:T(8,128)S(1)}, u32[]{:S(2)}, u32[]{:S(2)}) %collective-permute-start.14) | collective-permute-done | bytes 524320 | tf_op jit(solution)/shard_map/ppermute | solution.py:506
  120.6 0.7 slice.31
  121.3 0.7 slice.30
  122.1 3.0 %collective-permute-start.18 = (f32[4,1,64,256]{3,2,1,0:T(8,128)}, f32[4,1,64,256]{3,2,1,0:T(8,128)}, u32[]{:S(2)}, u32[]{:S(2)}) collective-permute-start(f32[4,1,64,256]{3,2,1,0:T(8,128)} %get-tuple-element.30.refs_14_), channel_id=1, source_target_pairs={{0,32},{32,64},{64,96},{96,0},{1,33},{33,65},{65,97},{97,1},{2,34}... | collective-permute-start | bytes 786440 | tf_op jit(solution)/shard_map/ppermute | solution.py:506
  125.1 3.7 %collective-permute-start.10 = (f32[2,2,64,256]{3,2,1,0:T(8,128)}, f32[2,2,64,256]{3,2,1,0:T(8,128)}, u32[]{:S(2)}, u32[]{:S(2)}) collective-permute-start(f32[2,2,64,256]{3,2,1,0:T(8,128)} %slice.31), channel_id=1, source_target_pairs={{0,24},{8,0},{16,8},{24,16},{1,25},{9,1},{17,9},{25,17},{2,26},{10... | collective-permute-start | bytes 786440 | tf_op jit(solution)/shard_map/ppermute | solution.py:506
  128.9 1.7 %collective-permute-start.17 = (f32[2,2,64,256]{3,2,1,0:T(8,128)S(1)}, f32[2,2,64,256]{3,2,1,0:T(8,128)}, u32[]{:S(2)}, u32[]{:S(2)}) collective-permute-start(f32[2,2,64,256]{3,2,1,0:T(8,128)S(1)} %slice.33), channel_id=1, source_target_pairs={{0,96},{32,0},{64,32},{96,64},{1,97},{33,1},{65,33},{97,65},{2,98}... | collective-permute-start | bytes 786440 | tf_op jit(solution)/shard_map/ppermute | solution.py:506
  130.6 0.7 copy-done.7
  131.3 0.4 collective-permute-start.16
  131.7 3.4 %moments.1 = (f32[3,256,256]{2,1,0:T(8,128)}, f32[3,256,256]{2,1,0:T(8,128)}, bf16[3,256,256]{2,1,0:T(8,128)(2,1)}, bf16[3,256,256]{2,1,0:T(8,128)(2,1)}, f32[8,24,256]{2,1,0:T(8,128)}) custom-call(s32[5]{0:T(128)S(1)} %stack.23.place_ref, f32[16,56,256]{2,1,0:T(8,128)S(1)} %all-to-all-done.2.sums_ref, f32[3,256,256]{2,1,0:T(8,128)} %first_hbm.1, ...), custom_call_target="tpu_custom_call" | custom-call | flops 10000000 | bytes 6000000 | tf_op jit(solution)/shard_map/moments/pallas_call | solution.py:298
  135.1 4.5 %all-to-all-start.3 = ((f32[8,24,256]{2,1,0:T(8,128)}), f32[8,24,256]{2,1,0:T(8,128)S(1)}, u32[]{:S(2)}, u32[]{:S(2)}) async-start(f32[8,24,256]{2,1,0:T(8,128)} %get-tuple-element.31), calls=%async_computation.3 | async-start | bytes 393216 | tf_op jit(solution)/shard_map/all_to_all | solution.py:558
  139.6 5.9 %products.1.product_hbm = f32[3,2048,256]{2,1,0:T(8,128)} custom-call(bf16[16,400,128]{2,1,0:T(8,128)(2,1)} %copy-done, bf16[16,400,128]{2,1,0:T(8,128)(2,1)} %copy-done.1, bf16[3,256,256]{2,1,0:T(8,128)(2,1)} %get-tuple-element.25.upper_hbm, bf16[3,256,256]{2,1,0:T(8,128)(2,1)} %get-tuple-element.26.lower_hbm), custom_call_target="tpu_custom_call" | custom-call | flops 1610612736 | bytes 10000000 | tf_op jit(solution)/shard_map/products/pallas_call | solution.py:356
  145.6 0.8 all-to-all-done.3.refs_18_
  146.4 7.4 %finals.1 = (f32[3,128,256]{2,1,0:T(8,128)}, f32[3,128,256]{2,1,0:T(8,128)}, bf16[3,2048,256]{2,1,0:T(8,128)(2,1)}, f32[16,2048]{1,0:T(8,128)}, bf16[16,2048]{1,...) custom-call(s32[5]{0:T(128)S(1)} %stack.23.place_ref, f32[3,2048,256]{2,1,0:T(8,128)} %products.1.product_hbm, ...), custom_call_target="tpu_custom_call" | custom-call | flops 10000000 | bytes 16000000 | tf_op jit(solution)/shard_map/finals/pallas_call | solution.py:454
  (46 shorter events, 0.2 us)
Async XLA Ops:
  0.7 34.6 %copy-start.14 = (bf16[3,3072,256]{2,1,0:T(8,128)(2,1)S(1)}, bf16[3,3072,256]{2,1,0:T(8,128)(2,1)}, u32[]{:S(2)}) copy-start(bf16[3,3072,256]{2,1,0:T(8,128)(2,1)} %param.12) | copy-start | bytes 14155780
  35.3 18.2 %copy-start = (bf16[16,400,128]{2,1,0:T(8,128)(2,1)}, bf16[16,400,128]{2,1,0:T(8,128)(2,1)S(1)}, u32[]{:S(2)}) copy-start(bf16[16,400,128]{2,1,0:T(8,128)(2,1)S(1)} %all_to_all.20.ends_hbm.near_ref.near_hbm) | copy-start | bytes 4915204
  35.3 18.1 %collective-permute-start = (bf16[16,400,128]{2,1,0:T(8,128)(2,1)S(1)}, bf16[16,400,128]{2,1,0:T(8,128)(2,1)S(1)}, u32[]{:S(2)}, u32[]{:S(2)}) collective-permute-start(bf16[16,400,128]{2,1,0:T(8,128)(2,1)S(1)} %all_to_all.20.ends_hbm.near_ref.near_hbm), channel_id=1, source_target_pairs={{0,1},{1,0},{2,3},{3,2},{4,5},{5,4},{6,7},{7,6},{8,9},{9,8},{10,11... | collective-permute-start | bytes 4915208 | tf_op jit(solution)/shard_map/ppermute | solution.py:530
  53.5 10.2 %copy-start.2 = (f32[3,128,256]{2,1,0:T(8,128)S(1)}, f32[3,128,256]{2,1,0:T(8,128)}, u32[]{:S(2)}) copy-start(f32[3,128,256]{2,1,0:T(8,128)} %refs_19_.1) | copy-start | bytes 1179652
  53.5 6.6 %copy-start.1 = (bf16[16,400,128]{2,1,0:T(8,128)(2,1)}, bf16[16,400,128]{2,1,0:T(8,128)(2,1)S(1)}, u32[]{:S(2)}) copy-start(bf16[16,400,128]{2,1,0:T(8,128)(2,1)S(1)} %collective-permute-done.far_ref.far_hbm) | copy-start | bytes 4915204
  60.1 35.4 %all-to-all-start.1 = ((f32[16,56,256]{2,1,0:T(8,128)}), f32[16,56,256]{2,1,0:T(8,128)S(1)}, u32[]{:S(2)}, u32[]{:S(2)}) async-start(f32[16,56,256]{2,1,0:T(8,128)} %low_parts.1), calls=%async_computation.1 | async-start | bytes 1835008 | tf_op jit(solution)/shard_map/all_to_all | solution.py:552
  63.8 17.5 %collective-permute-start.6 = (f32[1,3,64,256]{3,2,1,0:T(8,128)S(1)}, f32[1,3,64,256]{3,2,1,0:T(8,128)S(1)}, u32[]{:S(2)}, u32[]{:S(2)}) collective-permute-start(f32[1,3,64,256]{3,2,1,0:T(8,128)S(1)} %get-tuple-element.41), channel_id=1, source_target_pairs={{0,24},{8,0},{16,8},{24,16},{1,25},{9,1},{17,9},{25,17},{2,26},{10... | collective-permute-start | bytes 589832 | tf_op jit(solution)/shard_map/ppermute | solution.py:506
  66.9 16.0 %collective-permute-start.5 = (f32[1,3,64,256]{3,2,1,0:T(8,128)S(1)}, f32[1,3,64,256]{3,2,1,0:T(8,128)S(1)}, u32[]{:S(2)}, u32[]{:S(2)}) collective-permute-start(f32[1,3,64,256]{3,2,1,0:T(8,128)S(1)} %get-tuple-element.41), channel_id=1, source_target_pairs={{0,16},{8,24},{16,0},{24,8},{1,17},{9,25},{17,1},{25,9},{2,18},{10... | collective-permute-start | bytes 589832 | tf_op jit(solution)/shard_map/ppermute | solution.py:506
  67.7 18.0 %collective-permute-start.4 = (f32[1,3,64,256]{3,2,1,0:T(8,128)S(1)}, f32[1,3,64,256]{3,2,1,0:T(8,128)S(1)}, u32[]{:S(2)}, u32[]{:S(2)}) collective-permute-start(f32[1,3,64,256]{3,2,1,0:T(8,128)S(1)} %get-tuple-element.41), channel_id=1, source_target_pairs={{0,8},{8,16},{16,24},{24,0},{1,9},{9,17},{17,25},{25,1},{2,10},{10... | collective-permute-start | bytes 589832 | tf_op jit(solution)/shard_map/ppermute | solution.py:506
  68.6 17.1 %collective-permute-start.3 = (f32[1,3,64,256]{3,2,1,0:T(8,128)S(1)}, f32[1,3,64,256]{3,2,1,0:T(8,128)S(1)}, u32[]{:S(2)}, u32[]{:S(2)}) collective-permute-start(f32[1,3,64,256]{3,2,1,0:T(8,128)S(1)} %get-tuple-element.42), channel_id=1, source_target_pairs={{0,96},{32,0},{64,32},{96,64},{1,97},{33,1},{65,33},{97,65},{2,98}... | collective-permute-start | bytes 589832 | tf_op jit(solution)/shard_map/ppermute | solution.py:506
  71.3 14.4 %collective-permute-start.2 = (f32[1,3,64,256]{3,2,1,0:T(8,128)S(1)}, f32[1,3,64,256]{3,2,1,0:T(8,128)S(1)}, u32[]{:S(2)}, u32[]{:S(2)}) collective-permute-start(f32[1,3,64,256]{3,2,1,0:T(8,128)S(1)} %get-tuple-element.42), channel_id=1, source_target_pairs={{0,64},{32,96},{64,0},{96,32},{1,65},{33,97},{65,1},{97,33},{2,66}... | collective-permute-start | bytes 589832 | tf_op jit(solution)/shard_map/ppermute | solution.py:506
  81.3 6.9 %copy-start.8 = (f32[1,3,64,256]{3,2,1,0:T(8,128)}, f32[1,3,64,256]{3,2,1,0:T(8,128)S(1)}, u32[]{:S(2)}) copy-start(f32[1,3,64,256]{3,2,1,0:T(8,128)S(1)} %collective-permute-done.6.refs_5_) | copy-start | bytes 589828
  81.3 6.9 %collective-permute-start.1 = (f32[1,3,64,256]{3,2,1,0:T(8,128)S(1)}, f32[1,3,64,256]{3,2,1,0:T(8,128)S(1)}, u32[]{:S(2)}, u32[]{:S(2)}) collective-permute-start(f32[1,3,64,256]{3,2,1,0:T(8,128)S(1)} %get-tuple-element.42), channel_id=1, source_target_pairs={{0,32},{32,64},{64,96},{96,0},{1,33},{33,65},{65,97},{97,1},{2,34}... | collective-permute-start | bytes 589832 | tf_op jit(solution)/shard_map/ppermute | solution.py:506
  82.9 5.3 %copy-start.9 = (f32[1,3,64,256]{3,2,1,0:T(8,128)}, f32[1,3,64,256]{3,2,1,0:T(8,128)S(1)}, u32[]{:S(2)}) copy-start(f32[1,3,64,256]{3,2,1,0:T(8,128)S(1)} %collective-permute-done.5.refs_4_) | copy-start | bytes 589828
  85.7 2.5 %copy-start.10 = (f32[1,3,64,256]{3,2,1,0:T(8,128)}, f32[1,3,64,256]{3,2,1,0:T(8,128)S(1)}, u32[]{:S(2)}) copy-start(f32[1,3,64,256]{3,2,1,0:T(8,128)S(1)} %collective-permute-done.4.refs_3_) | copy-start | bytes 589828
  85.7 2.5 %copy-start.11 = (f32[1,3,64,256]{3,2,1,0:T(8,128)}, f32[1,3,64,256]{3,2,1,0:T(8,128)S(1)}, u32[]{:S(2)}) copy-start(f32[1,3,64,256]{3,2,1,0:T(8,128)S(1)} %collective-permute-done.3.refs_2_) | copy-start | bytes 589828
  85.7 2.5 %copy-start.12 = (f32[1,3,64,256]{3,2,1,0:T(8,128)}, f32[1,3,64,256]{3,2,1,0:T(8,128)S(1)}, u32[]{:S(2)}) copy-start(f32[1,3,64,256]{3,2,1,0:T(8,128)S(1)} %collective-permute-done.2.refs_1_) | copy-start | bytes 589828
  88.2 0.7 copy-start.13
  91.3 14.7 %collective-permute-start.8 = (f32[4,2,64,256]{3,2,1,0:T(8,128)}, f32[4,2,64,256]{3,2,1,0:T(8,128)S(1)}, u32[]{:S(2)}, u32[]{:S(2)}) collective-permute-start(f32[4,2,64,256]{3,2,1,0:T(8,128)} %get-tuple-element.27.refs_0_), channel_id=1, source_target_pairs={{0,24},{8,0},{16,8},{24,16},{1,25},{9,1},{17,9},{25,17},{2,26},{10... | collective-permute-start | bytes 1572872 | tf_op jit(solution)/shard_map/ppermute | solution.py:506
  92.4 17.2 %collective-permute-start.7 = (f32[4,2,64,256]{3,2,1,0:T(8,128)}, f32[4,2,64,256]{3,2,1,0:T(8,128)S(1)}, u32[]{:S(2)}, u32[]{:S(2)}) collective-permute-start(f32[4,2,64,256]{3,2,1,0:T(8,128)} %get-tuple-element.27.refs_0_), channel_id=1, source_target_pairs={{0,8},{8,16},{16,24},{24,0},{1,9},{9,17},{17,25},{25,1},{2,10},{10... | collective-permute-start | bytes 1572872 | tf_op jit(solution)/shard_map/ppermute | solution.py:506
  93.4 20.9 %collective-permute-start.15 = (f32[4,2,64,256]{3,2,1,0:T(8,128)}, f32[4,2,64,256]{3,2,1,0:T(8,128)S(1)}, u32[]{:S(2)}, u32[]{:S(2)}) collective-permute-start(f32[4,2,64,256]{3,2,1,0:T(8,128)} %get-tuple-element.29.refs_9_), channel_id=1, source_target_pairs={{0,96},{32,0},{64,32},{96,64},{1,97},{33,1},{65,33},{97,65},{2,98}... | collective-permute-start | bytes 1572872 | tf_op jit(solution)/shard_map/ppermute | solution.py:506
  94.9 25.6 %collective-permute-start.14 = (f32[4,2,64,256]{3,2,1,0:T(8,128)}, f32[4,2,64,256]{3,2,1,0:T(8,128)S(1)}, u32[]{:S(2)}, u32[]{:S(2)}) collective-permute-start(f32[4,2,64,256]{3,2,1,0:T(8,128)} %get-tuple-element.29.refs_9_), channel_id=1, source_target_pairs={{0,32},{32,64},{64,96},{96,0},{1,33},{33,65},{65,97},{97,1},{2,34}... | collective-permute-start | bytes 1572872 | tf_op jit(solution)/shard_map/ppermute | solution.py:506
  96.6 35.2 %all-to-all-start.2 = ((f32[16,56,256]{2,1,0:T(8,128)}), f32[16,56,256]{2,1,0:T(8,128)S(1)}, u32[]{:S(2)}, u32[]{:S(2)}) async-start(f32[16,56,256]{2,1,0:T(8,128)} %summed.1), calls=%async_computation.2 | async-start | bytes 1835008 | tf_op jit(solution)/shard_map/all_to_all | solution.py:553
  102.9 19.2 %collective-permute-start.13 = (f32[4,1,64,256]{3,2,1,0:T(8,128)}, f32[4,1,64,256]{3,2,1,0:T(8,128)S(1)}, u32[]{:S(2)}, u32[]{:S(2)}) collective-permute-start(f32[4,1,64,256]{3,2,1,0:T(8,128)} %get-tuple-element.28.refs_5_), channel_id=1, source_target_pairs={{0,24},{8,0},{16,8},{24,16},{1,25},{9,1},{17,9},{25,17},{2,26},{10... | collective-permute-start | bytes 786440 | tf_op jit(solution)/shard_map/ppermute | solution.py:506
  106.0 19.1 %collective-permute-start.12 = (f32[4,1,64,256]{3,2,1,0:T(8,128)}, f32[4,1,64,256]{3,2,1,0:T(8,128)S(1)}, u32[]{:S(2)}, u32[]{:S(2)}) collective-permute-start(f32[4,1,64,256]{3,2,1,0:T(8,128)} %get-tuple-element.28.refs_5_), channel_id=1, source_target_pairs={{0,16},{8,24},{16,0},{24,8},{1,17},{9,25},{17,1},{25,9},{2,18},{10... | collective-permute-start | bytes 786440 | tf_op jit(solution)/shard_map/ppermute | solution.py:506
  109.7 19.2 %collective-permute-start.11 = (f32[4,1,64,256]{3,2,1,0:T(8,128)}, f32[4,1,64,256]{3,2,1,0:T(8,128)S(1)}, u32[]{:S(2)}, u32[]{:S(2)}) collective-permute-start(f32[4,1,64,256]{3,2,1,0:T(8,128)} %get-tuple-element.28.refs_5_), channel_id=1, source_target_pairs={{0,8},{8,16},{16,24},{24,0},{1,9},{9,17},{17,25},{25,1},{2,10},{10... | collective-permute-start | bytes 786440 | tf_op jit(solution)/shard_map/ppermute | solution.py:506
  114.2 14.6 %collective-permute-start.20 = (f32[4,1,64,256]{3,2,1,0:T(8,128)}, f32[4,1,64,256]{3,2,1,0:T(8,128)S(1)}, u32[]{:S(2)}, u32[]{:S(2)}) collective-permute-start(f32[4,1,64,256]{3,2,1,0:T(8,128)} %get-tuple-element.30.refs_14_), channel_id=1, source_target_pairs={{0,96},{32,0},{64,32},{96,64},{1,97},{33,1},{65,33},{97,65},{2,98}... | collective-permute-start | bytes 786440 | tf_op jit(solution)/shard_map/ppermute | solution.py:506
  120.6 10.0 %collective-permute-start.19 = (f32[4,1,64,256]{3,2,1,0:T(8,128)}, f32[4,1,64,256]{3,2,1,0:T(8,128)S(1)}, u32[]{:S(2)}, u32[]{:S(2)}) collective-permute-start(f32[4,1,64,256]{3,2,1,0:T(8,128)} %get-tuple-element.30.refs_14_), channel_id=1, source_target_pairs={{0,64},{32,96},{64,0},{96,32},{1,65},{33,97},{65,1},{97,33},{2,66}... | collective-permute-start | bytes 786440 | tf_op jit(solution)/shard_map/ppermute | solution.py:506
  122.1 8.4 %copy-start.3 = (f32[4,1,64,256]{3,2,1,0:T(8,128)}, f32[4,1,64,256]{3,2,1,0:T(8,128)S(1)}, u32[]{:S(2)}) copy-start(f32[4,1,64,256]{3,2,1,0:T(8,128)S(1)} %collective-permute-done.13.refs_8_) | copy-start | bytes 786436
  122.1 23.4 %collective-permute-start.18 = (f32[4,1,64,256]{3,2,1,0:T(8,128)}, f32[4,1,64,256]{3,2,1,0:T(8,128)}, u32[]{:S(2)}, u32[]{:S(2)}) collective-permute-start(f32[4,1,64,256]{3,2,1,0:T(8,128)} %get-tuple-element.30.refs_14_), channel_id=1, source_target_pairs={{0,32},{32,64},{64,96},{96,0},{1,33},{33,65},{65,97},{97,1},{2,34}... | collective-permute-start | bytes 786440 | tf_op jit(solution)/shard_map/ppermute | solution.py:506
  125.1 5.5 %copy-start.4 = (f32[4,1,64,256]{3,2,1,0:T(8,128)}, f32[4,1,64,256]{3,2,1,0:T(8,128)S(1)}, u32[]{:S(2)}) copy-start(f32[4,1,64,256]{3,2,1,0:T(8,128)S(1)} %collective-permute-done.12.refs_7_) | copy-start | bytes 786436
  125.1 20.4 %collective-permute-start.10 = (f32[2,2,64,256]{3,2,1,0:T(8,128)}, f32[2,2,64,256]{3,2,1,0:T(8,128)}, u32[]{:S(2)}, u32[]{:S(2)}) collective-permute-start(f32[2,2,64,256]{3,2,1,0:T(8,128)} %slice.31), channel_id=1, source_target_pairs={{0,24},{8,0},{16,8},{24,16},{1,25},{9,1},{17,9},{25,17},{2,26},{10... | collective-permute-start | bytes 786440 | tf_op jit(solution)/shard_map/ppermute | solution.py:506
  128.8 1.7 %copy-start.5 = (f32[4,1,64,256]{3,2,1,0:T(8,128)}, f32[4,1,64,256]{3,2,1,0:T(8,128)S(1)}, u32[]{:S(2)}) copy-start(f32[4,1,64,256]{3,2,1,0:T(8,128)S(1)} %collective-permute-done.11.refs_6_) | copy-start | bytes 786436
  128.8 16.7 %collective-permute-start.9 = (f32[2,2,64,256]{3,2,1,0:T(8,128)}, f32[2,2,64,256]{3,2,1,0:T(8,128)}, u32[]{:S(2)}, u32[]{:S(2)}) collective-permute-start(f32[2,2,64,256]{3,2,1,0:T(8,128)} %slice.30), channel_id=1, source_target_pairs={{0,8},{8,16},{16,24},{24,0},{1,9},{9,17},{17,25},{25,1},{2,10},{10... | collective-permute-start | bytes 786440 | tf_op jit(solution)/shard_map/ppermute | solution.py:506
  128.9 1.7 %copy-start.6 = (f32[4,1,64,256]{3,2,1,0:T(8,128)}, f32[4,1,64,256]{3,2,1,0:T(8,128)S(1)}, u32[]{:S(2)}) copy-start(f32[4,1,64,256]{3,2,1,0:T(8,128)S(1)} %collective-permute-done.20.refs_17_) | copy-start | bytes 786436
  128.9 16.7 %collective-permute-start.17 = (f32[2,2,64,256]{3,2,1,0:T(8,128)S(1)}, f32[2,2,64,256]{3,2,1,0:T(8,128)}, u32[]{:S(2)}, u32[]{:S(2)}) collective-permute-start(f32[2,2,64,256]{3,2,1,0:T(8,128)S(1)} %slice.33), channel_id=1, source_target_pairs={{0,96},{32,0},{64,32},{96,64},{1,97},{33,1},{65,33},{97,65},{2,98}... | collective-permute-start | bytes 786440 | tf_op jit(solution)/shard_map/ppermute | solution.py:506
  130.6 0.7 copy-start.7
  131.3 14.3 %collective-permute-start.16 = (f32[2,2,64,256]{3,2,1,0:T(8,128)S(1)}, f32[2,2,64,256]{3,2,1,0:T(8,128)}, u32[]{:S(2)}, u32[]{:S(2)}) collective-permute-start(f32[2,2,64,256]{3,2,1,0:T(8,128)S(1)} %slice.32), channel_id=1, source_target_pairs={{0,32},{32,64},{64,96},{96,0},{1,33},{33,65},{65,97},{97,1},{2,34}... | collective-permute-start | bytes 786440 | tf_op jit(solution)/shard_map/ppermute | solution.py:506
  135.1 11.3 %all-to-all-start.3 = ((f32[8,24,256]{2,1,0:T(8,128)}), f32[8,24,256]{2,1,0:T(8,128)S(1)}, u32[]{:S(2)}, u32[]{:S(2)}) async-start(f32[8,24,256]{2,1,0:T(8,128)} %get-tuple-element.31), calls=%async_computation.3 | async-start | bytes 393216 | tf_op jit(solution)/shard_map/all_to_all | solution.py:558

commit v6 on v5

--- a/solution.py
+++ b/solution.py
@@ -168,15 +168,12 @@
 
 
 def low_kernel(
-    grad_hbm, near_ref, far_ref, gate_ref, out_hbm, grad_ref, out_ref, tail_ref, read_sems,
-    write_sems,
+    grad_ref, near_ref, far_ref, gate_ref, out_hbm, out_ref, tail_ref, write_sems,
 ):
     roles, width, depth = grad_ref.shape
     peers, _, half = near_ref.shape
     rows = depth // peers
     lines = half // peers
-    pairs = [(grad_hbm.at[role], grad_ref.at[role]) for role in range(roles)]
-    reads = started(pairs, read_sems)
     tail_ref[...] = jnp.zeros_like(tail_ref)
     for head in range(gate_ref.shape[0]):
         tail_ref[head, 0:1, :] = gate_ref[head : head + 1, :]
@@ -186,7 +183,6 @@
         at = slice(role * rows, (role + 1) * rows)
         sides = [ref[:, at, :].reshape(depth, half) for ref in (near_ref, far_ref)]
         pieces = jnp.concatenate(sides, axis=1)
-        reads[role].wait()
         both = jnp.concatenate(halves(grad_ref[role]), axis=0)
         low = jnp.dot(both, pieces, preferred_element_type=jnp.float32)
         low = (low[:width] + low[width:]).T
@@ -207,19 +203,17 @@
     return pl.pallas_call(
         low_kernel,
         out_shape=pltpu.HBM((peers, 2 * roles * lines + 8, width), jnp.float32),
-        in_specs=[HBM, VMEM, VMEM, VMEM],
+        in_specs=[VMEM, VMEM, VMEM, VMEM],
         out_specs=HBM,
         scratch_shapes=[
-            pltpu.VMEM(grad.shape, jnp.float32),
             pltpu.VMEM((2, roles, peers, lines, width), jnp.float32),
             pltpu.VMEM((peers, 8, width), jnp.float32),
-            pltpu.SemaphoreType.DMA((roles,)),
             pltpu.SemaphoreType.DMA((2 * roles + 1,)),
         ],
         compiler_params=room(22),
         cost_estimate=cost(4 * roles * width * depth * 2 * half, 11 * 10**6),
         name="low_parts",
-    )(*held(pltpu.HBM, grad), near, far, gate)
+    )(grad, near, far, gate)
 
 
 def sum_kernel(arrived_ref, out_ref, block, sems):

time: 155 us -> 150 us (0.968)
  Pallas kernels: 32.4 us -> 28.7 us
  matrix products: 15.6 us -> 13.9 us
    pallas_call x1, Pallas kernels: 6.53 us -> 2.83 us  [low_parts(): pl.pallas_call(low_kernel, out_shape=pltpu.HBM((peers, 2 * roles * lines...]
    dot_general x1, matrix products: 15.6 us -> 13.9 us  [local(): jnp.einsum('td,rtw->rwd', saved_input, proj_cot, preferred_element_type=j...]
  transfers between devices with their start and end apart: 24 -> 24, of which waited for: 8 -> 8; matrix products, arithmetic and copies ran while one was open for 11% -> 10% of each run, Pallas kernels for 10% -> 10%
where the time goes in v6:
time: 150 us; the launch traced here: 149 us
  starting transfers between devices  45.2 us (30%)
  blocking collectives  31.5 us (21%)
  Pallas kernels  28.7 us (19%)
  waiting for transfers between devices  25.1 us (17%)
  matrix products  13.9 us (9%)
  local copies, waits for them, and re-layouts  3.05 us (2%)
    all_to_all x1, blocking collectives, local(): near = lax.all_to_all(near, FS, split_axis=0, concat_axis=0, tiled=True)  31.5 us
    ppermute x20, starting transfers between devices, shift(): return lax.ppermute(x, axis, [(i, (i + by) % 4) for i in range(4)])  30.8 us
    ppermute x20, waiting for transfers between devices, shift(): return lax.ppermute(x, axis, [(i, (i + by) % 4) for i in range(4)])  24.3 us
    dot_general x1, matrix products, local(): jnp.einsum('td,rtw->rwd', saved_input, proj_cot, preferred_element_type=j...  13.9 us
    pallas_call x1, Pallas kernels, finals(): pl.pallas_call(functools.partial(final_kernel, entries), out_shape=[pltpu...  7.42 us
    all_to_all x1, starting transfers between devices, local(): lax.all_to_all(summed(arrived), FS, split_axis=0, concat_axis=0, tiled=True)  6.32 us
    pallas_call x1, Pallas kernels, products(): pl.pallas_call(product_kernel, out_shape=pltpu.HBM(shape, jnp.float32), i...  5.96 us
    all_to_all x1, starting transfers between devices, local(): shared = lax.all_to_all(shared, TP, split_axis=0, concat_axis=0, tiled=True)  4.48 us
  transfers between devices with their start and end apart: 24, of which 8 were waited for; matrix products, arithmetic and copies ran while one was open for 10% of the time, Pallas kernels for 10%

profile of v6, /device:TPU:0, one launch (start us, length us, event | category | flops | bytes accessed | tf_op | source)
XLA Modules:
  0.0 148.6 jit_solution(8758469550731660038)
XLA Ops:
  0.7 0.1 stack.23.place_ref
  0.7 3.1 %packed.1 = bf16[16,400,128]{2,1,0:T(8,128)(2,1)} custom-call(s32[5]{0:T(128)S(1)} %stack.23.place_ref, bf16[3,128,256]{2,1,0:T(8,128)(2,1)} %factor_ref.1, f32[16,3072]{1,0:T(8,128)} %log_hbm.1, f32[16,3072]{1,0:T(8,128)} %cot_hbm.1), custom_call_target="tpu_custom_call" | custom-call | flops 1000000 | bytes 2000000 | tf_op jit(solution)/shard_map/packed/pallas_call | solution.py:91
  3.8 31.5 %all_to_all.20.ends_hbm.near_ref.near_hbm = bf16[16,400,128]{2,1,0:T(8,128)(2,1)S(1)} all-to-all(bf16[16,400,128]{2,1,0:T(8,128)(2,1)} %packed.1), channel_id=1, replica_groups=mesh['z'=4,'x'=4,'y'=4,'c'=2] {'z','x'}, dimensions={0} | all-to-all | bytes 3276800 | tf_op jit(solution)/shard_map/all_to_all | solution.py:523
  35.3 0.0 collective-permute-start
  35.4 13.9 %fusion.grad_ref = f32[3,256,2048]{2,1,0:T(8,128)S(1)} fusion(bf16[3,3072,256]{2,1,0:T(8,128)(2,1)S(1)} %copy-done.14, bf16[3072,2048]{1,0:T(8,128)(2,1)} %input_hbm.1), kind=kOutput, calls=%fused_computation | convolution fusion | flops 9663676416 | bytes 23592960 | tf_op jit(solution)/shard_map/td,rtw->rwd/dot_general | solution.py:543
  49.3 2.5 %gate_columns.1.gate_ref = f32[16,256]{1,0:T(8,128)S(1)} custom-call(s32[5]{0:T(128)S(1)} %stack.23.place_ref, f32[16,3072]{1,0:T(8,128)} %log_hbm.1, f32[16,3072]{1,0:T(8,128)} %cot_hbm.1, bf16[16,400,128]{2,1,0:T(8,128)(2,1)S(1)} %all_to_all.20.ends_hbm.near_ref.near_hbm, bf16[3072,2048]{1,0:T(8,128)(2,1)} %input_hbm.1), custom_call_target="tpu_custom_call" | custom-call | flops 4000000000 | bytes 4000000 | tf_op jit(solution)/shard_map/gate_columns/pallas_call | solution.py:152
  51.8 0.0 copy-start.2
  51.9 2.8 %low_parts.1 = f32[16,56,256]{2,1,0:T(8,128)} custom-call(f32[3,256,2048]{2,1,0:T(8,128)S(1)} %fusion.grad_ref, bf16[16,400,128]{2,1,0:T(8,128)(2,1)S(1)} %all_to_all.20.ends_hbm.near_ref.near_hbm, bf16[16,400,128]{2,1,0:T(8,128)(2,1)S(1)} %collective-permute-done.far_ref.far_hbm, f32[16,256]{1,0:T(8,128)S(1)} %gate_columns.1.gate_ref), custom_call_target="tpu_custom_call" | custom-call | flops 1610612736 | bytes 11000000 | tf_op jit(solution)/shard_map/low_parts/pallas_call | solution.py:203
  54.7 3.6 %all-to-all-start.1 = ((f32[16,56,256]{2,1,0:T(8,128)}), f32[16,56,256]{2,1,0:T(8,128)S(1)}, u32[]{:S(2)}, u32[]{:S(2)}) async-start(f32[16,56,256]{2,1,0:T(8,128)} %low_parts.1), calls=%async_computation.1 | async-start | bytes 1835008 | tf_op jit(solution)/shard_map/all_to_all | solution.py:546
  58.4 3.1 %collective-permute-start.6 = (f32[1,3,64,256]{3,2,1,0:T(8,128)S(1)}, f32[1,3,64,256]{3,2,1,0:T(8,128)S(1)}, u32[]{:S(2)}, u32[]{:S(2)}) collective-permute-start(f32[1,3,64,256]{3,2,1,0:T(8,128)S(1)} %get-tuple-element.41), channel_id=1, source_target_pairs={{0,24},{8,0},{16,8},{24,16},{1,25},{9,1},{17,9},{25,17},{2,26},{10... | collective-permute-start | bytes 589832 | tf_op jit(solution)/shard_map/ppermute | solution.py:500
  61.5 0.8 collective-permute-start.5
  62.4 0.9 collective-permute-start.4
  63.2 2.8 %collective-permute-start.3 = (f32[1,3,64,256]{3,2,1,0:T(8,128)S(1)}, f32[1,3,64,256]{3,2,1,0:T(8,128)S(1)}, u32[]{:S(2)}, u32[]{:S(2)}) collective-permute-start(f32[1,3,64,256]{3,2,1,0:T(8,128)S(1)} %get-tuple-element.42), channel_id=1, source_target_pairs={{0,96},{32,0},{64,32},{96,64},{1,97},{33,1},{65,33},{97,65},{2,98}... | collective-permute-start | bytes 589832 | tf_op jit(solution)/shard_map/ppermute | solution.py:500
  66.0 0.8 collective-permute-start.2
  66.8 9.2 %collective-permute-done.6.refs_5_ = f32[1,3,64,256]{3,2,1,0:T(8,128)S(1)} collective-permute-done((f32[1,3,64,256]{3,2,1,0:T(8,128)S(1)}, f32[1,3,64,256]{3,2,1,0:T(8,128)S(1)}, u32[]{:S(2)}, u32[]{:S(2)}) %collective-permute-start.6) | collective-permute-done | bytes 196640 | tf_op jit(solution)/shard_map/ppermute | solution.py:500
  76.0 1.5 %collective-permute-start.1 = (f32[1,3,64,256]{3,2,1,0:T(8,128)S(1)}, f32[1,3,64,256]{3,2,1,0:T(8,128)S(1)}, u32[]{:S(2)}, u32[]{:S(2)}) collective-permute-start(f32[1,3,64,256]{3,2,1,0:T(8,128)S(1)} %get-tuple-element.42), channel_id=1, source_target_pairs={{0,32},{32,64},{64,96},{96,0},{1,33},{33,65},{65,97},{97,1},{2,34}... | collective-permute-start | bytes 589832 | tf_op jit(solution)/shard_map/ppermute | solution.py:500
  77.5 0.1 collective-permute-done.5.refs_4_
  77.5 2.8 %collective-permute-done.4.refs_3_ = f32[1,3,64,256]{3,2,1,0:T(8,128)S(1)} collective-permute-done((f32[1,3,64,256]{3,2,1,0:T(8,128)S(1)}, f32[1,3,64,256]{3,2,1,0:T(8,128)S(1)}, u32[]{:S(2)}, u32[]{:S(2)}) %collective-permute-start.4) | collective-permute-done | bytes 196640 | tf_op jit(solution)/shard_map/ppermute | solution.py:500
  80.4 0.0 copy-start.12
  80.4 2.5 %collective-permute-done.1.refs_0_ = f32[1,3,64,256]{3,2,1,0:T(8,128)S(1)} collective-permute-done((f32[1,3,64,256]{3,2,1,0:T(8,128)S(1)}, f32[1,3,64,256]{3,2,1,0:T(8,128)S(1)}, u32[]{:S(2)}, u32[]{:S(2)}) %collective-permute-start.1) | collective-permute-done | bytes 196640 | tf_op jit(solution)/shard_map/ppermute | solution.py:500
  82.9 0.0 copy-start.13
  82.9 0.7 copy-done.13
  83.6 2.4 %joined.1 = (f32[4,2,64,256]{3,2,1,0:T(8,128)}, f32[4,2,64,256]{3,2,1,0:T(8,128)}, f32[4,1,64,256]{3,2,1,0:T(8,128)}, f32[4,1,64,256]{3,2,1,0:T(8,128)}) custom-call(f32[3,128,256]{2,1,0:T(8,128)} %refs_19_.1, f32[1,3,64,256]{3,2,1,0:T(8,128)} %copy-done.13, f32[1,3,64,256]{3,2,1,0:T(8,128)} %copy-done.12, f32[1,3,64,256]{3,2,1,0:T(8,128)} %copy-done.11, ...), custom_call_target="tpu_custom_call" | custom-call | flops 1000000 | bytes 6000000 | tf_op jit(solution)/shard_map/joined/pallas_call | solution.py:483
  86.0 1.1 collective-permute-start.8
  87.1 1.0 collective-permute-start.7
  88.1 1.5 %collective-permute-start.15 = (f32[4,2,64,256]{3,2,1,0:T(8,128)}, f32[4,2,64,256]{3,2,1,0:T(8,128)S(1)}, u32[]{:S(2)}, u32[]{:S(2)}) collective-permute-start(f32[4,2,64,256]{3,2,1,0:T(8,128)} %get-tuple-element.29.refs_9_), channel_id=1, source_target_pairs={{0,96},{32,0},{64,32},{96,64},{1,97},{33,1},{65,33},{97,65},{2,98}... | collective-permute-start | bytes 1572872 | tf_op jit(solution)/shard_map/ppermute | solution.py:500
  89.6 0.5 collective-permute-start.14
  90.1 1.1 summed.1
  91.2 6.3 %all-to-all-start.2 = ((f32[16,56,256]{2,1,0:T(8,128)}), f32[16,56,256]{2,1,0:T(8,128)S(1)}, u32[]{:S(2)}, u32[]{:S(2)}) async-start(f32[16,56,256]{2,1,0:T(8,128)} %summed.1), calls=%async_computation.2 | async-start | bytes 1835008 | tf_op jit(solution)/shard_map/all_to_all | solution.py:547
  97.6 3.1 %collective-permute-start.13 = (f32[4,1,64,256]{3,2,1,0:T(8,128)}, f32[4,1,64,256]{3,2,1,0:T(8,128)S(1)}, u32[]{:S(2)}, u32[]{:S(2)}) collective-permute-start(f32[4,1,64,256]{3,2,1,0:T(8,128)} %get-tuple-element.28.refs_5_), channel_id=1, source_target_pairs={{0,24},{8,0},{16,8},{24,16},{1,25},{9,1},{17,9},{25,17},{2,26},{10... | collective-permute-start | bytes 786440 | tf_op jit(solution)/shard_map/ppermute | solution.py:500
  100.7 0.9 collective-permute-start.12
  101.6 2.8 %collective-permute-done.7.refs_1_ = f32[4,2,64,256]{3,2,1,0:T(8,128)S(1)} collective-permute-done((f32[4,2,64,256]{3,2,1,0:T(8,128)}, f32[4,2,64,256]{3,2,1,0:T(8,128)S(1)}, u32[]{:S(2)}, u32[]{:S(2)}) %collective-permute-start.7) | collective-permute-done | bytes 524320 | tf_op jit(solution)/shard_map/ppermute | solution.py:500
  104.4 0.3 collective-permute-start.11
  104.7 4.3 %collective-permute-done.15.refs_11_ = f32[4,2,64,256]{3,2,1,0:T(8,128)S(1)} collective-permute-done((f32[4,2,64,256]{3,2,1,0:T(8,128)}, f32[4,2,64,256]{3,2,1,0:T(8,128)S(1)}, u32[]{:S(2)}, u32[]{:S(2)}) %collective-permute-start.15) | collective-permute-done | bytes 524320 | tf_op jit(solution)/shard_map/ppermute | solution.py:500
  108.9 3.7 %collective-permute-start.20 = (f32[4,1,64,256]{3,2,1,0:T(8,128)}, f32[4,1,64,256]{3,2,1,0:T(8,128)S(1)}, u32[]{:S(2)}, u32[]{:S(2)}) collective-permute-start(f32[4,1,64,256]{3,2,1,0:T(8,128)} %get-tuple-element.30.refs_14_), channel_id=1, source_target_pairs={{0,96},{32,0},{64,32},{96,64},{1,97},{33,1},{65,33},{97,65},{2,98}... | collective-permute-start | bytes 786440 | tf_op jit(solution)/shard_map/ppermute | solution.py:500
  112.7 2.6 %collective-permute-done.14.refs_10_ = f32[4,2,64,256]{3,2,1,0:T(8,128)S(1)} collective-permute-done((f32[4,2,64,256]{3,2,1,0:T(8,128)}, f32[4,2,64,256]{3,2,1,0:T(8,128)S(1)}, u32[]{:S(2)}, u32[]{:S(2)}) %collective-permute-start.14) | collective-permute-done | bytes 524320 | tf_op jit(solution)/shard_map/ppermute | solution.py:500
  115.3 0.7 slice.31
  116.0 0.7 slice.30
  116.8 3.0 %collective-permute-start.18 = (f32[4,1,64,256]{3,2,1,0:T(8,128)}, f32[4,1,64,256]{3,2,1,0:T(8,128)}, u32[]{:S(2)}, u32[]{:S(2)}) collective-permute-start(f32[4,1,64,256]{3,2,1,0:T(8,128)} %get-tuple-element.30.refs_14_), channel_id=1, source_target_pairs={{0,32},{32,64},{64,96},{96,0},{1,33},{33,65},{65,97},{97,1},{2,34}... | collective-permute-start | bytes 786440 | tf_op jit(solution)/shard_map/ppermute | solution.py:500
  119.8 3.7 %collective-permute-start.10 = (f32[2,2,64,256]{3,2,1,0:T(8,128)}, f32[2,2,64,256]{3,2,1,0:T(8,128)}, u32[]{:S(2)}, u32[]{:S(2)}) collective-permute-start(f32[2,2,64,256]{3,2,1,0:T(8,128)} %slice.31), channel_id=1, source_target_pairs={{0,24},{8,0},{16,8},{24,16},{1,25},{9,1},{17,9},{25,17},{2,26},{10... | collective-permute-start | bytes 786440 | tf_op jit(solution)/shard_map/ppermute | solution.py:500
  123.5 1.7 %collective-permute-start.17 = (f32[2,2,64,256]{3,2,1,0:T(8,128)S(1)}, f32[2,2,64,256]{3,2,1,0:T(8,128)}, u32[]{:S(2)}, u32[]{:S(2)}) collective-permute-start(f32[2,2,64,256]{3,2,1,0:T(8,128)S(1)} %slice.33), channel_id=1, source_target_pairs={{0,96},{32,0},{64,32},{96,64},{1,97},{33,1},{65,33},{97,65},{2,98}... | collective-permute-start | bytes 786440 | tf_op jit(solution)/shard_map/ppermute | solution.py:500
  125.3 0.7 copy-done.7
  126.0 0.4 collective-permute-start.16
  126.4 3.4 %moments.1 = (f32[3,256,256]{2,1,0:T(8,128)}, f32[3,256,256]{2,1,0:T(8,128)}, bf16[3,256,256]{2,1,0:T(8,128)(2,1)}, bf16[3,256,256]{2,1,0:T(8,128)(2,1)}, f32[8,24,256]{2,1,0:T(8,128)}) custom-call(s32[5]{0:T(128)S(1)} %stack.23.place_ref, f32[16,56,256]{2,1,0:T(8,128)S(1)} %all-to-all-done.2.sums_ref, f32[3,256,256]{2,1,0:T(8,128)} %first_hbm.1, ...), custom_call_target="tpu_custom_call" | custom-call | flops 10000000 | bytes 6000000 | tf_op jit(solution)/shard_map/moments/pallas_call | solution.py:292
  129.8 4.5 %all-to-all-start.3 = ((f32[8,24,256]{2,1,0:T(8,128)}), f32[8,24,256]{2,1,0:T(8,128)S(1)}, u32[]{:S(2)}, u32[]{:S(2)}) async-start(f32[8,24,256]{2,1,0:T(8,128)} %get-tuple-element.31), calls=%async_computation.3 | async-start | bytes 393216 | tf_op jit(solution)/shard_map/all_to_all | solution.py:552
  134.2 6.0 %products.1.product_hbm = f32[3,2048,256]{2,1,0:T(8,128)} custom-call(bf16[16,400,128]{2,1,0:T(8,128)(2,1)} %copy-done, bf16[16,400,128]{2,1,0:T(8,128)(2,1)} %copy-done.1, bf16[3,256,256]{2,1,0:T(8,128)(2,1)} %get-tuple-element.25.upper_hbm, bf16[3,256,256]{2,1,0:T(8,128)(2,1)} %get-tuple-element.26.lower_hbm), custom_call_target="tpu_custom_call" | custom-call | flops 1610612736 | bytes 10000000 | tf_op jit(solution)/shard_map/products/pallas_call | solution.py:350
  140.3 0.8 all-to-all-done.3.refs_18_
  141.0 7.4 %finals.1 = (f32[3,128,256]{2,1,0:T(8,128)}, f32[3,128,256]{2,1,0:T(8,128)}, bf16[3,2048,256]{2,1,0:T(8,128)(2,1)}, f32[16,2048]{1,0:T(8,128)}, bf16[16,2048]{1,...) custom-call(s32[5]{0:T(128)S(1)} %stack.23.place_ref, f32[3,2048,256]{2,1,0:T(8,128)} %products.1.product_hbm, ...), custom_call_target="tpu_custom_call" | custom-call | flops 10000000 | bytes 16000000 | tf_op jit(solution)/shard_map/finals/pallas_call | solution.py:448
  (46 shorter events, 0.2 us)
Async XLA Ops:
  0.7 34.6 %copy-start.14 = (bf16[3,3072,256]{2,1,0:T(8,128)(2,1)S(1)}, bf16[3,3072,256]{2,1,0:T(8,128)(2,1)}, u32[]{:S(2)}) copy-start(bf16[3,3072,256]{2,1,0:T(8,128)(2,1)} %param.12) | copy-start | bytes 14155780
  35.3 16.5 %copy-start = (bf16[16,400,128]{2,1,0:T(8,128)(2,1)}, bf16[16,400,128]{2,1,0:T(8,128)(2,1)S(1)}, u32[]{:S(2)}) copy-start(bf16[16,400,128]{2,1,0:T(8,128)(2,1)S(1)} %all_to_all.20.ends_hbm.near_ref.near_hbm) | copy-start | bytes 4915204
  35.3 16.5 %collective-permute-start = (bf16[16,400,128]{2,1,0:T(8,128)(2,1)S(1)}, bf16[16,400,128]{2,1,0:T(8,128)(2,1)S(1)}, u32[]{:S(2)}, u32[]{:S(2)}) collective-permute-start(bf16[16,400,128]{2,1,0:T(8,128)(2,1)S(1)} %all_to_all.20.ends_hbm.near_ref.near_hbm), channel_id=1, source_target_pairs={{0,1},{1,0},{2,3},{3,2},{4,5},{5,4},{6,7},{7,6},{8,9},{9,8},{10,11... | collective-permute-start | bytes 4915208 | tf_op jit(solution)/shard_map/ppermute | solution.py:524
  51.8 6.5 %copy-start.2 = (f32[3,128,256]{2,1,0:T(8,128)S(1)}, f32[3,128,256]{2,1,0:T(8,128)}, u32[]{:S(2)}) copy-start(f32[3,128,256]{2,1,0:T(8,128)} %refs_19_.1) | copy-start | bytes 1179652
  51.9 2.9 %copy-start.1 = (bf16[16,400,128]{2,1,0:T(8,128)(2,1)}, bf16[16,400,128]{2,1,0:T(8,128)(2,1)S(1)}, u32[]{:S(2)}) copy-start(bf16[16,400,128]{2,1,0:T(8,128)(2,1)S(1)} %collective-permute-done.far_ref.far_hbm) | copy-start | bytes 4915204
  54.7 35.4 %all-to-all-start.1 = ((f32[16,56,256]{2,1,0:T(8,128)}), f32[16,56,256]{2,1,0:T(8,128)S(1)}, u32[]{:S(2)}, u32[]{:S(2)}) async-start(f32[16,56,256]{2,1,0:T(8,128)} %low_parts.1), calls=%async_computation.1 | async-start | bytes 1835008 | tf_op jit(solution)/shard_map/all_to_all | solution.py:546
  58.4 17.5 %collective-permute-start.6 = (f32[1,3,64,256]{3,2,1,0:T(8,128)S(1)}, f32[1,3,64,256]{3,2,1,0:T(8,128)S(1)}, u32[]{:S(2)}, u32[]{:S(2)}) collective-permute-start(f32[1,3,64,256]{3,2,1,0:T(8,128)S(1)} %get-tuple-element.41), channel_id=1, source_target_pairs={{0,24},{8,0},{16,8},{24,16},{1,25},{9,1},{17,9},{25,17},{2,26},{10... | collective-permute-start | bytes 589832 | tf_op jit(solution)/shard_map/ppermute | solution.py:500
  61.5 16.0 %collective-permute-start.5 = (f32[1,3,64,256]{3,2,1,0:T(8,128)S(1)}, f32[1,3,64,256]{3,2,1,0:T(8,128)S(1)}, u32[]{:S(2)}, u32[]{:S(2)}) collective-permute-start(f32[1,3,64,256]{3,2,1,0:T(8,128)S(1)} %get-tuple-element.41), channel_id=1, source_target_pairs={{0,16},{8,24},{16,0},{24,8},{1,17},{9,25},{17,1},{25,9},{2,18},{10... | collective-permute-start | bytes 589832 | tf_op jit(solution)/shard_map/ppermute | solution.py:500
  62.4 18.0 %collective-permute-start.4 = (f32[1,3,64,256]{3,2,1,0:T(8,128)S(1)}, f32[1,3,64,256]{3,2,1,0:T(8,128)S(1)}, u32[]{:S(2)}, u32[]{:S(2)}) collective-permute-start(f32[1,3,64,256]{3,2,1,0:T(8,128)S(1)} %get-tuple-element.41), channel_id=1, source_target_pairs={{0,8},{8,16},{16,24},{24,0},{1,9},{9,17},{17,25},{25,1},{2,10},{10... | collective-permute-start | bytes 589832 | tf_op jit(solution)/shard_map/ppermute | solution.py:500
  63.2 17.1 %collective-permute-start.3 = (f32[1,3,64,256]{3,2,1,0:T(8,128)S(1)}, f32[1,3,64,256]{3,2,1,0:T(8,128)S(1)}, u32[]{:S(2)}, u32[]{:S(2)}) collective-permute-start(f32[1,3,64,256]{3,2,1,0:T(8,128)S(1)} %get-tuple-element.42), channel_id=1, source_target_pairs={{0,96},{32,0},{64,32},{96,64},{1,97},{33,1},{65,33},{97,65},{2,98}... | collective-permute-start | bytes 589832 | tf_op jit(solution)/shard_map/ppermute | solution.py:500
  66.0 14.4 %collective-permute-start.2 = (f32[1,3,64,256]{3,2,1,0:T(8,128)S(1)}, f32[1,3,64,256]{3,2,1,0:T(8,128)S(1)}, u32[]{:S(2)}, u32[]{:S(2)}) collective-permute-start(f32[1,3,64,256]{3,2,1,0:T(8,128)S(1)} %get-tuple-element.42), channel_id=1, source_target_pairs={{0,64},{32,96},{64,0},{96,32},{1,65},{33,97},{65,1},{97,33},{2,66}... | collective-permute-start | bytes 589832 | tf_op jit(solution)/shard_map/ppermute | solution.py:500
  76.0 6.9 %copy-start.8 = (f32[1,3,64,256]{3,2,1,0:T(8,128)}, f32[1,3,64,256]{3,2,1,0:T(8,128)S(1)}, u32[]{:S(2)}) copy-start(f32[1,3,64,256]{3,2,1,0:T(8,128)S(1)} %collective-permute-done.6.refs_5_) | copy-start | bytes 589828
  76.0 6.9 %collective-permute-start.1 = (f32[1,3,64,256]{3,2,1,0:T(8,128)S(1)}, f32[1,3,64,256]{3,2,1,0:T(8,128)S(1)}, u32[]{:S(2)}, u32[]{:S(2)}) collective-permute-start(f32[1,3,64,256]{3,2,1,0:T(8,128)S(1)} %get-tuple-element.42), channel_id=1, source_target_pairs={{0,32},{32,64},{64,96},{96,0},{1,33},{33,65},{65,97},{97,1},{2,34}... | collective-permute-start | bytes 589832 | tf_op jit(solution)/shard_map/ppermute | solution.py:500
  77.5 5.3 %copy-start.9 = (f32[1,3,64,256]{3,2,1,0:T(8,128)}, f32[1,3,64,256]{3,2,1,0:T(8,128)S(1)}, u32[]{:S(2)}) copy-start(f32[1,3,64,256]{3,2,1,0:T(8,128)S(1)} %collective-permute-done.5.refs_4_) | copy-start | bytes 589828
  80.3 2.5 %copy-start.10 = (f32[1,3,64,256]{3,2,1,0:T(8,128)}, f32[1,3,64,256]{3,2,1,0:T(8,128)S(1)}, u32[]{:S(2)}) copy-start(f32[1,3,64,256]{3,2,1,0:T(8,128)S(1)} %collective-permute-done.4.refs_3_) | copy-start | bytes 589828
  80.4 2.5 %copy-start.11 = (f32[1,3,64,256]{3,2,1,0:T(8,128)}, f32[1,3,64,256]{3,2,1,0:T(8,128)S(1)}, u32[]{:S(2)}) copy-start(f32[1,3,64,256]{3,2,1,0:T(8,128)S(1)} %collective-permute-done.3.refs_2_) | copy-start | bytes 589828
  80.4 2.5 %copy-start.12 = (f32[1,3,64,256]{3,2,1,0:T(8,128)}, f32[1,3,64,256]{3,2,1,0:T(8,128)S(1)}, u32[]{:S(2)}) copy-start(f32[1,3,64,256]{3,2,1,0:T(8,128)S(1)} %collective-permute-done.2.refs_1_) | copy-start | bytes 589828
  82.9 0.7 copy-start.13
  86.0 14.7 %collective-permute-start.8 = (f32[4,2,64,256]{3,2,1,0:T(8,128)}, f32[4,2,64,256]{3,2,1,0:T(8,128)S(1)}, u32[]{:S(2)}, u32[]{:S(2)}) collective-permute-start(f32[4,2,64,256]{3,2,1,0:T(8,128)} %get-tuple-element.27.refs_0_), channel_id=1, source_target_pairs={{0,24},{8,0},{16,8},{24,16},{1,25},{9,1},{17,9},{25,17},{2,26},{10... | collective-permute-start | bytes 1572872 | tf_op jit(solution)/shard_map/ppermute | solution.py:500
  87.1 17.3 %collective-permute-start.7 = (f32[4,2,64,256]{3,2,1,0:T(8,128)}, f32[4,2,64,256]{3,2,1,0:T(8,128)S(1)}, u32[]{:S(2)}, u32[]{:S(2)}) collective-permute-start(f32[4,2,64,256]{3,2,1,0:T(8,128)} %get-tuple-element.27.refs_0_), channel_id=1, source_target_pairs={{0,8},{8,16},{16,24},{24,0},{1,9},{9,17},{17,25},{25,1},{2,10},{10... | collective-permute-start | bytes 1572872 | tf_op jit(solution)/shard_map/ppermute | solution.py:500
  88.1 20.9 %collective-permute-start.15 = (f32[4,2,64,256]{3,2,1,0:T(8,128)}, f32[4,2,64,256]{3,2,1,0:T(8,128)S(1)}, u32[]{:S(2)}, u32[]{:S(2)}) collective-permute-start(f32[4,2,64,256]{3,2,1,0:T(8,128)} %get-tuple-element.29.refs_9_), channel_id=1, source_target_pairs={{0,96},{32,0},{64,32},{96,64},{1,97},{33,1},{65,33},{97,65},{2,98}... | collective-permute-start | bytes 1572872 | tf_op jit(solution)/shard_map/ppermute | solution.py:500
  89.6 25.6 %collective-permute-start.14 = (f32[4,2,64,256]{3,2,1,0:T(8,128)}, f32[4,2,64,256]{3,2,1,0:T(8,128)S(1)}, u32[]{:S(2)}, u32[]{:S(2)}) collective-permute-start(f32[4,2,64,256]{3,2,1,0:T(8,128)} %get-tuple-element.29.refs_9_), channel_id=1, source_target_pairs={{0,32},{32,64},{64,96},{96,0},{1,33},{33,65},{65,97},{97,1},{2,34}... | collective-permute-start | bytes 1572872 | tf_op jit(solution)/shard_map/ppermute | solution.py:500
  91.2 35.1 %all-to-all-start.2 = ((f32[16,56,256]{2,1,0:T(8,128)}), f32[16,56,256]{2,1,0:T(8,128)S(1)}, u32[]{:S(2)}, u32[]{:S(2)}) async-start(f32[16,56,256]{2,1,0:T(8,128)} %summed.1), calls=%async_computation.2 | async-start | bytes 1835008 | tf_op jit(solution)/shard_map/all_to_all | solution.py:547
  97.6 19.2 %collective-permute-start.13 = (f32[4,1,64,256]{3,2,1,0:T(8,128)}, f32[4,1,64,256]{3,2,1,0:T(8,128)S(1)}, u32[]{:S(2)}, u32[]{:S(2)}) collective-permute-start(f32[4,1,64,256]{3,2,1,0:T(8,128)} %get-tuple-element.28.refs_5_), channel_id=1, source_target_pairs={{0,24},{8,0},{16,8},{24,16},{1,25},{9,1},{17,9},{25,17},{2,26},{10... | collective-permute-start | bytes 786440 | tf_op jit(solution)/shard_map/ppermute | solution.py:500
  100.7 19.1 %collective-permute-start.12 = (f32[4,1,64,256]{3,2,1,0:T(8,128)}, f32[4,1,64,256]{3,2,1,0:T(8,128)S(1)}, u32[]{:S(2)}, u32[]{:S(2)}) collective-permute-start(f32[4,1,64,256]{3,2,1,0:T(8,128)} %get-tuple-element.28.refs_5_), channel_id=1, source_target_pairs={{0,16},{8,24},{16,0},{24,8},{1,17},{9,25},{17,1},{25,9},{2,18},{10... | collective-permute-start | bytes 786440 | tf_op jit(solution)/shard_map/ppermute | solution.py:500
  104.4 19.1 %collective-permute-start.11 = (f32[4,1,64,256]{3,2,1,0:T(8,128)}, f32[4,1,64,256]{3,2,1,0:T(8,128)S(1)}, u32[]{:S(2)}, u32[]{:S(2)}) collective-permute-start(f32[4,1,64,256]{3,2,1,0:T(8,128)} %get-tuple-element.28.refs_5_), channel_id=1, source_target_pairs={{0,8},{8,16},{16,24},{24,0},{1,9},{9,17},{17,25},{25,1},{2,10},{10... | collective-permute-start | bytes 786440 | tf_op jit(solution)/shard_map/ppermute | solution.py:500
  108.9 14.6 %collective-permute-start.20 = (f32[4,1,64,256]{3,2,1,0:T(8,128)}, f32[4,1,64,256]{3,2,1,0:T(8,128)S(1)}, u32[]{:S(2)}, u32[]{:S(2)}) collective-permute-start(f32[4,1,64,256]{3,2,1,0:T(8,128)} %get-tuple-element.30.refs_14_), channel_id=1, source_target_pairs={{0,96},{32,0},{64,32},{96,64},{1,97},{33,1},{65,33},{97,65},{2,98}... | collective-permute-start | bytes 786440 | tf_op jit(solution)/shard_map/ppermute | solution.py:500
  115.3 10.0 %collective-permute-start.19 = (f32[4,1,64,256]{3,2,1,0:T(8,128)}, f32[4,1,64,256]{3,2,1,0:T(8,128)S(1)}, u32[]{:S(2)}, u32[]{:S(2)}) collective-permute-start(f32[4,1,64,256]{3,2,1,0:T(8,128)} %get-tuple-element.30.refs_14_), channel_id=1, source_target_pairs={{0,64},{32,96},{64,0},{96,32},{1,65},{33,97},{65,1},{97,33},{2,66}... | collective-permute-start | bytes 786440 | tf_op jit(solution)/shard_map/ppermute | solution.py:500
  116.8 8.5 %copy-start.3 = (f32[4,1,64,256]{3,2,1,0:T(8,128)}, f32[4,1,64,256]{3,2,1,0:T(8,128)S(1)}, u32[]{:S(2)}) copy-start(f32[4,1,64,256]{3,2,1,0:T(8,128)S(1)} %collective-permute-done.13.refs_8_) | copy-start | bytes 786436
  116.8 23.4 %collective-permute-start.18 = (f32[4,1,64,256]{3,2,1,0:T(8,128)}, f32[4,1,64,256]{3,2,1,0:T(8,128)}, u32[]{:S(2)}, u32[]{:S(2)}) collective-permute-start(f32[4,1,64,256]{3,2,1,0:T(8,128)} %get-tuple-element.30.refs_14_), channel_id=1, source_target_pairs={{0,32},{32,64},{64,96},{96,0},{1,33},{33,65},{65,97},{97,1},{2,34}... | collective-permute-start | bytes 786440 | tf_op jit(solution)/shard_map/ppermute | solution.py:500
  119.8 5.5 %copy-start.4 = (f32[4,1,64,256]{3,2,1,0:T(8,128)}, f32[4,1,64,256]{3,2,1,0:T(8,128)S(1)}, u32[]{:S(2)}) copy-start(f32[4,1,64,256]{3,2,1,0:T(8,128)S(1)} %collective-permute-done.12.refs_7_) | copy-start | bytes 786436
  119.8 20.5 %collective-permute-start.10 = (f32[2,2,64,256]{3,2,1,0:T(8,128)}, f32[2,2,64,256]{3,2,1,0:T(8,128)}, u32[]{:S(2)}, u32[]{:S(2)}) collective-permute-start(f32[2,2,64,256]{3,2,1,0:T(8,128)} %slice.31), channel_id=1, source_target_pairs={{0,24},{8,0},{16,8},{24,16},{1,25},{9,1},{17,9},{25,17},{2,26},{10... | collective-permute-start | bytes 786440 | tf_op jit(solution)/shard_map/ppermute | solution.py:500
  123.5 1.8 %copy-start.5 = (f32[4,1,64,256]{3,2,1,0:T(8,128)}, f32[4,1,64,256]{3,2,1,0:T(8,128)S(1)}, u32[]{:S(2)}) copy-start(f32[4,1,64,256]{3,2,1,0:T(8,128)S(1)} %collective-permute-done.11.refs_6_) | copy-start | bytes 786436
  123.5 16.7 %collective-permute-start.9 = (f32[2,2,64,256]{3,2,1,0:T(8,128)}, f32[2,2,64,256]{3,2,1,0:T(8,128)}, u32[]{:S(2)}, u32[]{:S(2)}) collective-permute-start(f32[2,2,64,256]{3,2,1,0:T(8,128)} %slice.30), channel_id=1, source_target_pairs={{0,8},{8,16},{16,24},{24,0},{1,9},{9,17},{17,25},{25,1},{2,10},{10... | collective-permute-start | bytes 786440 | tf_op jit(solution)/shard_map/ppermute | solution.py:500
  123.5 1.8 %copy-start.6 = (f32[4,1,64,256]{3,2,1,0:T(8,128)}, f32[4,1,64,256]{3,2,1,0:T(8,128)S(1)}, u32[]{:S(2)}) copy-start(f32[4,1,64,256]{3,2,1,0:T(8,128)S(1)} %collective-permute-done.20.refs_17_) | copy-start | bytes 786436
  123.5 16.7 %collective-permute-start.17 = (f32[2,2,64,256]{3,2,1,0:T(8,128)S(1)}, f32[2,2,64,256]{3,2,1,0:T(8,128)}, u32[]{:S(2)}, u32[]{:S(2)}) collective-permute-start(f32[2,2,64,256]{3,2,1,0:T(8,128)S(1)} %slice.33), channel_id=1, source_target_pairs={{0,96},{32,0},{64,32},{96,64},{1,97},{33,1},{65,33},{97,65},{2,98}... | collective-permute-start | bytes 786440 | tf_op jit(solution)/shard_map/ppermute | solution.py:500
  125.3 0.7 copy-start.7
  126.0 14.3 %collective-permute-start.16 = (f32[2,2,64,256]{3,2,1,0:T(8,128)S(1)}, f32[2,2,64,256]{3,2,1,0:T(8,128)}, u32[]{:S(2)}, u32[]{:S(2)}) collective-permute-start(f32[2,2,64,256]{3,2,1,0:T(8,128)S(1)} %slice.32), channel_id=1, source_target_pairs={{0,32},{32,64},{64,96},{96,0},{1,33},{33,65},{65,97},{97,1},{2,34}... | collective-permute-start | bytes 786440 | tf_op jit(solution)/shard_map/ppermute | solution.py:500
  129.8 11.3 %all-to-all-start.3 = ((f32[8,24,256]{2,1,0:T(8,128)}), f32[8,24,256]{2,1,0:T(8,128)S(1)}, u32[]{:S(2)}, u32[]{:S(2)}) async-start(f32[8,24,256]{2,1,0:T(8,128)} %get-tuple-element.31), calls=%async_computation.3 | async-start | bytes 393216 | tf_op jit(solution)/shard_map/all_to_all | solution.py:552

commit v7 on v6

--- a/solution.py
+++ b/solution.py
@@ -334,12 +334,15 @@
     writes = []
     for role in range(roles):
         finished(reads[role])
-        factor = factor_ref[role].reshape(peers * rows, rank)
-        product_ref[role] = jnp.dot(
-            factor, direction_ref[role, 0], preferred_element_type=jnp.float32
-        ) + jnp.dot(factor, direction_ref[role, 1], preferred_element_type=jnp.float32)
-        pairs = [(product_ref.at[role], out_hbm.at[role])]
-        writes += started(pairs, write_sems.at[pl.ds(role, 1)])
+        for part in range(2):
+            at = slice(part * peers // 2, (part + 1) * peers // 2)
+            factor = factor_ref[role, at].reshape(peers * rows // 2, rank)
+            at = pl.ds(part * peers * rows // 2, peers * rows // 2)
+            product_ref[role, at] = jnp.dot(
+                factor, direction_ref[role, 0], preferred_element_type=jnp.float32
+            ) + jnp.dot(factor, direction_ref[role, 1], preferred_element_type=jnp.float32)
+            pairs = [(product_ref.at[role, at], out_hbm.at[role, at])]
+            writes += started(pairs, write_sems.at[pl.ds(role * 2 + part, 1)])
     finished(writes)
 
 
@@ -357,7 +360,7 @@
             pltpu.VMEM((roles, 2, rank, width), jnp.bfloat16),
             pltpu.VMEM(shape, jnp.float32),
             pltpu.SemaphoreType.DMA((roles, 4)),
-            pltpu.SemaphoreType.DMA((roles,)),
+            pltpu.SemaphoreType.DMA((roles * 2,)),
         ],
         compiler_params=room(20),
         cost_estimate=cost(4 * roles * peers * rows * rank * width, 10**7),

time: 150 us -> 150 us (level)
  no operation moved by 1% of the time
where the time goes in v7:
time: 150 us; the launch traced here: 149 us
  starting transfers between devices  45.2 us (30%)
  blocking collectives  31.5 us (21%)
  Pallas kernels  27.8 us (19%)
  waiting for transfers between devices  26 us (17%)
  matrix products  13.9 us (9%)
  local copies, waits for them, and re-layouts  3.05 us (2%)
    all_to_all x1, blocking collectives, local(): near = lax.all_to_all(near, FS, split_axis=0, concat_axis=0, tiled=True)  31.5 us
    ppermute x20, starting transfers between devices, shift(): return lax.ppermute(x, axis, [(i, (i + by) % 4) for i in range(4)])  30.8 us
    ppermute x20, waiting for transfers between devices, shift(): return lax.ppermute(x, axis, [(i, (i + by) % 4) for i in range(4)])  24.3 us
    dot_general x1, matrix products, local(): jnp.einsum('td,rtw->rwd', saved_input, proj_cot, preferred_element_type=j...  13.9 us
    pallas_call x1, Pallas kernels, finals(): pl.pallas_call(functools.partial(final_kernel, entries), out_shape=[pltpu...  7.42 us
    all_to_all x1, starting transfers between devices, local(): lax.all_to_all(summed(arrived), FS, split_axis=0, concat_axis=0, tiled=True)  6.32 us
    pallas_call x1, Pallas kernels, products(): pl.pallas_call(product_kernel, out_shape=pltpu.HBM(shape, jnp.float32), i...  5.06 us
    all_to_all x1, starting transfers between devices, local(): shared = lax.all_to_all(shared, TP, split_axis=0, concat_axis=0, tiled=True)  4.48 us
  transfers between devices with their start and end apart: 24, of which 8 were waited for; matrix products, arithmetic and copies ran while one was open for 10% of the time, Pallas kernels for 10%

profile of v7, /device:TPU:0, one launch (start us, length us, event | category | flops | bytes accessed | tf_op | source)
XLA Modules:
  0.0 148.6 jit_solution(13719510933416007855)
XLA Ops:
  0.7 0.1 stack.23.place_ref
  0.7 3.1 %packed.1 = bf16[16,400,128]{2,1,0:T(8,128)(2,1)} custom-call(s32[5]{0:T(128)S(1)} %stack.23.place_ref, bf16[3,128,256]{2,1,0:T(8,128)(2,1)} %factor_ref.1, f32[16,3072]{1,0:T(8,128)} %log_hbm.1, f32[16,3072]{1,0:T(8,128)} %cot_hbm.1), custom_call_target="tpu_custom_call" | custom-call | flops 1000000 | bytes 2000000 | tf_op jit(solution)/shard_map/packed/pallas_call | solution.py:91
  3.8 31.5 %all_to_all.20.ends_hbm.near_ref.near_hbm = bf16[16,400,128]{2,1,0:T(8,128)(2,1)S(1)} all-to-all(bf16[16,400,128]{2,1,0:T(8,128)(2,1)} %packed.1), channel_id=1, replica_groups=mesh['z'=4,'x'=4,'y'=4,'c'=2] {'z','x'}, dimensions={0} | all-to-all | bytes 3276800 | tf_op jit(solution)/shard_map/all_to_all | solution.py:526
  35.3 0.0 collective-permute-start
  35.4 13.9 %fusion.grad_ref = f32[3,256,2048]{2,1,0:T(8,128)S(1)} fusion(bf16[3,3072,256]{2,1,0:T(8,128)(2,1)S(1)} %copy-done.14, bf16[3072,2048]{1,0:T(8,128)(2,1)} %input_hbm.1), kind=kOutput, calls=%fused_computation | convolution fusion | flops 9663676416 | bytes 23592960 | tf_op jit(solution)/shard_map/td,rtw->rwd/dot_general | solution.py:546
  49.3 2.5 %gate_columns.1.gate_ref = f32[16,256]{1,0:T(8,128)S(1)} custom-call(s32[5]{0:T(128)S(1)} %stack.23.place_ref, f32[16,3072]{1,0:T(8,128)} %log_hbm.1, f32[16,3072]{1,0:T(8,128)} %cot_hbm.1, bf16[16,400,128]{2,1,0:T(8,128)(2,1)S(1)} %all_to_all.20.ends_hbm.near_ref.near_hbm, bf16[3072,2048]{1,0:T(8,128)(2,1)} %input_hbm.1), custom_call_target="tpu_custom_call" | custom-call | flops 4000000000 | bytes 4000000 | tf_op jit(solution)/shard_map/gate_columns/pallas_call | solution.py:152
  51.8 0.0 copy-start.2
  51.9 2.8 %low_parts.1 = f32[16,56,256]{2,1,0:T(8,128)} custom-call(f32[3,256,2048]{2,1,0:T(8,128)S(1)} %fusion.grad_ref, bf16[16,400,128]{2,1,0:T(8,128)(2,1)S(1)} %all_to_all.20.ends_hbm.near_ref.near_hbm, bf16[16,400,128]{2,1,0:T(8,128)(2,1)S(1)} %collective-permute-done.far_ref.far_hbm, f32[16,256]{1,0:T(8,128)S(1)} %gate_columns.1.gate_ref), custom_call_target="tpu_custom_call" | custom-call | flops 1610612736 | bytes 11000000 | tf_op jit(solution)/shard_map/low_parts/pallas_call | solution.py:203
  54.7 3.6 %all-to-all-start.1 = ((f32[16,56,256]{2,1,0:T(8,128)}), f32[16,56,256]{2,1,0:T(8,128)S(1)}, u32[]{:S(2)}, u32[]{:S(2)}) async-start(f32[16,56,256]{2,1,0:T(8,128)} %low_parts.1), calls=%async_computation.1 | async-start | bytes 1835008 | tf_op jit(solution)/shard_map/all_to_all | solution.py:549
  58.4 3.1 %collective-permute-start.6 = (f32[1,3,64,256]{3,2,1,0:T(8,128)S(1)}, f32[1,3,64,256]{3,2,1,0:T(8,128)S(1)}, u32[]{:S(2)}, u32[]{:S(2)}) collective-permute-start(f32[1,3,64,256]{3,2,1,0:T(8,128)S(1)} %get-tuple-element.41), channel_id=1, source_target_pairs={{0,24},{8,0},{16,8},{24,16},{1,25},{9,1},{17,9},{25,17},{2,26},{10... | collective-permute-start | bytes 589832 | tf_op jit(solution)/shard_map/ppermute | solution.py:503
  61.5 0.8 collective-permute-start.5
  62.4 0.9 collective-permute-start.4
  63.2 2.8 %collective-permute-start.3 = (f32[1,3,64,256]{3,2,1,0:T(8,128)S(1)}, f32[1,3,64,256]{3,2,1,0:T(8,128)S(1)}, u32[]{:S(2)}, u32[]{:S(2)}) collective-permute-start(f32[1,3,64,256]{3,2,1,0:T(8,128)S(1)} %get-tuple-element.42), channel_id=1, source_target_pairs={{0,96},{32,0},{64,32},{96,64},{1,97},{33,1},{65,33},{97,65},{2,98}... | collective-permute-start | bytes 589832 | tf_op jit(solution)/shard_map/ppermute | solution.py:503
  66.0 0.8 collective-permute-start.2
  66.8 9.2 %collective-permute-done.6.refs_5_ = f32[1,3,64,256]{3,2,1,0:T(8,128)S(1)} collective-permute-done((f32[1,3,64,256]{3,2,1,0:T(8,128)S(1)}, f32[1,3,64,256]{3,2,1,0:T(8,128)S(1)}, u32[]{:S(2)}, u32[]{:S(2)}) %collective-permute-start.6) | collective-permute-done | bytes 196640 | tf_op jit(solution)/shard_map/ppermute | solution.py:503
  76.0 1.5 %collective-permute-start.1 = (f32[1,3,64,256]{3,2,1,0:T(8,128)S(1)}, f32[1,3,64,256]{3,2,1,0:T(8,128)S(1)}, u32[]{:S(2)}, u32[]{:S(2)}) collective-permute-start(f32[1,3,64,256]{3,2,1,0:T(8,128)S(1)} %get-tuple-element.42), channel_id=1, source_target_pairs={{0,32},{32,64},{64,96},{96,0},{1,33},{33,65},{65,97},{97,1},{2,34}... | collective-permute-start | bytes 589832 | tf_op jit(solution)/shard_map/ppermute | solution.py:503
  77.5 0.1 collective-permute-done.5.refs_4_
  77.5 2.8 %collective-permute-done.4.refs_3_ = f32[1,3,64,256]{3,2,1,0:T(8,128)S(1)} collective-permute-done((f32[1,3,64,256]{3,2,1,0:T(8,128)S(1)}, f32[1,3,64,256]{3,2,1,0:T(8,128)S(1)}, u32[]{:S(2)}, u32[]{:S(2)}) %collective-permute-start.4) | collective-permute-done | bytes 196640 | tf_op jit(solution)/shard_map/ppermute | solution.py:503
  80.4 0.0 copy-start.12
  80.4 2.5 %collective-permute-done.1.refs_0_ = f32[1,3,64,256]{3,2,1,0:T(8,128)S(1)} collective-permute-done((f32[1,3,64,256]{3,2,1,0:T(8,128)S(1)}, f32[1,3,64,256]{3,2,1,0:T(8,128)S(1)}, u32[]{:S(2)}, u32[]{:S(2)}) %collective-permute-start.1) | collective-permute-done | bytes 196640 | tf_op jit(solution)/shard_map/ppermute | solution.py:503
  82.9 0.0 copy-start.13
  82.9 0.7 copy-done.13
  83.6 2.4 %joined.1 = (f32[4,2,64,256]{3,2,1,0:T(8,128)}, f32[4,2,64,256]{3,2,1,0:T(8,128)}, f32[4,1,64,256]{3,2,1,0:T(8,128)}, f32[4,1,64,256]{3,2,1,0:T(8,128)}) custom-call(f32[3,128,256]{2,1,0:T(8,128)} %refs_19_.1, f32[1,3,64,256]{3,2,1,0:T(8,128)} %copy-done.13, f32[1,3,64,256]{3,2,1,0:T(8,128)} %copy-done.12, f32[1,3,64,256]{3,2,1,0:T(8,128)} %copy-done.11, ...), custom_call_target="tpu_custom_call" | custom-call | flops 1000000 | bytes 6000000 | tf_op jit(solution)/shard_map/joined/pallas_call | solution.py:486
  86.0 1.1 collective-permute-start.8
  87.1 1.0 collective-permute-start.7
  88.1 1.5 %collective-permute-start.15 = (f32[4,2,64,256]{3,2,1,0:T(8,128)}, f32[4,2,64,256]{3,2,1,0:T(8,128)S(1)}, u32[]{:S(2)}, u32[]{:S(2)}) collective-permute-start(f32[4,2,64,256]{3,2,1,0:T(8,128)} %get-tuple-element.29.refs_9_), channel_id=1, source_target_pairs={{0,96},{32,0},{64,32},{96,64},{1,97},{33,1},{65,33},{97,65},{2,98}... | collective-permute-start | bytes 1572872 | tf_op jit(solution)/shard_map/ppermute | solution.py:503
  89.6 0.5 collective-permute-start.14
  90.1 1.1 summed.1
  91.2 6.3 %all-to-all-start.2 = ((f32[16,56,256]{2,1,0:T(8,128)}), f32[16,56,256]{2,1,0:T(8,128)S(1)}, u32[]{:S(2)}, u32[]{:S(2)}) async-start(f32[16,56,256]{2,1,0:T(8,128)} %summed.1), calls=%async_computation.2 | async-start | bytes 1835008 | tf_op jit(solution)/shard_map/all_to_all | solution.py:550
  97.6 3.1 %collective-permute-start.13 = (f32[4,1,64,256]{3,2,1,0:T(8,128)}, f32[4,1,64,256]{3,2,1,0:T(8,128)S(1)}, u32[]{:S(2)}, u32[]{:S(2)}) collective-permute-start(f32[4,1,64,256]{3,2,1,0:T(8,128)} %get-tuple-element.28.refs_5_), channel_id=1, source_target_pairs={{0,24},{8,0},{16,8},{24,16},{1,25},{9,1},{17,9},{25,17},{2,26},{10... | collective-permute-start | bytes 786440 | tf_op jit(solution)/shard_map/ppermute | solution.py:503
  100.7 0.9 collective-permute-start.12
  101.6 2.8 %collective-permute-done.7.refs_1_ = f32[4,2,64,256]{3,2,1,0:T(8,128)S(1)} collective-permute-done((f32[4,2,64,256]{3,2,1,0:T(8,128)}, f32[4,2,64,256]{3,2,1,0:T(8,128)S(1)}, u32[]{:S(2)}, u32[]{:S(2)}) %collective-permute-start.7) | collective-permute-done | bytes 524320 | tf_op jit(solution)/shard_map/ppermute | solution.py:503
  104.4 0.3 collective-permute-start.11
  104.7 4.3 %collective-permute-done.15.refs_11_ = f32[4,2,64,256]{3,2,1,0:T(8,128)S(1)} collective-permute-done((f32[4,2,64,256]{3,2,1,0:T(8,128)}, f32[4,2,64,256]{3,2,1,0:T(8,128)S(1)}, u32[]{:S(2)}, u32[]{:S(2)}) %collective-permute-start.15) | collective-permute-done | bytes 524320 | tf_op jit(solution)/shard_map/ppermute | solution.py:503
  108.9 3.7 %collective-permute-start.20 = (f32[4,1,64,256]{3,2,1,0:T(8,128)}, f32[4,1,64,256]{3,2,1,0:T(8,128)S(1)}, u32[]{:S(2)}, u32[]{:S(2)}) collective-permute-start(f32[4,1,64,256]{3,2,1,0:T(8,128)} %get-tuple-element.30.refs_14_), channel_id=1, source_target_pairs={{0,96},{32,0},{64,32},{96,64},{1,97},{33,1},{65,33},{97,65},{2,98}... | collective-permute-start | bytes 786440 | tf_op jit(solution)/shard_map/ppermute | solution.py:503
  112.7 2.6 %collective-permute-done.14.refs_10_ = f32[4,2,64,256]{3,2,1,0:T(8,128)S(1)} collective-permute-done((f32[4,2,64,256]{3,2,1,0:T(8,128)}, f32[4,2,64,256]{3,2,1,0:T(8,128)S(1)}, u32[]{:S(2)}, u32[]{:S(2)}) %collective-permute-start.14) | collective-permute-done | bytes 524320 | tf_op jit(solution)/shard_map/ppermute | solution.py:503
  115.3 0.7 slice.31
  116.0 0.7 slice.30
  116.8 3.0 %collective-permute-start.18 = (f32[4,1,64,256]{3,2,1,0:T(8,128)}, f32[4,1,64,256]{3,2,1,0:T(8,128)}, u32[]{:S(2)}, u32[]{:S(2)}) collective-permute-start(f32[4,1,64,256]{3,2,1,0:T(8,128)} %get-tuple-element.30.refs_14_), channel_id=1, source_target_pairs={{0,32},{32,64},{64,96},{96,0},{1,33},{33,65},{65,97},{97,1},{2,34}... | collective-permute-start | bytes 786440 | tf_op jit(solution)/shard_map/ppermute | solution.py:503
  119.8 3.7 %collective-permute-start.10 = (f32[2,2,64,256]{3,2,1,0:T(8,128)}, f32[2,2,64,256]{3,2,1,0:T(8,128)}, u32[]{:S(2)}, u32[]{:S(2)}) collective-permute-start(f32[2,2,64,256]{3,2,1,0:T(8,128)} %slice.31), channel_id=1, source_target_pairs={{0,24},{8,0},{16,8},{24,16},{1,25},{9,1},{17,9},{25,17},{2,26},{10... | collective-permute-start | bytes 786440 | tf_op jit(solution)/shard_map/ppermute | solution.py:503
  123.5 1.7 %collective-permute-start.17 = (f32[2,2,64,256]{3,2,1,0:T(8,128)S(1)}, f32[2,2,64,256]{3,2,1,0:T(8,128)}, u32[]{:S(2)}, u32[]{:S(2)}) collective-permute-start(f32[2,2,64,256]{3,2,1,0:T(8,128)S(1)} %slice.33), channel_id=1, source_target_pairs={{0,96},{32,0},{64,32},{96,64},{1,97},{33,1},{65,33},{97,65},{2,98}... | collective-permute-start | bytes 786440 | tf_op jit(solution)/shard_map/ppermute | solution.py:503
  125.3 0.7 copy-done.7
  126.0 0.4 collective-permute-start.16
  126.4 3.4 %moments.1 = (f32[3,256,256]{2,1,0:T(8,128)}, f32[3,256,256]{2,1,0:T(8,128)}, bf16[3,256,256]{2,1,0:T(8,128)(2,1)}, bf16[3,256,256]{2,1,0:T(8,128)(2,1)}, f32[8,24,256]{2,1,0:T(8,128)}) custom-call(s32[5]{0:T(128)S(1)} %stack.23.place_ref, f32[16,56,256]{2,1,0:T(8,128)S(1)} %all-to-all-done.2.sums_ref, f32[3,256,256]{2,1,0:T(8,128)} %first_hbm.1, ...), custom_call_target="tpu_custom_call" | custom-call | flops 10000000 | bytes 6000000 | tf_op jit(solution)/shard_map/moments/pallas_call | solution.py:292
  129.8 4.5 %all-to-all-start.3 = ((f32[8,24,256]{2,1,0:T(8,128)}), f32[8,24,256]{2,1,0:T(8,128)S(1)}, u32[]{:S(2)}, u32[]{:S(2)}) async-start(f32[8,24,256]{2,1,0:T(8,128)} %get-tuple-element.31), calls=%async_computation.3 | async-start | bytes 393216 | tf_op jit(solution)/shard_map/all_to_all | solution.py:555
  134.2 5.1 %products.1.product_hbm = f32[3,2048,256]{2,1,0:T(8,128)} custom-call(bf16[16,400,128]{2,1,0:T(8,128)(2,1)} %copy-done, bf16[16,400,128]{2,1,0:T(8,128)(2,1)} %copy-done.1, bf16[3,256,256]{2,1,0:T(8,128)(2,1)} %get-tuple-element.25.upper_hbm, bf16[3,256,256]{2,1,0:T(8,128)(2,1)} %get-tuple-element.26.lower_hbm), custom_call_target="tpu_custom_call" | custom-call | flops 1610612736 | bytes 10000000 | tf_op jit(solution)/shard_map/products/pallas_call | solution.py:353
  139.4 1.7 %all-to-all-done.3.refs_18_ = f32[8,24,256]{2,1,0:T(8,128)S(1)} async-done(((f32[8,24,256]{2,1,0:T(8,128)}), f32[8,24,256]{2,1,0:T(8,128)S(1)}, u32[]{:S(2)}, u32[]{:S(2)}) %all-to-all-start.3) | async-done | bytes 196640 | tf_op jit(solution)/shard_map/all_to_all | solution.py:555
  141.0 7.4 %finals.1 = (f32[3,128,256]{2,1,0:T(8,128)}, f32[3,128,256]{2,1,0:T(8,128)}, bf16[3,2048,256]{2,1,0:T(8,128)(2,1)}, f32[16,2048]{1,0:T(8,128)}, bf16[16,2048]{1,...) custom-call(s32[5]{0:T(128)S(1)} %stack.23.place_ref, f32[3,2048,256]{2,1,0:T(8,128)} %products.1.product_hbm, ...), custom_call_target="tpu_custom_call" | custom-call | flops 10000000 | bytes 16000000 | tf_op jit(solution)/shard_map/finals/pallas_call | solution.py:451
  (46 shorter events, 0.2 us)
Async XLA Ops:
  0.7 34.6 %copy-start.14 = (bf16[3,3072,256]{2,1,0:T(8,128)(2,1)S(1)}, bf16[3,3072,256]{2,1,0:T(8,128)(2,1)}, u32[]{:S(2)}) copy-start(bf16[3,3072,256]{2,1,0:T(8,128)(2,1)} %param.12) | copy-start | bytes 14155780
  35.3 16.5 %copy-start = (bf16[16,400,128]{2,1,0:T(8,128)(2,1)}, bf16[16,400,128]{2,1,0:T(8,128)(2,1)S(1)}, u32[]{:S(2)}) copy-start(bf16[16,400,128]{2,1,0:T(8,128)(2,1)S(1)} %all_to_all.20.ends_hbm.near_ref.near_hbm) | copy-start | bytes 4915204
  35.3 16.5 %collective-permute-start = (bf16[16,400,128]{2,1,0:T(8,128)(2,1)S(1)}, bf16[16,400,128]{2,1,0:T(8,128)(2,1)S(1)}, u32[]{:S(2)}, u32[]{:S(2)}) collective-permute-start(bf16[16,400,128]{2,1,0:T(8,128)(2,1)S(1)} %all_to_all.20.ends_hbm.near_ref.near_hbm), channel_id=1, source_target_pairs={{0,1},{1,0},{2,3},{3,2},{4,5},{5,4},{6,7},{7,6},{8,9},{9,8},{10,11... | collective-permute-start | bytes 4915208 | tf_op jit(solution)/shard_map/ppermute | solution.py:527
  51.8 6.5 %copy-start.2 = (f32[3,128,256]{2,1,0:T(8,128)S(1)}, f32[3,128,256]{2,1,0:T(8,128)}, u32[]{:S(2)}) copy-start(f32[3,128,256]{2,1,0:T(8,128)} %refs_19_.1) | copy-start | bytes 1179652
  51.9 2.9 %copy-start.1 = (bf16[16,400,128]{2,1,0:T(8,128)(2,1)}, bf16[16,400,128]{2,1,0:T(8,128)(2,1)S(1)}, u32[]{:S(2)}) copy-start(bf16[16,400,128]{2,1,0:T(8,128)(2,1)S(1)} %collective-permute-done.far_ref.far_hbm) | copy-start | bytes 4915204
  54.7 35.4 %all-to-all-start.1 = ((f32[16,56,256]{2,1,0:T(8,128)}), f32[16,56,256]{2,1,0:T(8,128)S(1)}, u32[]{:S(2)}, u32[]{:S(2)}) async-start(f32[16,56,256]{2,1,0:T(8,128)} %low_parts.1), calls=%async_computation.1 | async-start | bytes 1835008 | tf_op jit(solution)/shard_map/all_to_all | solution.py:549
  58.4 17.5 %collective-permute-start.6 = (f32[1,3,64,256]{3,2,1,0:T(8,128)S(1)}, f32[1,3,64,256]{3,2,1,0:T(8,128)S(1)}, u32[]{:S(2)}, u32[]{:S(2)}) collective-permute-start(f32[1,3,64,256]{3,2,1,0:T(8,128)S(1)} %get-tuple-element.41), channel_id=1, source_target_pairs={{0,24},{8,0},{16,8},{24,16},{1,25},{9,1},{17,9},{25,17},{2,26},{10... | collective-permute-start | bytes 589832 | tf_op jit(solution)/shard_map/ppermute | solution.py:503
  61.5 16.0 %collective-permute-start.5 = (f32[1,3,64,256]{3,2,1,0:T(8,128)S(1)}, f32[1,3,64,256]{3,2,1,0:T(8,128)S(1)}, u32[]{:S(2)}, u32[]{:S(2)}) collective-permute-start(f32[1,3,64,256]{3,2,1,0:T(8,128)S(1)} %get-tuple-element.41), channel_id=1, source_target_pairs={{0,16},{8,24},{16,0},{24,8},{1,17},{9,25},{17,1},{25,9},{2,18},{10... | collective-permute-start | bytes 589832 | tf_op jit(solution)/shard_map/ppermute | solution.py:503
  62.4 18.0 %collective-permute-start.4 = (f32[1,3,64,256]{3,2,1,0:T(8,128)S(1)}, f32[1,3,64,256]{3,2,1,0:T(8,128)S(1)}, u32[]{:S(2)}, u32[]{:S(2)}) collective-permute-start(f32[1,3,64,256]{3,2,1,0:T(8,128)S(1)} %get-tuple-element.41), channel_id=1, source_target_pairs={{0,8},{8,16},{16,24},{24,0},{1,9},{9,17},{17,25},{25,1},{2,10},{10... | collective-permute-start | bytes 589832 | tf_op jit(solution)/shard_map/ppermute | solution.py:503
  63.2 17.1 %collective-permute-start.3 = (f32[1,3,64,256]{3,2,1,0:T(8,128)S(1)}, f32[1,3,64,256]{3,2,1,0:T(8,128)S(1)}, u32[]{:S(2)}, u32[]{:S(2)}) collective-permute-start(f32[1,3,64,256]{3,2,1,0:T(8,128)S(1)} %get-tuple-element.42), channel_id=1, source_target_pairs={{0,96},{32,0},{64,32},{96,64},{1,97},{33,1},{65,33},{97,65},{2,98}... | collective-permute-start | bytes 589832 | tf_op jit(solution)/shard_map/ppermute | solution.py:503
  66.0 14.4 %collective-permute-start.2 = (f32[1,3,64,256]{3,2,1,0:T(8,128)S(1)}, f32[1,3,64,256]{3,2,1,0:T(8,128)S(1)}, u32[]{:S(2)}, u32[]{:S(2)}) collective-permute-start(f32[1,3,64,256]{3,2,1,0:T(8,128)S(1)} %get-tuple-element.42), channel_id=1, source_target_pairs={{0,64},{32,96},{64,0},{96,32},{1,65},{33,97},{65,1},{97,33},{2,66}... | collective-permute-start | bytes 589832 | tf_op jit(solution)/shard_map/ppermute | solution.py:503
  76.0 6.9 %copy-start.8 = (f32[1,3,64,256]{3,2,1,0:T(8,128)}, f32[1,3,64,256]{3,2,1,0:T(8,128)S(1)}, u32[]{:S(2)}) copy-start(f32[1,3,64,256]{3,2,1,0:T(8,128)S(1)} %collective-permute-done.6.refs_5_) | copy-start | bytes 589828
  76.0 6.9 %collective-permute-start.1 = (f32[1,3,64,256]{3,2,1,0:T(8,128)S(1)}, f32[1,3,64,256]{3,2,1,0:T(8,128)S(1)}, u32[]{:S(2)}, u32[]{:S(2)}) collective-permute-start(f32[1,3,64,256]{3,2,1,0:T(8,128)S(1)} %get-tuple-element.42), channel_id=1, source_target_pairs={{0,32},{32,64},{64,96},{96,0},{1,33},{33,65},{65,97},{97,1},{2,34}... | collective-permute-start | bytes 589832 | tf_op jit(solution)/shard_map/ppermute | solution.py:503
  77.5 5.3 %copy-start.9 = (f32[1,3,64,256]{3,2,1,0:T(8,128)}, f32[1,3,64,256]{3,2,1,0:T(8,128)S(1)}, u32[]{:S(2)}) copy-start(f32[1,3,64,256]{3,2,1,0:T(8,128)S(1)} %collective-permute-done.5.refs_4_) | copy-start | bytes 589828
  80.3 2.5 %copy-start.10 = (f32[1,3,64,256]{3,2,1,0:T(8,128)}, f32[1,3,64,256]{3,2,1,0:T(8,128)S(1)}, u32[]{:S(2)}) copy-start(f32[1,3,64,256]{3,2,1,0:T(8,128)S(1)} %collective-permute-done.4.refs_3_) | copy-start | bytes 589828
  80.4 2.5 %copy-start.11 = (f32[1,3,64,256]{3,2,1,0:T(8,128)}, f32[1,3,64,256]{3,2,1,0:T(8,128)S(1)}, u32[]{:S(2)}) copy-start(f32[1,3,64,256]{3,2,1,0:T(8,128)S(1)} %collective-permute-done.3.refs_2_) | copy-start | bytes 589828
  80.4 2.5 %copy-start.12 = (f32[1,3,64,256]{3,2,1,0:T(8,128)}, f32[1,3,64,256]{3,2,1,0:T(8,128)S(1)}, u32[]{:S(2)}) copy-start(f32[1,3,64,256]{3,2,1,0:T(8,128)S(1)} %collective-permute-done.2.refs_1_) | copy-start | bytes 589828
  82.9 0.7 copy-start.13
  86.0 14.7 %collective-permute-start.8 = (f32[4,2,64,256]{3,2,1,0:T(8,128)}, f32[4,2,64,256]{3,2,1,0:T(8,128)S(1)}, u32[]{:S(2)}, u32[]{:S(2)}) collective-permute-start(f32[4,2,64,256]{3,2,1,0:T(8,128)} %get-tuple-element.27.refs_0_), channel_id=1, source_target_pairs={{0,24},{8,0},{16,8},{24,16},{1,25},{9,1},{17,9},{25,17},{2,26},{10... | collective-permute-start | bytes 1572872 | tf_op jit(solution)/shard_map/ppermute | solution.py:503
  87.1 17.3 %collective-permute-start.7 = (f32[4,2,64,256]{3,2,1,0:T(8,128)}, f32[4,2,64,256]{3,2,1,0:T(8,128)S(1)}, u32[]{:S(2)}, u32[]{:S(2)}) collective-permute-start(f32[4,2,64,256]{3,2,1,0:T(8,128)} %get-tuple-element.27.refs_0_), channel_id=1, source_target_pairs={{0,8},{8,16},{16,24},{24,0},{1,9},{9,17},{17,25},{25,1},{2,10},{10... | collective-permute-start | bytes 1572872 | tf_op jit(solution)/shard_map/ppermute | solution.py:503
  88.1 20.9 %collective-permute-start.15 = (f32[4,2,64,256]{3,2,1,0:T(8,128)}, f32[4,2,64,256]{3,2,1,0:T(8,128)S(1)}, u32[]{:S(2)}, u32[]{:S(2)}) collective-permute-start(f32[4,2,64,256]{3,2,1,0:T(8,128)} %get-tuple-element.29.refs_9_), channel_id=1, source_target_pairs={{0,96},{32,0},{64,32},{96,64},{1,97},{33,1},{65,33},{97,65},{2,98}... | collective-permute-start | bytes 1572872 | tf_op jit(solution)/shard_map/ppermute | solution.py:503
  89.6 25.6 %collective-permute-start.14 = (f32[4,2,64,256]{3,2,1,0:T(8,128)}, f32[4,2,64,256]{3,2,1,0:T(8,128)S(1)}, u32[]{:S(2)}, u32[]{:S(2)}) collective-permute-start(f32[4,2,64,256]{3,2,1,0:T(8,128)} %get-tuple-element.29.refs_9_), channel_id=1, source_target_pairs={{0,32},{32,64},{64,96},{96,0},{1,33},{33,65},{65,97},{97,1},{2,34}... | collective-permute-start | bytes 1572872 | tf_op jit(solution)/shard_map/ppermute | solution.py:503
  91.2 35.1 %all-to-all-start.2 = ((f32[16,56,256]{2,1,0:T(8,128)}), f32[16,56,256]{2,1,0:T(8,128)S(1)}, u32[]{:S(2)}, u32[]{:S(2)}) async-start(f32[16,56,256]{2,1,0:T(8,128)} %summed.1), calls=%async_computation.2 | async-start | bytes 1835008 | tf_op jit(solution)/shard_map/all_to_all | solution.py:550
  97.6 19.2 %collective-permute-start.13 = (f32[4,1,64,256]{3,2,1,0:T(8,128)}, f32[4,1,64,256]{3,2,1,0:T(8,128)S(1)}, u32[]{:S(2)}, u32[]{:S(2)}) collective-permute-start(f32[4,1,64,256]{3,2,1,0:T(8,128)} %get-tuple-element.28.refs_5_), channel_id=1, source_target_pairs={{0,24},{8,0},{16,8},{24,16},{1,25},{9,1},{17,9},{25,17},{2,26},{10... | collective-permute-start | bytes 786440 | tf_op jit(solution)/shard_map/ppermute | solution.py:503
  100.7 19.1 %collective-permute-start.12 = (f32[4,1,64,256]{3,2,1,0:T(8,128)}, f32[4,1,64,256]{3,2,1,0:T(8,128)S(1)}, u32[]{:S(2)}, u32[]{:S(2)}) collective-permute-start(f32[4,1,64,256]{3,2,1,0:T(8,128)} %get-tuple-element.28.refs_5_), channel_id=1, source_target_pairs={{0,16},{8,24},{16,0},{24,8},{1,17},{9,25},{17,1},{25,9},{2,18},{10... | collective-permute-start | bytes 786440 | tf_op jit(solution)/shard_map/ppermute | solution.py:503
  104.4 19.1 %collective-permute-start.11 = (f32[4,1,64,256]{3,2,1,0:T(8,128)}, f32[4,1,64,256]{3,2,1,0:T(8,128)S(1)}, u32[]{:S(2)}, u32[]{:S(2)}) collective-permute-start(f32[4,1,64,256]{3,2,1,0:T(8,128)} %get-tuple-element.28.refs_5_), channel_id=1, source_target_pairs={{0,8},{8,16},{16,24},{24,0},{1,9},{9,17},{17,25},{25,1},{2,10},{10... | collective-permute-start | bytes 786440 | tf_op jit(solution)/shard_map/ppermute | solution.py:503
  108.9 14.6 %collective-permute-start.20 = (f32[4,1,64,256]{3,2,1,0:T(8,128)}, f32[4,1,64,256]{3,2,1,0:T(8,128)S(1)}, u32[]{:S(2)}, u32[]{:S(2)}) collective-permute-start(f32[4,1,64,256]{3,2,1,0:T(8,128)} %get-tuple-element.30.refs_14_), channel_id=1, source_target_pairs={{0,96},{32,0},{64,32},{96,64},{1,97},{33,1},{65,33},{97,65},{2,98}... | collective-permute-start | bytes 786440 | tf_op jit(solution)/shard_map/ppermute | solution.py:503
  115.3 10.0 %collective-permute-start.19 = (f32[4,1,64,256]{3,2,1,0:T(8,128)}, f32[4,1,64,256]{3,2,1,0:T(8,128)S(1)}, u32[]{:S(2)}, u32[]{:S(2)}) collective-permute-start(f32[4,1,64,256]{3,2,1,0:T(8,128)} %get-tuple-element.30.refs_14_), channel_id=1, source_target_pairs={{0,64},{32,96},{64,0},{96,32},{1,65},{33,97},{65,1},{97,33},{2,66}... | collective-permute-start | bytes 786440 | tf_op jit(solution)/shard_map/ppermute | solution.py:503
  116.8 8.5 %copy-start.3 = (f32[4,1,64,256]{3,2,1,0:T(8,128)}, f32[4,1,64,256]{3,2,1,0:T(8,128)S(1)}, u32[]{:S(2)}) copy-start(f32[4,1,64,256]{3,2,1,0:T(8,128)S(1)} %collective-permute-done.13.refs_8_) | copy-start | bytes 786436
  116.8 22.5 %collective-permute-start.18 = (f32[4,1,64,256]{3,2,1,0:T(8,128)}, f32[4,1,64,256]{3,2,1,0:T(8,128)}, u32[]{:S(2)}, u32[]{:S(2)}) collective-permute-start(f32[4,1,64,256]{3,2,1,0:T(8,128)} %get-tuple-element.30.refs_14_), channel_id=1, source_target_pairs={{0,32},{32,64},{64,96},{96,0},{1,33},{33,65},{65,97},{97,1},{2,34}... | collective-permute-start | bytes 786440 | tf_op jit(solution)/shard_map/ppermute | solution.py:503
  119.8 5.5 %copy-start.4 = (f32[4,1,64,256]{3,2,1,0:T(8,128)}, f32[4,1,64,256]{3,2,1,0:T(8,128)S(1)}, u32[]{:S(2)}) copy-start(f32[4,1,64,256]{3,2,1,0:T(8,128)S(1)} %collective-permute-done.12.refs_7_) | copy-start | bytes 786436
  119.8 19.5 %collective-permute-start.10 = (f32[2,2,64,256]{3,2,1,0:T(8,128)}, f32[2,2,64,256]{3,2,1,0:T(8,128)}, u32[]{:S(2)}, u32[]{:S(2)}) collective-permute-start(f32[2,2,64,256]{3,2,1,0:T(8,128)} %slice.31), channel_id=1, source_target_pairs={{0,24},{8,0},{16,8},{24,16},{1,25},{9,1},{17,9},{25,17},{2,26},{10... | collective-permute-start | bytes 786440 | tf_op jit(solution)/shard_map/ppermute | solution.py:503
  123.5 1.8 %copy-start.5 = (f32[4,1,64,256]{3,2,1,0:T(8,128)}, f32[4,1,64,256]{3,2,1,0:T(8,128)S(1)}, u32[]{:S(2)}) copy-start(f32[4,1,64,256]{3,2,1,0:T(8,128)S(1)} %collective-permute-done.11.refs_6_) | copy-start | bytes 786436
  123.5 15.8 %collective-permute-start.9 = (f32[2,2,64,256]{3,2,1,0:T(8,128)}, f32[2,2,64,256]{3,2,1,0:T(8,128)}, u32[]{:S(2)}, u32[]{:S(2)}) collective-permute-start(f32[2,2,64,256]{3,2,1,0:T(8,128)} %slice.30), channel_id=1, source_target_pairs={{0,8},{8,16},{16,24},{24,0},{1,9},{9,17},{17,25},{25,1},{2,10},{10... | collective-permute-start | bytes 786440 | tf_op jit(solution)/shard_map/ppermute | solution.py:503
  123.5 1.8 %copy-start.6 = (f32[4,1,64,256]{3,2,1,0:T(8,128)}, f32[4,1,64,256]{3,2,1,0:T(8,128)S(1)}, u32[]{:S(2)}) copy-start(f32[4,1,64,256]{3,2,1,0:T(8,128)S(1)} %collective-permute-done.20.refs_17_) | copy-start | bytes 786436
  123.5 15.8 %collective-permute-start.17 = (f32[2,2,64,256]{3,2,1,0:T(8,128)S(1)}, f32[2,2,64,256]{3,2,1,0:T(8,128)}, u32[]{:S(2)}, u32[]{:S(2)}) collective-permute-start(f32[2,2,64,256]{3,2,1,0:T(8,128)S(1)} %slice.33), channel_id=1, source_target_pairs={{0,96},{32,0},{64,32},{96,64},{1,97},{33,1},{65,33},{97,65},{2,98}... | collective-permute-start | bytes 786440 | tf_op jit(solution)/shard_map/ppermute | solution.py:503
  125.3 0.7 copy-start.7
  126.0 13.4 %collective-permute-start.16 = (f32[2,2,64,256]{3,2,1,0:T(8,128)S(1)}, f32[2,2,64,256]{3,2,1,0:T(8,128)}, u32[]{:S(2)}, u32[]{:S(2)}) collective-permute-start(f32[2,2,64,256]{3,2,1,0:T(8,128)S(1)} %slice.32), channel_id=1, source_target_pairs={{0,32},{32,64},{64,96},{96,0},{1,33},{33,65},{65,97},{97,1},{2,34}... | collective-permute-start | bytes 786440 | tf_op jit(solution)/shard_map/ppermute | solution.py:503
  129.8 11.3 %all-to-all-start.3 = ((f32[8,24,256]{2,1,0:T(8,128)}), f32[8,24,256]{2,1,0:T(8,128)S(1)}, u32[]{:S(2)}, u32[]{:S(2)}) async-start(f32[8,24,256]{2,1,0:T(8,128)} %get-tuple-element.31), calls=%async_computation.3 | async-start | bytes 393216 | tf_op jit(solution)/shard_map/all_to_all | solution.py:555
